TPU v7x, 128 devices: a whole 4x4x4 slice. The times are simulated.
128 devices in a mesh: sp: 32 (over z, y, core), tp: 4 (over x).
Axes of the slice: x: 4, y: 4, z: 4, core: 2. Of those that a mesh axis runs over, the one named last changes fastest.
Arguments:
- output_cotangent: bfloat16 [12288, 2048], P('sp'), may hold values from -8 to 8
- chosen_expert_index: int32 [12288, 2], P('sp'), may hold values from 0 to 31, all different within a row; in each aligned block of 384 rows (0 to 383, 384 to 767, ...) at most 40 rows name the same one
- chosen_expert_weight: float32 [12288, 2], P('sp'), may hold values from 0.2 to 1
- expert_slot_tokens: bfloat16 [32, 1280, 2048], P('sp'), may hold values from -48 to 48, as said below
- expert_gate_matrix: bfloat16 [32, 2048, 2048], P('sp', None, 'tp'), may hold values from -0.125 to 0.125
- expert_up_matrix: bfloat16 [32, 2048, 2048], P('sp', None, 'tp'), may hold values from -0.125 to 0.125
- expert_down_matrix: bfloat16 [32, 2048, 2048], P('sp', 'tp'), may hold values from -0.125 to 0.125
- output_projection_matrix: bfloat16 [2048, 2048], P(None, 'tp'), may hold values from -0.125 to 0.125
- recurrence_input: bfloat16 [12288, 2048], P('sp', 'tp'), may hold values from -6 to 6
- branch_activation_values: bfloat16 [12288, 2048], P('sp', 'tp'), may hold values from -6 to 6
- forward_scan_state: float32 [12288, 2048], P('sp', 'tp'), may hold values from -6 to 6
- reverse_scan_state: float32 [12288, 2048], P('sp', 'tp'), may hold values from -6 to 6
- channel_decay_rate: float32 [2048], P('tp'), may hold values from 5.08626302e-07 to 0.01
- position_extra_log_decay: float32 [12288], P('sp'), may hold values from -0.7 to 0, as said below
- recurrence_gate_weights: bfloat16 [8, 256, 256], P('tp'), may hold values from -0.375 to 0.375
- input_gate_weights: bfloat16 [8, 256, 256], P('tp'), may hold values from -0.375 to 0.375
Outputs:
- expert_gate_grad: bfloat16 [32, 2048, 2048], P('sp', None, 'tp')
- expert_up_grad: bfloat16 [32, 2048, 2048], P('sp', None, 'tp')
- expert_down_grad: bfloat16 [32, 2048, 2048], P('sp', 'tp')
- proj_grad: float32 [2048, 2048], P('sp', 'tp')
- branch_grad: bfloat16 [12288, 2048], P('sp', 'tp')
- input_grad: bfloat16 [12288, 2048], P('sp', 'tp')
Inputs may be any that keep to these rules, and one draw needn't show every extreme that they name: `chosen_expert_index`: each row names 2 different experts; among the rows of one index of sp no expert is named more than 40 times, a bound that some block reaches. `expert_slot_tokens`: row s * 40 + c of expert e holds the input of slot c that source s fills for e, slots filled as the steps number them. `position_extra_log_decay`: zero except at a few positions.
All inputs are finite; a program needn't handle non-finite values.
Results may differ from a plain program's by a relative error of at most 0.022.
Values may be sent and summed in bfloat16 or wider, within the bound.
No kernel may reach another device: no remote copies, remote signals or barrier semaphores. Data moves between devices by JAX's collectives and lax.ppermute only.
A program may use at most 192 MiB of HBM per device.

v0:
```python
import jax
import jax.numpy as jnp
from jax import lax
from jax.sharding import PartitionSpec as P

gate_scale_factor = 8.0
clamp_limit = 7.0
glu_alpha = 1.702


def from_everyone(x, axis):
    copies = jnp.broadcast_to(x, (lax.axis_size(axis), *x.shape))
    return lax.all_to_all(copies, axis, split_axis=0, concat_axis=0, tiled=True)


def in_order(blocks, dim):
    blocks = jnp.moveaxis(blocks, 0, dim)
    shape = blocks.shape
    return blocks.reshape(*shape[:dim], shape[dim] * shape[dim + 1], *shape[dim + 2 :])


def gathered_copies(x, axis, dim):
    blocks = from_everyone(x, axis)
    return in_order(blocks, dim)


def gathered_once(x, axis):
    leaves = jax.tree.leaves(x)
    sequence = sorted(range(len(leaves)), key=lambda k: -leaves[k].size)
    width = (1, *leaves[sequence[0]].shape)[-1]
    lines = [
        jnp.pad(leaves[k].reshape(-1), (0, -leaves[k].size % width)).reshape(-1, width)
        for k in sequence
    ]
    both, at, found = (from_everyone(jnp.concatenate(lines), axis), 0, {})
    for k, line in zip(sequence, lines):
        piece = both[:, at : at + len(line)].reshape(len(both), -1)
        found[k] = piece[:, : leaves[k].size].reshape(-1, *leaves[k].shape)
        at += len(line)
    numbers = iter(range(len(leaves)))
    return jax.tree.map(lambda _: found[next(numbers)], x)


def folded_in_pairs(pieces, combine):
    while len(jax.tree.leaves(pieces)[0]) > 1:
        pieces = jax.vmap(combine)(
            *(jax.tree.map(lambda part: part[side::2], pieces) for side in (0, 1))
        )
    return jax.tree.map(lambda part: part[0], pieces)


def prefix(x, axis, combine, identity, reverse):
    count, index = (lax.axis_size(axis), lax.axis_index(axis))
    passed = jnp.arange(count) > index if reverse else jnp.arange(count) < index

    def kept(part, zero, own):
        part = jnp.where(
            passed.reshape(-1, *(1 for _ in own.shape)), part, jnp.asarray(zero, own.dtype)
        )
        return part[::-1] if reverse else part

    pieces = gathered_once(x, axis)
    return folded_in_pairs(jax.tree.map(kept, pieces, identity, x), combine)


def linear_prefix(coef, value):

    def combine(first, second):
        return (first[0] * second[0], second[0] * first[1] + second[1])

    return lax.associative_scan(combine, (coef, value), axis=0)[1]


def affine_join(earlier, later):
    return (earlier[0] * later[0], later[0] * earlier[1] + later[1])


def blockwise(rows, weights):
    count = rows.shape[0]
    split = rows.reshape(count, weights.shape[0], weights.shape[1])
    return jnp.einsum("tbi,bij->tbj", split, weights, preferred_element_type=jnp.float32).reshape(
        count, -1
    )


def blockwise_back(rows, weights):
    count = rows.shape[0]
    split = rows.reshape(count, weights.shape[0], weights.shape[1])
    return jnp.einsum("tbj,bij->tbi", split, weights, preferred_element_type=jnp.float32).reshape(
        count, -1
    )


def expert_grads(expert_slot_tokens, received, d_gate, d_up, act):
    down_grad = jnp.einsum(
        "erf,erd->efd", act, received, preferred_element_type=jnp.float32
    ).astype(jnp.bfloat16)
    gate_grad = jnp.einsum(
        "erd,erf->edf", expert_slot_tokens, d_gate, preferred_element_type=jnp.float32
    ).astype(jnp.bfloat16)
    up_grad = jnp.einsum(
        "erd,erf->edf", expert_slot_tokens, d_up, preferred_element_type=jnp.float32
    ).astype(jnp.bfloat16)
    return (gate_grad, up_grad, down_grad)


def slot_rows(cotangent, chosen_expert_weight, owner, experts, capacity):
    pairs = owner.shape[0] and chosen_expert_weight.shape[0] * chosen_expert_weight.shape[1]
    width = cotangent.shape[1]
    weighted = (
        chosen_expert_weight[:, :, None] * cotangent.astype(jnp.float32)[:, None, :]
    ).astype(jnp.bfloat16)
    padded = jnp.concatenate(
        [weighted.reshape(pairs, width), jnp.zeros((1, width), jnp.bfloat16)], axis=0
    )
    return jnp.take(padded, owner, axis=0).reshape(experts, capacity, width)


def shards(
    output_cotangent,
    chosen_expert_index,
    chosen_expert_weight,
    expert_slot_tokens,
    expert_gate_matrix,
    expert_up_matrix,
    expert_down_matrix,
    output_projection_matrix,
    recurrence_input,
    branch_activation_values,
    forward_scan_state,
    reverse_scan_state,
    channel_decay_rate,
    position_extra_log_decay,
    recurrence_gate_weights,
    input_gate_weights,
):
    n_sp = lax.axis_size("sp")
    n_tp = lax.axis_size("tp")
    tok_rows, model_width = output_cotangent.shape
    top_count = chosen_expert_index.shape[1]
    experts = n_sp * expert_gate_matrix.shape[0]
    capacity = expert_slot_tokens.shape[1] // n_sp
    pairs = tok_rows * top_count
    assigned = chosen_expert_index.reshape(-1)
    onehot = (assigned[:, None] == jnp.arange(experts, dtype=jnp.int32)[None, None, :][0]).astype(
        jnp.int32
    )
    before = jnp.cumsum(onehot, axis=0) - onehot
    target = assigned * capacity + jnp.sum(before * onehot, axis=1)
    owner = (
        jnp.full((experts * capacity,), pairs, jnp.int32)
        .at[target]
        .set(jnp.arange(pairs, dtype=jnp.int32))
    )
    outgoing = slot_rows(output_cotangent, chosen_expert_weight, owner, experts, capacity)
    received = lax.all_to_all(outgoing, "sp", split_axis=0, concat_axis=1, tiled=True)
    gate_pre = jnp.einsum(
        "erd,edf->erf", expert_slot_tokens, expert_gate_matrix, preferred_element_type=jnp.float32
    )
    up_pre = jnp.einsum(
        "erd,edf->erf", expert_slot_tokens, expert_up_matrix, preferred_element_type=jnp.float32
    )
    glu = jnp.minimum(gate_pre, clamp_limit)
    lin = jnp.clip(up_pre, -clamp_limit, clamp_limit)
    sig = jax.nn.sigmoid(glu_alpha * glu)
    silu_part = glu * sig
    act = (silu_part * (lin + 1.0)).astype(jnp.bfloat16)
    d_act = jnp.einsum(
        "erd,efd->erf", received, expert_down_matrix, preferred_element_type=jnp.float32
    )
    d_glu = d_act * (lin + 1.0) * (sig + glu_alpha * silu_part * (1.0 - sig))
    d_gate = jnp.where(gate_pre < clamp_limit, d_glu, 0.0).astype(jnp.bfloat16)
    d_up = jnp.where(jnp.abs(up_pre) < clamp_limit, d_act * silu_part, 0.0).astype(jnp.bfloat16)
    partial_value = jnp.einsum(
        "erf,edf->erd", d_gate, expert_gate_matrix, preferred_element_type=jnp.float32
    )
    partial_value = partial_value + jnp.einsum(
        "erf,edf->erd", d_up, expert_up_matrix, preferred_element_type=jnp.float32
    )
    partial_value = partial_value.astype(jnp.bfloat16)
    weight_grads = expert_grads(expert_slot_tokens, received, d_gate, d_up, act)
    summed = (
        lax.psum_scatter(partial_value, "tp", scatter_dimension=2, tiled=True)
        .astype(jnp.float32)
        .astype(jnp.bfloat16)
    )
    back = lax.all_to_all(summed, "sp", split_axis=1, concat_axis=0, tiled=True)
    width = model_width // n_tp
    cot_part = lax.dynamic_slice_in_dim(
        output_cotangent, lax.axis_index("tp") * width, width, 1
    ).astype(jnp.float32)
    gate_grad, up_grad, down_grad = weight_grads
    columns_here = back.shape[2]
    rows = jnp.take(back.reshape(experts * capacity, columns_here), target, axis=0).astype(
        jnp.float32
    )
    z_part = (cot_part + jnp.sum(rows.reshape(tok_rows, top_count, columns_here), axis=1)).astype(
        jnp.bfloat16
    )
    z_grad = gathered_copies(z_part, "tp", 1)
    recurrence_gate_value = jax.nn.sigmoid(blockwise(recurrence_input, recurrence_gate_weights))
    inp = jax.nn.sigmoid(blockwise(recurrence_input, input_gate_weights))
    log_decay_factor = (
        -gate_scale_factor * recurrence_gate_value * channel_decay_rate[None, :]
        + position_extra_log_decay[:, None]
    )
    decay = jnp.exp(log_decay_factor)
    scale_in = jnp.sqrt(-jnp.expm1(2.0 * log_decay_factor))
    inputs = recurrence_input.astype(jnp.float32)
    xin = scale_in * inp * inputs
    forward_state = decay * forward_scan_state + xin
    backward_state = decay * reverse_scan_state + xin
    mixed_state = (forward_state + backward_state).astype(jnp.bfloat16)
    branch = branch_activation_values.astype(jnp.float32)
    gated = (mixed_state.astype(jnp.float32) * branch).astype(jnp.bfloat16)
    proj_grad = lax.psum_scatter(
        lax.dot_general(
            z_grad, gated, (((0,), (0,)), ((), ())), preferred_element_type=jnp.float32
        ).astype(jnp.bfloat16),
        "sp",
        scatter_dimension=0,
        tiled=True,
    ).astype(jnp.float32)
    d_gated = jnp.dot(z_grad, output_projection_matrix, preferred_element_type=jnp.float32)
    branch_grad = (d_gated * mixed_state.astype(jnp.float32)).astype(jnp.bfloat16)
    d_state = d_gated * branch
    channels = d_state.shape[1]
    zero_row = jnp.zeros((1, channels), jnp.float32)
    later_local = jnp.flip(
        linear_prefix(
            jnp.flip(jnp.concatenate([decay[1:], zero_row], axis=0), 0), jnp.flip(d_state, 0)
        ),
        0,
    )
    earlier_local = linear_prefix(jnp.concatenate([zero_row, decay[:-1]], axis=0), d_state)
    running = jnp.cumsum(log_decay_factor, axis=0)
    whole = running[-1]
    through = jnp.exp(whole)
    neutral = (jnp.ones((channels,), jnp.float32), jnp.zeros((channels,), jnp.float32))
    _, from_above = prefix((through, decay[0] * later_local[0]), "sp", affine_join, neutral, True)
    _, from_below = prefix(
        (through, decay[-1] * earlier_local[-1]), "sp", affine_join, neutral, False
    )
    later = later_local + jnp.exp(whole[None, :] - running) * from_above[None, :]
    earlier = earlier_local + jnp.exp(running - log_decay_factor) * from_below[None, :]
    total = later + earlier
    d_log_a = (
        later * forward_scan_state + earlier * reverse_scan_state
    ) * decay - total * inp * inputs * decay * decay / scale_in
    rec_pre_grad = (
        d_log_a
        * (-gate_scale_factor * channel_decay_rate[None, :])
        * recurrence_gate_value
        * (1.0 - recurrence_gate_value)
    ).astype(jnp.bfloat16)
    inp_pre_grad = (total * scale_in * inputs * inp * (1.0 - inp)).astype(jnp.bfloat16)
    input_grad = (
        total * scale_in * inp
        + blockwise_back(rec_pre_grad, recurrence_gate_weights)
        + blockwise_back(inp_pre_grad, input_gate_weights)
    ).astype(jnp.bfloat16)
    return (gate_grad, up_grad, down_grad, proj_grad, branch_grad, input_grad)


def solution(mesh):
    in_specs = (
        P("sp", None),
        P("sp", None),
        P("sp", None),
        P("sp", None, None),
        P("sp", None, "tp"),
        P("sp", None, "tp"),
        P("sp", "tp", None),
        P(None, "tp"),
        P("sp", "tp"),
        P("sp", "tp"),
        P("sp", "tp"),
        P("sp", "tp"),
        P("tp"),
        P("sp"),
        P("tp", None, None),
        P("tp", None, None),
    )
    out_specs = (
        P("sp", None, "tp"),
        P("sp", None, "tp"),
        P("sp", "tp", None),
        P("sp", "tp"),
        P("sp", "tp"),
        P("sp", "tp"),
    )
    return jax.shard_map(shards, mesh=mesh, in_specs=in_specs, out_specs=out_specs, check_vma=False)
```

profile of v0, /device:TPU:0, one launch (start us, length us, event | category | flops | bytes accessed | tf_op | source)
XLA Modules:
  0.0 578.0 jit_solution(5304392975098235761)
XLA Ops:
  15.1 6.7 %mul.394 = f32[384,2,2048]{2,1,0:T(2,128)} broadcast(bf16[384,2048]{1,0:T(8,128)(2,1)} %param.16), dimensions={0,2} | broadcast | bytes 7864320 | tf_op jit(solution)/shard_map/mul | solution.py:111
  21.8 8.5 %mul.395 = f32[768,2048]{1,0:T(8,128)} reshape(f32[384,2,2048]{2,1,0:T(2,128)} %mul.394) | data formatting | bytes 12582912 | tf_op jit(solution)/shard_map/mul | solution.py:111
  36.0 13.2 %gather_fusion = bf16[1280,2048]{1,0:T(8,128)(2,1)} fusion(bf16[769,2048]{1,0:T(8,128)(2,1)} %concatenate.63, s32[2048]{0:T(1024)S(1)} %pad_clamp_fusion), kind=kCustom, calls=%fused_computation | custom fusion | bytes 10490880 | tf_op jit(solution)/shard_map/jit(_take)/gather | solution.py:116
  49.2 5.4 broadcast_select_fusion
  54.6 8.6 %all-to-all-start = ((bf16[32,40,2048]{2,1,0:T(8,128)(2,1)}), bf16[32,40,2048]{2,1,0:T(8,128)(2,1)}, u32[]{:S(2)}, u32[]{:S(2)}) async-start(bf16[32,40,2048]{2,1,0:T(8,128)(2,1)} %broadcast_select_fusion), calls=%async_computation | async-start | bytes 10485760 | tf_op jit(solution)/shard_map/all_to_all | solution.py:156
  63.8 7.6 %fusion.5 = f32[1280,512]{1,0:T(8,128)} fusion(bf16[1,1280,2048]{2,1,0:T(8,128)(2,1)} %param.19, bf16[1,2048,512]{2,1,0:T(8,128)(2,1)} %param.21), kind=kOutput, calls=%fused_computation.10 | convolution fusion | flops 2684354560 | bytes 9961472 | tf_op jit(solution)/shard_map/erd,edf->erf/dot_general | solution.py:160
  71.4 6.8 %fusion.7 = f32[1280,512]{1,0:T(8,128)} fusion(bf16[1,1280,2048]{2,1,0:T(8,128)(2,1)} %param.19, bf16[1,2048,512]{2,1,0:T(8,128)(2,1)S(1)} %copy-done), kind=kOutput, calls=%fused_computation.12 | convolution fusion | flops 2684354560 | bytes 9961472 | tf_op jit(solution)/shard_map/erd,edf->erf/dot_general | solution.py:157
  78.2 50.8 %all-to-all-done = bf16[32,40,2048]{2,1,0:T(8,128)(2,1)} async-done(((bf16[32,40,2048]{2,1,0:T(8,128)(2,1)}), bf16[32,40,2048]{2,1,0:T(8,128)(2,1)}, u32[]{:S(2)}, u32[]{:S(2)}) %all-to-all-start) | async-done | bytes 5242912 | tf_op jit(solution)/shard_map/all_to_all | solution.py:156
  129.1 9.2 %select_convert_fusion = (bf16[1280,512]{1,0:T(8,128)(2,1)S(1)}, bf16[1280,512]{1,0:T(8,128)(2,1)S(1)}) fusion(f32[1280,512]{1,0:T(8,128)} %fusion.5, f32[1280,512]{1,0:T(8,128)} %fusion.7, bf16[1280,2048]{1,0:T(8,128)(2,1)} %bitcast.4, bf16[1,512,2048]{2,1,0:T(8,128)(2,1)} %param.22), kind=kOutput, calls=%fused_computation.23 | convolution fusion | flops 2698772480 | bytes 15204352 | tf_op jit(solution)/shard_map/erd,efd->erf/dot_general | solution.py:168
  141.2 4.9 fusion
  146.3 52.0 %reduce-scatter.3.cloned.1.call-done = bf16[1,1280,512]{2,1,0:T(8,128)(2,1)} async-done(((bf16[1,1280,2048]{2,1,0:T(8,128)(2,1)}), bf16[1,1280,512]{2,1,0:T(8,128)(2,1)}) %reduce-scatter.3.cloned.1.call-update) | async-done | bytes 1310736 | tf_op jit(solution)/shard_map/reduce_scatter | solution.py:183
  198.4 5.3 copy.206
  204.1 9.4 %reduce.4 = bf16[1280,512]{1,0:T(8,128)(2,1)S(1)} reduce(bf16[1280,1,512]{2,1,0:T(2,128)(2,1)} %bitcast.148, bf16[]{:T(256)} %broadcast.259), dimensions={1}, to_apply=%bitcast.141.reduce_sub_computation | reduce | bytes 2621442
  215.0 7.4 %all-to-all-start.1 = ((bf16[32,2,10240]{2,1,0:T(2,128)(2,1)}), bf16[32,2,10240]{2,1,0:T(2,128)(2,1)}, u32[]{:S(2)}, u32[]{:S(2)}) async-start(bf16[32,2,10240]{2,1,0:T(2,128)(2,1)} %reshape.294), calls=%async_computation.2 | async-start | bytes 2621440 | tf_op jit(solution)/shard_map/all_to_all | solution.py:187
  232.1 10.8 %all-to-all-done.1 = bf16[32,2,10240]{2,1,0:T(2,128)(2,1)} async-done(((bf16[32,2,10240]{2,1,0:T(2,128)(2,1)}), bf16[32,2,10240]{2,1,0:T(2,128)(2,1)}, u32[]{:S(2)}, u32[]{:S(2)}) %all-to-all-start.1) | async-done | bytes 1310752 | tf_op jit(solution)/shard_map/all_to_all | solution.py:187
  242.9 8.9 %reshape.295 = bf16[1280,1,512]{2,1,0:T(2,128)(2,1)} reshape(bf16[32,2,10240]{2,1,0:T(2,128)(2,1)} %all-to-all-done.1) | data formatting | bytes 2621440
  459.5 6.8 %rev.8 = f32[384,512]{1,0:T(8,128)} reverse(f32[384,512]{1,0:T(8,128)} %add.413), dimensions={0} | reverse | bytes 1572864 | tf_op jit(solution)/shard_map/jit(_flip)/rev | solution.py:229
  467.0 7.4 %all-to-all-start.3 = ((f32[32,2,512]{2,1,0:T(2,128)}), f32[32,2,512]{2,1,0:T(2,128)S(1)}, u32[]{:S(2)}, u32[]{:S(2)}) async-start(f32[32,2,512]{2,1,0:T(2,128)} %broadcast_in_dim.89), calls=%async_computation.5 | async-start | bytes 262144 | tf_op jit(solution)/shard_map/all_to_all | solution.py:13
  475.0 7.1 %all-to-all-done.3 = f32[32,2,512]{2,1,0:T(2,128)S(1)} async-done(((f32[32,2,512]{2,1,0:T(2,128)}), f32[32,2,512]{2,1,0:T(2,128)S(1)}, u32[]{:S(2)}, u32[]{:S(2)}) %all-to-all-start.3) | async-done | bytes 131104 | tf_op jit(solution)/shard_map/all_to_all | solution.py:13
  483.5 5.5 fusion.44
  491.6 5.8 %fusion.19 = bf16[1,2048,512]{1,2,0:T(8,128)(2,1)S(1)} fusion(bf16[1280,512]{1,0:T(8,128)(2,1)} %copy-done.48, bf16[1,1280,2048]{2,1,0:T(8,128)(2,1)} %param.19), kind=kOutput, calls=%fused_computation.21 | convolution fusion | flops 2685403136 | bytes 8650752 | tf_op jit(solution)/shard_map/erd,erf->edf/dot_general | solution.py:98
  500.0 5.9 %fusion.16 = bf16[1,2048,512]{1,2,0:T(8,128)(2,1)S(1)} fusion(bf16[1280,512]{1,0:T(8,128)(2,1)} %copy-done.47, bf16[1,1280,2048]{2,1,0:T(8,128)(2,1)} %param.19), kind=kOutput, calls=%fused_computation.20 | convolution fusion | flops 2685403136 | bytes 8650752 | tf_op jit(solution)/shard_map/erd,erf->edf/dot_general | solution.py:101
  508.7 9.0 %fusion.15 = bf16[1,512,2048]{2,1,0:T(8,128)(2,1)} fusion(bf16[1280,2048]{1,0:T(8,128)(2,1)} %bitcast.4, f32[1280,512]{1,0:T(8,128)} %fusion.5, f32[1280,512]{1,0:T(8,128)} %fusion.7), kind=kOutput, calls=%fused_computation.19 | convolution fusion | flops 2691956736 | bytes 12582912 | tf_op jit(solution)/shard_map/erf,erd->efd/dot_general | solution.py:95
  525.5 43.7 %reduce-scatter.5.cloned.1.call-done = bf16[64,512]{1,0:T(8,128)(2,1)} async-done(((bf16[2048,512]{1,0:T(8,128)(2,1)}), bf16[64,512]{1,0:T(8,128)(2,1)}) %reduce-scatter.5.cloned.1.call-update) | async-done | bytes 65552 | tf_op jit(solution)/shard_map/reduce_scatter | solution.py:216
  (415 shorter events, 255.2 us)
Async XLA Ops:
  7.2 64.2 %copy-start = (bf16[1,2048,512]{2,1,0:T(8,128)(2,1)S(1)}, bf16[1,2048,512]{2,1,0:T(8,128)(2,1)}, u32[]{:S(2)}) copy-start(bf16[1,2048,512]{2,1,0:T(8,128)(2,1)} %param.20) | copy-start | bytes 6291460
  54.6 74.4 %all-to-all-start = ((bf16[32,40,2048]{2,1,0:T(8,128)(2,1)}), bf16[32,40,2048]{2,1,0:T(8,128)(2,1)}, u32[]{:S(2)}, u32[]{:S(2)}) async-start(bf16[32,40,2048]{2,1,0:T(8,128)(2,1)} %broadcast_select_fusion), calls=%async_computation | async-start | bytes 10485760 | tf_op jit(solution)/shard_map/all_to_all | solution.py:156
  63.2 135.2 %reduce-scatter.3.cloned.1.call-start = ((), (), s32[]{:S(2)}) async-start(), calls=%async_computation.7 | async-start | bytes 6553600 | tf_op jit(solution)/shard_map/reduce_scatter | solution.py:183
  215.0 27.9 %all-to-all-start.1 = ((bf16[32,2,10240]{2,1,0:T(2,128)(2,1)}), bf16[32,2,10240]{2,1,0:T(2,128)(2,1)}, u32[]{:S(2)}, u32[]{:S(2)}) async-start(bf16[32,2,10240]{2,1,0:T(2,128)(2,1)} %reshape.294), calls=%async_computation.2 | async-start | bytes 2621440 | tf_op jit(solution)/shard_map/all_to_all | solution.py:187
  263.8 25.8 %all-to-all-start.2 = ((bf16[4,384,512]{1,2,0:T(8,128)(2,1)}), bf16[4,384,512]{1,2,0:T(8,128)(2,1)S(1)}, u32[]{:S(2)}, u32[]{:S(2)}) async-start(bf16[4,384,512]{1,2,0:T(8,128)(2,1)} %broadcast_in_dim.87), calls=%async_computation.3 | async-start | bytes 3145728 | tf_op jit(solution)/shard_map/all_to_all | solution.py:13
  271.7 15.6 %copy-start.18 = (bf16[2,256,256]{2,1,0:T(8,128)(2,1)S(1)}, bf16[2,256,256]{2,1,0:T(8,128)(2,1)}, u32[]{:S(2)}) copy-start(bf16[2,256,256]{2,1,0:T(8,128)(2,1)} %param.31) | copy-start | bytes 786436
  280.1 9.5 %copy-start.12 = (bf16[384,512]{1,0:T(8,128)(2,1)S(1)}, bf16[384,512]{1,0:T(8,128)(2,1)}, u32[]{:S(2)}) copy-start(bf16[384,512]{1,0:T(8,128)(2,1)} %param.25) | copy-start | bytes 1179652
  367.8 41.3 %copy-start.6 = (f32[192,512]{1,0:T(8,128)S(1)}, f32[192,512]{1,0:T(8,128)}, u32[]{:S(2)}) copy-start(f32[192,512]{1,0:T(8,128)} %get-tuple-element.62) | copy-start | bytes 1179652
  369.5 40.4 %copy-start.7 = (f32[192,512]{1,0:T(8,128)S(1)}, f32[192,512]{1,0:T(8,128)}, u32[]{:S(2)}) copy-start(f32[192,512]{1,0:T(8,128)} %get-tuple-element.61) | copy-start | bytes 1179652
  406.9 10.8 %copy-start.39 = (f32[1,512]{1,0:T(1,128)S(1)}, f32[1,512]{1,0:T(1,128)}, u32[]{:S(2)}) copy-start(f32[1,512]{1,0:T(1,128)} %slice.762) | copy-start | bytes 6148
  417.7 9.7 %copy-start.26 = (f32[3,512]{1,0:T(4,128)S(1)}, f32[3,512]{1,0:T(4,128)}, u32[]{:S(2)}) copy-start(f32[3,512]{1,0:T(4,128)} %slice.712) | copy-start | bytes 18436
  417.7 9.7 %copy-start.27 = (f32[3,512]{1,0:T(4,128)S(1)}, f32[3,512]{1,0:T(4,128)}, u32[]{:S(2)}) copy-start(f32[3,512]{1,0:T(4,128)} %slice.708) | copy-start | bytes 18436
  417.8 9.7 %copy-start.28 = (f32[3,512]{1,0:T(4,128)S(1)}, f32[3,512]{1,0:T(4,128)}, u32[]{:S(2)}) copy-start(f32[3,512]{1,0:T(4,128)} %slice.710) | copy-start | bytes 18436
  417.8 9.7 %copy-start.29 = (f32[3,512]{1,0:T(4,128)S(1)}, f32[3,512]{1,0:T(4,128)}, u32[]{:S(2)}) copy-start(f32[3,512]{1,0:T(4,128)} %slice.709) | copy-start | bytes 18436
  419.1 10.3 %copy-start.15 = (f32[47,512]{1,0:T(8,128)S(1)}, f32[47,512]{1,0:T(8,128)}, u32[]{:S(2)}) copy-start(f32[47,512]{1,0:T(8,128)} %slice.683) | copy-start | bytes 288772
  451.8 14.5 %all-to-all-start.4 = ((f32[32,2,512]{2,1,0:T(2,128)}), f32[32,2,512]{2,1,0:T(2,128)S(1)}, u32[]{:S(2)}, u32[]{:S(2)}) async-start(f32[32,2,512]{2,1,0:T(2,128)} %broadcast_in_dim.93), calls=%async_computation.6 | async-start | bytes 262144 | tf_op jit(solution)/shard_map/all_to_all | solution.py:13
  459.4 24.0 %copy-start.32 = (f32[512]{0:T(512)S(1)}, f32[512]{0:T(512)}, u32[]{:S(2)}) copy-start(f32[512]{0:T(512)} %copy-done.31) | copy-start | bytes 6148
  459.5 24.0 %copy-start.36 = (f32[384]{0:T(512)S(1)}, f32[384]{0:T(512)}, u32[]{:S(2)}) copy-start(f32[384]{0:T(512)} %param.29) | copy-start | bytes 4612
  459.5 24.0 %copy-start.37 = (f32[1,512]{1,0:T(1,128)S(1)}, f32[1,512]{1,0:T(1,128)}, u32[]{:S(2)}) copy-start(f32[1,512]{1,0:T(1,128)} %get-tuple-element.51) | copy-start | bytes 6148
  467.0 15.2 %all-to-all-start.3 = ((f32[32,2,512]{2,1,0:T(2,128)}), f32[32,2,512]{2,1,0:T(2,128)S(1)}, u32[]{:S(2)}, u32[]{:S(2)}) async-start(f32[32,2,512]{2,1,0:T(2,128)} %broadcast_in_dim.89), calls=%async_computation.5 | async-start | bytes 262144 | tf_op jit(solution)/shard_map/all_to_all | solution.py:13
  474.4 94.8 %reduce-scatter.5.cloned.1.call-start = ((), (), s32[]{:S(2)}) async-start(), calls=%async_computation.8 | async-start | bytes 2162688 | tf_op jit(solution)/shard_map/reduce_scatter | solution.py:216
  508.7 9.0 %copy-start.8 = (bf16[384,512]{1,0:T(8,128)(2,1)S(1)}, bf16[384,512]{1,0:T(8,128)(2,1)}, u32[]{:S(2)}) copy-start(bf16[384,512]{1,0:T(8,128)(2,1)} %get-tuple-element.36) | copy-start | bytes 1179652
  508.7 9.0 %copy-start.19 = (bf16[2,256,256]{2,1,0:T(8,128)(2,1)S(1)}, bf16[2,256,256]{2,1,0:T(8,128)(2,1)}, u32[]{:S(2)}) copy-start(bf16[2,256,256]{2,1,0:T(8,128)(2,1)} %param.31) | copy-start | bytes 786436
  520.3 50.3 %copy-start.1 = (bf16[1,2048,512]{2,1,0:T(8,128)(2,1)S(1)}, bf16[1,2048,512]{2,1,0:T(8,128)(2,1)}, u32[]{:S(2)}) copy-start(bf16[1,2048,512]{2,1,0:T(8,128)(2,1)} %param.20) | copy-start | bytes 6291460
  (32 other events, 171.9 us)
Sparse Core Ops, SparseCore 0:
  146.3 52.0 reduce-scatter.2
  491.7 77.3 reduce-scatter.4
where the time goes:
time: 589 us; the launch traced here: 578 us
  local copies, waits for them, and re-layouts  224 us (38%)
  waiting for transfers between devices  164 us (28%)
  other arithmetic  79 us (13%)
  matrix products  62.7 us (11%)
  starting transfers between devices  31.6 us (5%)
  between operations  16 us (3%)
    slice x101, local copies, waits for them, and re-layouts, linear_prefix(): return lax.associative_scan(combine, (coef, value), axis=0)[1]  123 us
    reduce_scatter x1, waiting for transfers between devices, shards(): lax.psum_scatter(partial_value, 'tp', scatter_dimension=2, tiled=True)  52 us
    all_to_all x1, waiting for transfers between devices, shards(): lax.all_to_all(outgoing, 'sp', split_axis=0, concat_axis=1, tiled=True)  50.8 us
    reduce_scatter x1, waiting for transfers between devices, shards(): lax.psum_scatter(lax.dot_general(z_grad, gated, (((0,), (0,)), ((), ())),...  43.7 us
    unnamed x106, local copies, waits for them, and re-layouts  20.3 us
    mul x14, other arithmetic, combine(): return (first[0] * second[0], second[0] * first[1] + second[1])  19.4 us
    pad x30, local copies, waits for them, and re-layouts, linear_prefix(): return lax.associative_scan(combine, (coef, value), axis=0)[1]  16.6 us
    mul x3, local copies, waits for them, and re-layouts, slot_rows(): chosen_expert_weight[:, :, None] * cotangent.astype(jnp.float32)[:, None, :]  15.4 us
  transfers between devices with their start and end apart: 7, of which 5 were waited for; matrix products, arithmetic and copies ran while one was open for 16% of the time, Pallas kernels for 0%

commit v1 on v0

v1 whole, which is shorter than its diff:
```python
import functools

import jax
import jax.numpy as jnp
from jax import lax
from jax.experimental import pallas as pl
from jax.experimental.pallas import tpu as pltpu
from jax.sharding import PartitionSpec as P


gate_scale_factor = 8.0
clamp_limit = 7.0
glu_alpha = 1.702

BF = jnp.bfloat16
F32 = jnp.float32

SLOT_GROUPS = (24, 16)

ROWS_ROWS = (((1,), (1,)), ((), ()))
COLS_COLS = (((0,), (0,)), ((), ()))


def params(limit_mib=48):
    return pltpu.CompilerParams(vmem_limit_bytes=limit_mib * 1024 * 1024)


def iota(shape, dim):
    return lax.broadcasted_iota(jnp.int32, shape, dim)


def placed_row(expert, slot, experts):
    base, row = 0, None
    for size in SLOT_GROUPS:
        here = base * experts + expert * size + (slot - base)
        row = here if row is None else jnp.where(slot >= base, here, row)
        base += size
    return row


def slots_kernel(idx_ref, idx_t_ref, col_ref, row_ref, *, experts):
    tokens, top = idx_ref.shape
    a, b = iota((tokens, tokens), 0), iota((tokens, tokens), 1)
    hot = [idx_ref[:, k : k + 1] == iota((tokens, experts), 1) for k in range(top)]
    both = sum(h.astype(F32) for h in hot).astype(BF)
    before = jnp.dot((b < a).astype(F32).astype(BF), both, preferred_element_type=F32)
    for k in range(top):
        rank = jnp.sum(jnp.where(hot[k], before, 0.0), axis=1, keepdims=True).astype(jnp.int32)
        col_ref[:, k : k + 1] = placed_row(idx_ref[:, k : k + 1], rank, experts)
    hot = [idx_t_ref[k : k + 1, :] == iota((experts, tokens), 0) for k in range(top)]
    both = sum(h.astype(F32) for h in hot).astype(BF)
    before = jnp.dot(both, (a < b).astype(F32).astype(BF), preferred_element_type=F32)
    for k in range(top):
        rank = jnp.sum(jnp.where(hot[k], before, 0.0), axis=0, keepdims=True).astype(jnp.int32)
        row_ref[k : k + 1, :] = placed_row(idx_t_ref[k : k + 1, :], rank, experts)


def slot_rows(chosen, experts):
    tokens, top = chosen.shape
    return pl.pallas_call(
        functools.partial(slots_kernel, experts=experts),
        out_shape=(
            jax.ShapeDtypeStruct((tokens, top), jnp.int32),
            jax.ShapeDtypeStruct((top, tokens), jnp.int32),
        ),
        compiler_params=params(),
        name="slots",
    )(chosen, chosen.T)


def dispatch_kernel(row_ref, weight_ref, cot_ref, out_ref, *, first):
    rows, tokens = out_ref.shape[0], cot_ref.shape[0]
    at = first + pl.program_id(0) * rows + iota((rows, tokens), 0)
    weight = jnp.zeros((rows, tokens), F32)
    for k in range(row_ref.shape[0]):
        weight = jnp.where(row_ref[k : k + 1, :] == at, weight_ref[k : k + 1, :], weight)
    picked = jnp.dot((weight > 0.0).astype(F32).astype(BF), cot_ref[...], preferred_element_type=F32)
    out_ref[...] = (picked * jnp.sum(weight, axis=1, keepdims=True)).astype(BF)


def dispatch(row, weight_t, cot, first, count):
    _, width = cot.shape
    block = 128
    return pl.pallas_call(
        functools.partial(dispatch_kernel, first=first),
        grid=(count // block,),
        in_specs=[
            pl.BlockSpec(row.shape, lambda i: (0, 0)),
            pl.BlockSpec(weight_t.shape, lambda i: (0, 0)),
            pl.BlockSpec(cot.shape, lambda i: (0, 0)),
        ],
        out_specs=pl.BlockSpec((block, width), lambda i: (i, 0)),
        out_shape=jax.ShapeDtypeStruct((count, width), BF),
        compiler_params=params(),
        name="dispatch",
    )(row, weight_t, cot)


def forward_kernel(x_ref, gate_ref, up_ref, act_ref, slope_ref):
    x = x_ref[...]
    hidden = gate_ref.shape[1]
    gate_pre = jnp.dot(x, gate_ref[...], preferred_element_type=F32)
    up_pre = jnp.dot(x, up_ref[...], preferred_element_type=F32)
    glu = jnp.minimum(gate_pre, clamp_limit)
    lin = jnp.clip(up_pre, -clamp_limit, clamp_limit) + 1.0
    sig = 1.0 / (1.0 + jnp.exp(-glu_alpha * glu))
    silu = glu * sig
    act_ref[...] = (silu * lin).astype(BF)
    slope = lin * (sig + glu_alpha * silu * (1.0 - sig))
    slope_ref[:, :hidden] = jnp.where(gate_pre < clamp_limit, slope, 0.0)
    slope_ref[:, hidden:] = jnp.where(jnp.abs(up_pre) < clamp_limit, silu, 0.0)


def expert_forward(x, w_gate, w_up):
    rows, width = x.shape
    hidden = w_gate.shape[1]
    block = 256
    whole = pl.BlockSpec((width, hidden), lambda i: (0, 0))
    return pl.pallas_call(
        forward_kernel,
        grid=(rows // block,),
        in_specs=[pl.BlockSpec((block, width), lambda i: (i, 0)), whole, whole],
        out_specs=(
            pl.BlockSpec((block, hidden), lambda i: (i, 0)),
            pl.BlockSpec((block, 2 * hidden), lambda i: (i, 0)),
        ),
        out_shape=(
            jax.ShapeDtypeStruct((rows, hidden), BF),
            jax.ShapeDtypeStruct((rows, 2 * hidden), F32),
        ),
        compiler_params=params(),
        name="expert_forward",
    )(x, w_gate, w_up)


def backward_kernel(
    rank_ref,
    got_ref,
    slope_ref,
    down_ref,
    gate_hbm,
    up_hbm,
    both_ref,
    up1_ref,
    dn1_ref,
    up2_ref,
    dn2_ref,
    mine_ref,
    gate_ref,
    up_ref,
    sems,
    *,
    n_tp,
):
    half = got_ref.shape[0] // 2
    hidden = down_ref.shape[0]
    width = mine_ref.shape[1]
    copies = [
        pltpu.make_async_copy(gate_hbm, gate_ref, sems.at[0]),
        pltpu.make_async_copy(up_hbm, up_ref, sems.at[1]),
    ]
    for copy in copies:
        copy.start()
    d_act = lax.dot_general(got_ref[...], down_ref[...], ROWS_ROWS, preferred_element_type=F32)
    d_gate = (d_act * slope_ref[:, :hidden]).astype(BF)
    d_up = (d_act * slope_ref[:, hidden:]).astype(BF)
    both_ref[:, :hidden] = d_gate
    both_ref[:, hidden:] = d_up
    for copy in copies:
        copy.wait()

    def term(ahead):
        at = pl.multiple_of(lax.rem(rank_ref[0] + ahead, n_tp) * width, width)
        both = lax.dot_general(
            d_gate, gate_ref[pl.ds(at, width), :], ROWS_ROWS, preferred_element_type=F32
        )
        both = both + lax.dot_general(
            d_up, up_ref[pl.ds(at, width), :], ROWS_ROWS, preferred_element_type=F32
        )
        return both.astype(BF)

    away = term(2)
    up1_ref[:half, :] = away[:half]
    dn1_ref[:half, :] = away[half:]
    above = term(1)
    up1_ref[half:, :] = above[half:]
    up2_ref[...] = above[:half]
    below = term(3)
    dn1_ref[half:, :] = below[:half]
    dn2_ref[...] = below[half:]
    mine_ref[...] = term(0)


def expert_backward(rank, got, slope, w_down, w_gate, w_up, n_tp):
    rows, width = got.shape
    hidden = w_down.shape[0]
    part = width // n_tp
    full = lambda a, b: pl.BlockSpec((a, b), lambda i: (0, 0))
    outs = [
        (rows, 2 * hidden),
        (rows, part),
        (rows, part),
        (rows // 2, part),
        (rows // 2, part),
        (rows, part),
    ]
    return pl.pallas_call(
        functools.partial(backward_kernel, n_tp=n_tp),
        grid=(1,),
        in_specs=[
            pl.BlockSpec(memory_space=pltpu.SMEM),
            full(rows, width),
            full(rows, 2 * hidden),
            full(hidden, width),
            pl.BlockSpec(memory_space=pl.ANY),
            pl.BlockSpec(memory_space=pl.ANY),
        ],
        out_specs=tuple(full(*s) for s in outs),
        out_shape=tuple(jax.ShapeDtypeStruct(s, BF) for s in outs),
        scratch_shapes=[
            pltpu.VMEM(w_gate.shape, BF),
            pltpu.VMEM(w_up.shape, BF),
            pltpu.SemaphoreType.DMA((2,)),
        ],
        compiler_params=params(),
        name="expert_backward",
    )(rank, got, slope, w_down, w_gate, w_up)


def summed_products(lefts, rights):
    total = None
    for left, right in zip(lefts, rights):
        term = lax.dot_general(left[...], right[...], COLS_COLS, preferred_element_type=F32)
        total = term if total is None else total + term
    return total


def gate_up_kernel(*refs, groups):
    gate_ref, up_ref = refs[2 * groups :]
    total = summed_products(refs[:groups], refs[groups : 2 * groups])
    hidden = gate_ref.shape[1]
    gate_ref[...] = total[:, :hidden].astype(BF)
    up_ref[...] = total[:, hidden:].astype(BF)


def gate_up_grads(saved, both):
    width, hidden = saved[0].shape[1], both[0].shape[1] // 2
    block = 256
    out = pl.BlockSpec((block, hidden), lambda i: (i, 0))
    return pl.pallas_call(
        functools.partial(gate_up_kernel, groups=len(saved)),
        grid=(width // block,),
        in_specs=[pl.BlockSpec((x.shape[0], block), lambda i: (0, i)) for x in saved]
        + [pl.BlockSpec(g.shape, lambda i: (0, 0)) for g in both],
        out_specs=(out, out),
        out_shape=(jax.ShapeDtypeStruct((width, hidden), BF),) * 2,
        compiler_params=params(),
        name="gate_up_grads",
    )(*saved, *both)


def down_kernel(*refs, groups):
    refs[-1][...] = summed_products(refs[:groups], refs[groups : 2 * groups]).astype(BF)


def down_grads(acts, gots):
    width, hidden = gots[0].shape[1], acts[0].shape[1]
    block = 512
    return pl.pallas_call(
        functools.partial(down_kernel, groups=len(acts)),
        grid=(width // block,),
        in_specs=[pl.BlockSpec(a.shape, lambda i: (0, 0)) for a in acts]
        + [pl.BlockSpec((g.shape[0], block), lambda i: (0, i)) for g in gots],
        out_specs=pl.BlockSpec((hidden, block), lambda i: (0, i)),
        out_shape=jax.ShapeDtypeStruct((hidden, width), BF),
        compiler_params=params(),
        name="down_grads",
    )(*acts, *gots)


def ring(n, step):
    return [(i, (i + step) % n) for i in range(n)]


def summed_over_tp(up1, dn1, up2, dn2, mine, n_tp):
    half = up2.shape[0]
    from_below = lax.ppermute(up1, "tp", ring(n_tp, 1))
    from_above = lax.ppermute(dn1, "tp", ring(n_tp, -1))
    add = lambda a, b: (a.astype(F32) + b.astype(F32)).astype(BF)
    up2 = add(up2, from_below[:half])
    dn2 = add(dn2, from_above[:half])
    top = lax.ppermute(up2, "tp", ring(n_tp, 1))
    bottom = lax.ppermute(dn2, "tp", ring(n_tp, -1))
    upper = (
        mine[:half].astype(F32) + top.astype(F32) + from_above[half:].astype(F32)
    ).astype(BF)
    lower = (
        mine[half:].astype(F32) + bottom.astype(F32) + from_below[half:].astype(F32)
    ).astype(BF)
    return jnp.concatenate([upper, lower], axis=0)


def combine_kernel(col_ref, cot_ref, *refs):
    back_refs, out_ref = refs[:-1], refs[-1]
    tokens, top = col_ref.shape
    total, first = None, 0
    for back_ref in back_refs:
        rows = back_ref.shape[0]
        at = first + iota((tokens, rows), 1)
        hit = col_ref[:, 0:1] == at
        for k in range(1, top):
            hit = hit | (col_ref[:, k : k + 1] == at)
        term = jnp.dot(hit.astype(F32).astype(BF), back_ref[...], preferred_element_type=F32)
        total = term if total is None else total + term
        first += rows
    out_ref[...] = (cot_ref[...].astype(F32) + total).astype(BF)


def combine(col, cot_part, backs):
    return pl.pallas_call(
        combine_kernel,
        out_shape=jax.ShapeDtypeStruct(cot_part.shape, BF),
        compiler_params=params(),
        name="combine",
    )(col, cot_part, *backs)


def pieces_of(rank_ref, z_refs, n_tp):
    z0, z_below, z_above, z_top, z_bottom = z_refs
    me = rank_ref[0]
    away = jnp.concatenate([z_top[...], z_bottom[...]], axis=0)
    order = ((0, z0[...]), (n_tp - 1, z_below[...]), (1, z_above[...]), (2, away))
    width = z0.shape[1]
    return [(pl.multiple_of(lax.rem(me + a, n_tp) * width, width), z) for a, z in order]


def state_kernel(
    rank_ref,
    z0,
    z1,
    z2,
    z3,
    z4,
    w_hbm,
    mixed_ref,
    branch_ref,
    decay_ref,
    later_ref,
    earlier_ref,
    branch_grad_ref,
    state_ref,
    carry_ref,
    w_ref,
    sem,
    *,
    n_tp,
):
    copy = pltpu.make_async_copy(w_hbm, w_ref, sem)
    copy.start()
    copy.wait()
    total = None
    for at, z in pieces_of(rank_ref, (z0, z1, z2, z3, z4), n_tp):
        term = jnp.dot(z, w_ref[pl.ds(at, z.shape[1]), :], preferred_element_type=F32)
        total = term if total is None else total + term
    branch_grad_ref[...] = (total * mixed_ref[...].astype(F32)).astype(BF)
    state = total * branch_ref[...].astype(F32)
    state_ref[...] = state
    scaled = state * decay_ref[...]
    ahead = jnp.sum(scaled * earlier_ref[...], axis=0, keepdims=True)
    behind = jnp.sum(scaled * later_ref[...], axis=0, keepdims=True)
    last = slice(state.shape[0] - 1, state.shape[0])
    through = decay_ref[last, :] * earlier_ref[last, :]
    lanes = carry_ref.shape[2]
    count = ahead.shape[1] // lanes
    tile = jnp.concatenate(
        [
            v[:, b * lanes : (b + 1) * lanes]
            for v in (ahead, behind, through, through)
            for b in range(count)
        ],
        axis=0,
    )
    carry_ref[...] = jnp.broadcast_to(tile[None], carry_ref.shape)


def state_grads(rank, zs, w_out, mixed, branch, decay, later_prod, earlier_prod, n_sp, n_tp):
    tokens, channels = mixed.shape
    return pl.pallas_call(
        functools.partial(state_kernel, n_tp=n_tp),
        in_specs=[pl.BlockSpec(memory_space=pltpu.SMEM)]
        + [pl.BlockSpec(memory_space=pltpu.VMEM)] * 5
        + [pl.BlockSpec(memory_space=pl.ANY)]
        + [pl.BlockSpec(memory_space=pltpu.VMEM)] * 5,
        out_shape=(
            jax.ShapeDtypeStruct((tokens, channels), BF),
            jax.ShapeDtypeStruct((tokens, channels), F32),
            jax.ShapeDtypeStruct((n_sp, 16, channels // 4), F32),
        ),
        scratch_shapes=[pltpu.VMEM(w_out.shape, BF), pltpu.SemaphoreType.DMA(())],
        compiler_params=params(),
        name="state_grads",
    )(rank, *zs, w_out, mixed, branch, decay, later_prod, earlier_prod)


def proj_kernel(rank_ref, core_ref, z0, z1, z2, z3, z4, gated_ref, keep_ref, send_ref, *, n_tp, size):
    gated = gated_ref[...]
    odd = core_ref[0] == 1
    for at, z in pieces_of(rank_ref, (z0, z1, z2, z3, z4), n_tp):
        term = lax.dot_general(z, gated, COLS_COLS, preferred_element_type=F32).astype(BF)
        for i in range(term.shape[0] // (2 * size)):
            first = term[2 * i * size : (2 * i + 1) * size]
            second = term[(2 * i + 1) * size : (2 * i + 2) * size]
            rows = pl.ds(pl.multiple_of(at // 2, size) + i * size, size)
            keep_ref[rows, :] = jnp.where(odd, second, first)
            send_ref[rows, :] = jnp.where(odd, first, second)


def proj_terms(rank, core, zs, gated, n_tp, n_sp):
    width = zs[0].shape[1] * n_tp
    half = jax.ShapeDtypeStruct((width // 2, gated.shape[1]), BF)
    return pl.pallas_call(
        functools.partial(proj_kernel, n_tp=n_tp, size=width // n_sp),
        in_specs=[pl.BlockSpec(memory_space=pltpu.SMEM)] * 2
        + [pl.BlockSpec(memory_space=pltpu.VMEM)] * 6,
        out_shape=(half, half),
        compiler_params=params(),
        name="proj_terms",
    )(rank, core, *zs, gated)


def scan_kernel(state_ref, decay_ref, later_ref, earlier_ref):
    rows, channels = state_ref.shape
    zero = jnp.zeros((1, channels), F32)

    def step(i, carry):
        ahead, behind = carry
        t = rows - 1 - i
        later = state_ref[pl.ds(t, 1), :] + ahead
        later_ref[pl.ds(t, 1), :] = later
        earlier = state_ref[pl.ds(i, 1), :] + behind
        earlier_ref[pl.ds(i, 1), :] = earlier
        return (later * decay_ref[pl.ds(t, 1), :], earlier * decay_ref[pl.ds(i, 1), :])

    lax.fori_loop(0, rows, step, (zero, zero), unroll=8)


def local_scans(state, decay):
    return pl.pallas_call(
        scan_kernel,
        out_shape=(
            jax.ShapeDtypeStruct(state.shape, F32),
            jax.ShapeDtypeStruct(state.shape, F32),
        ),
        compiler_params=params(),
        name="local_scans",
    )(state, decay)


def carried_in(me, got_ref):
    count, half = got_ref.shape[0], got_ref.shape[1] // 2
    carry = lambda q: got_ref[q, :half, :]
    through = lambda q: got_ref[q, half:, :]
    zero = jnp.zeros((half, got_ref.shape[2]), F32)
    ahead, behind = zero, zero
    for q in range(count):
        p = count - 1 - q
        ahead = jnp.where(p > me, carry(p) + through(p) * ahead, ahead)
        behind = jnp.where(q < me, carry(q) + through(q) * behind, behind)
    return ahead[: half // 2], behind[half // 2 :]


def final_kernel(
    me_ref,
    got_ref,
    later_ref,
    earlier_ref,
    later_prod,
    earlier_prod,
    h_later,
    h_earlier,
    q_ref,
    r_ref,
    rec_w,
    inp_w,
    out_ref,
):
    ahead, behind = carried_in(me_ref[0], got_ref)
    spread = lambda v: jnp.concatenate([v[b : b + 1] for b in range(v.shape[0])], axis=1)
    later = later_ref[...] + later_prod[...] * spread(ahead)
    earlier = earlier_ref[...] + earlier_prod[...] * spread(behind)
    total = later + earlier
    rec_pre = (later * h_later[...] + earlier * h_earlier[...]).astype(BF)
    inp_pre = (total * q_ref[...]).astype(BF)
    direct = total * r_ref[...]
    size = rec_w.shape[1]
    for b in range(rec_w.shape[0]):
        cols = slice(b * size, (b + 1) * size)
        term = lax.dot_general(rec_pre[:, cols], rec_w[b], ROWS_ROWS, preferred_element_type=F32)
        term = term + lax.dot_general(
            inp_pre[:, cols], inp_w[b], ROWS_ROWS, preferred_element_type=F32
        )
        out_ref[:, cols] = (direct[:, cols] + term).astype(BF)


def final_grads(me, got, arrays, rec_w, inp_w):
    tokens, channels = arrays[0].shape
    return pl.pallas_call(
        final_kernel,
        in_specs=[pl.BlockSpec(memory_space=pltpu.SMEM)]
        + [pl.BlockSpec(memory_space=pltpu.VMEM)] * 11,
        out_shape=jax.ShapeDtypeStruct((tokens, channels), BF),
        compiler_params=params(),
        name="final_grads",
    )(me, got, *arrays, rec_w, inp_w)


def blockwise(rows, weights):
    size = weights.shape[1]
    return jnp.concatenate(
        [
            jnp.dot(rows[:, b * size : (b + 1) * size], weights[b], preferred_element_type=F32)
            for b in range(weights.shape[0])
        ],
        axis=1,
    )


def shards(
    output_cotangent,
    chosen_expert_index,
    chosen_expert_weight,
    expert_slot_tokens,
    expert_gate_matrix,
    expert_up_matrix,
    expert_down_matrix,
    output_projection_matrix,
    recurrence_input,
    branch_activation_values,
    forward_scan_state,
    reverse_scan_state,
    channel_decay_rate,
    position_extra_log_decay,
    recurrence_gate_weights,
    input_gate_weights,
):
    n_sp = lax.axis_size("sp")
    n_tp = lax.axis_size("tp")
    tokens, model_width = output_cotangent.shape
    experts = n_sp * expert_gate_matrix.shape[0]
    capacity = expert_slot_tokens.shape[1] // n_sp
    part = model_width // n_tp
    rank = lax.axis_index("tp").astype(jnp.int32).reshape(1)
    place = lax.axis_index("sp").astype(jnp.int32).reshape(1)
    bounds, at = [], 0
    for size in SLOT_GROUPS:
        bounds.append((at, size))
        at += size

    col, row = slot_rows(chosen_expert_index, experts)
    weight_t = chosen_expert_weight.T
    received = []
    for base, size in bounds:
        out = dispatch(row, weight_t, output_cotangent, base * experts, size * experts)
        out = out.reshape(experts, size, model_width)
        got = lax.all_to_all(out, "sp", 0, 0, tiled=True)
        received.append(got.reshape(n_sp * size, model_width))

    w_gate, w_up, w_down = expert_gate_matrix[0], expert_up_matrix[0], expert_down_matrix[0]
    by_source = expert_slot_tokens.reshape(n_sp, capacity, model_width)
    saved, acts, slopes = [], [], []
    for base, size in bounds:
        x = by_source[:, base : base + size].reshape(n_sp * size, model_width)
        act, slope = expert_forward(x, w_gate, w_up)
        saved.append(x)
        acts.append(act)
        slopes.append(slope)

    rec = jax.nn.sigmoid(blockwise(recurrence_input, recurrence_gate_weights))
    inp = jax.nn.sigmoid(blockwise(recurrence_input, input_gate_weights))
    rate = -gate_scale_factor * channel_decay_rate[None, :]
    log_decay = rec * rate + position_extra_log_decay[:, None]
    decay = jnp.exp(log_decay)
    scale_in = jnp.sqrt(-jnp.expm1(2.0 * log_decay))
    inputs = recurrence_input.astype(F32)
    xin = scale_in * inp * inputs
    mixed = (
        (decay * forward_scan_state + xin) + (decay * reverse_scan_state + xin)
    ).astype(BF)
    gated = (mixed.astype(F32) * branch_activation_values.astype(F32)).astype(BF)
    lower = (iota((tokens, tokens), 1) <= iota((tokens, tokens), 0)).astype(F32)
    running = jnp.dot(lower, log_decay, precision=lax.Precision.HIGHEST)
    later_prod = jnp.exp(running[-1:] - running)
    earlier_prod = jnp.exp(running - log_decay)
    rec_slope = rate * rec * (1.0 - rec)
    shared = inp * inputs * decay * decay / scale_in
    h_later = (forward_scan_state * decay - shared) * rec_slope
    h_earlier = (reverse_scan_state * decay - shared) * rec_slope
    q = scale_in * inputs * inp * (1.0 - inp)
    r = scale_in * inp
    cot_part = lax.dynamic_slice_in_dim(output_cotangent, rank[0] * part, part, 1)

    boths, backs = [], []
    for g, ((base, size), got) in enumerate(zip(bounds, received)):
        both, *terms = expert_backward(rank, got, slopes[g], w_down, w_gate, w_up, n_tp)
        summed = summed_over_tp(*terms, n_tp)
        back = lax.all_to_all(summed.reshape(n_sp, size, part), "sp", 0, 0, tiled=True)
        backs.append(back.reshape(experts * size, part))
        boths.append(both)
    gate_grad, up_grad = gate_up_grads(saved, boths)
    down_grad = down_grads(acts, received)

    z0 = combine(col, cot_part, backs)
    z_below = lax.ppermute(z0, "tp", ring(n_tp, 1))
    z_above = lax.ppermute(z0, "tp", ring(n_tp, -1))
    z_top = lax.ppermute(z_below[: tokens // 2], "tp", ring(n_tp, 1))
    z_bottom = lax.ppermute(z_above[tokens // 2 :], "tp", ring(n_tp, -1))
    zs = (z0, z_below, z_above, z_top, z_bottom)

    branch_grad, state, carry = state_grads(
        rank,
        zs,
        output_projection_matrix,
        mixed,
        branch_activation_values,
        decay,
        later_prod,
        earlier_prod,
        n_sp,
        n_tp,
    )
    carried = lax.all_to_all(carry, "sp", 0, 0, tiled=True)
    keep, send = proj_terms(rank, place % 2, zs, gated, n_tp, n_sp)
    other = lax.ppermute(send, "sp", [(i, i ^ 1) for i in range(n_sp)])
    terms = (keep.astype(F32) + other.astype(F32)).astype(BF)
    terms = terms.reshape(n_sp // 2, model_width // n_sp, -1)
    groups = [list(range(c, n_sp, 2)) for c in range(2)]
    terms = lax.all_to_all(terms, "sp", 0, 0, axis_index_groups=groups, tiled=True)
    later, earlier = local_scans(state, decay)
    input_grad = final_grads(
        place,
        carried,
        (later, earlier, later_prod, earlier_prod, h_later, h_earlier, q, r),
        recurrence_gate_weights,
        input_gate_weights,
    )
    proj_grad = jnp.sum(terms.astype(F32), axis=0)
    return (gate_grad[None], up_grad[None], down_grad[None], proj_grad, branch_grad, input_grad)


def solution(mesh):
    in_specs = (
        P("sp", None),
        P("sp", None),
        P("sp", None),
        P("sp", None, None),
        P("sp", None, "tp"),
        P("sp", None, "tp"),
        P("sp", "tp", None),
        P(None, "tp"),
        P("sp", "tp"),
        P("sp", "tp"),
        P("sp", "tp"),
        P("sp", "tp"),
        P("tp"),
        P("sp"),
        P("tp", None, None),
        P("tp", None, None),
    )
    out_specs = (
        P("sp", None, "tp"),
        P("sp", None, "tp"),
        P("sp", "tp", None),
        P("sp", "tp"),
        P("sp", "tp"),
        P("sp", "tp"),
    )
    return jax.shard_map(shards, mesh=mesh, in_specs=in_specs, out_specs=out_specs, check_vma=False)
```

time: 589 us -> 259 us (0.44); the launches traced: 578 us -> 256 us
  local copies, waits for them, and re-layouts: 224 us -> 24 us
  waiting for transfers between devices: 164 us -> 93.5 us
  Pallas kernels: 0 us -> 61.7 us
  other arithmetic: 79 us -> 18.7 us
  matrix products: 62.7 us -> 6.63 us
  starting transfers between devices: 31.6 us -> 50.3 us
  between operations: 16 us -> 1.34 us
    slice x142 -> x5, local copies, waits for them, and re-layouts: 126 us -> 5.16 us  [the longest x2 3.79 us: shards(): x = by_source[:, base:base + size].reshape(n_sp * size, model_width)]
    reduce_scatter x2 -> x0, waiting for transfers between devices: 95.7 us -> none  [the longest x1 52 us: shards(): lax.psum_scatter(partial_value, 'tp', scatter_dimension=2, tiled=True)]
    pallas_call x0 -> x14, Pallas kernels: none -> 61.7 us  [the longest x2 16.6 us: expert_backward(): pl.pallas_call(functools.partial(backward_kernel, n_tp=n_tp), grid=(1,),...]
    dot_general x14 -> x5, matrix products: 62.7 us -> 6.63 us  [the longest x4 4.02 us: blockwise(): jnp.dot(rows[:, b * size:(b + 1) * size], weights[b], preferred_element_t...]
    ppermute x0 -> x13, waiting for transfers between devices: none -> 32 us  [the longest x2 20.2 us: summed_over_tp(): from_above = lax.ppermute(dn1, 'tp', ring(n_tp, -1))]
    ppermute x0 -> x13, starting transfers between devices: none -> 20.2 us  [the longest x2 5.98 us: summed_over_tp(): bottom = lax.ppermute(dn2, 'tp', ring(n_tp, -1))]
    mul x23 -> x2, other arithmetic: 21.1 us -> 2.4 us  [the longest x1 2.4 us: shards(): xin = scale_in * inp * inputs]
    gather x3 -> x0, local copies, waits for them, and re-layouts: 17 us -> none  [the longest x1 13.2 us: slot_rows(): return jnp.take(padded, owner, axis=0).reshape(experts, capacity, width)]
  transfers between devices with their start and end apart: 7 -> 19, of which waited for: 5 -> 10; matrix products, arithmetic and copies ran while one was open for 16% -> 12% of each run, Pallas kernels for 0% -> 22%
where the time goes in v1:
time: 259 us; the launch traced here: 256 us
  waiting for transfers between devices  93.5 us (36%)
  Pallas kernels  61.7 us (24%)
  starting transfers between devices  50.3 us (19%)
  local copies, waits for them, and re-layouts  24 us (9%)
  other arithmetic  18.7 us (7%)
  matrix products  6.63 us (3%)
    all_to_all x2, waiting for transfers between devices, shards(): got = lax.all_to_all(out, 'sp', 0, 0, tiled=True)  36.9 us
    ppermute x2, waiting for transfers between devices, summed_over_tp(): from_above = lax.ppermute(dn1, 'tp', ring(n_tp, -1))  20.2 us
    all_to_all x2, waiting for transfers between devices, shards(): lax.all_to_all(summed.reshape(n_sp, size, part), 'sp', 0, 0, tiled=True)  18.8 us
    unnamed x121, local copies, waits for them, and re-layouts  17.8 us
    pallas_call x2, Pallas kernels, expert_backward(): pl.pallas_call(functools.partial(backward_kernel, n_tp=n_tp), grid=(1,),...  16.6 us
    all_to_all x2, starting transfers between devices, shards(): got = lax.all_to_all(out, 'sp', 0, 0, tiled=True)  13.4 us
    pallas_call x2, Pallas kernels, expert_forward(): pl.pallas_call(forward_kernel, grid=(rows // block,), in_specs=[pl.BlockS...  12.4 us
    pallas_call x1, Pallas kernels, gate_up_grads(): pl.pallas_call(functools.partial(gate_up_kernel, groups=len(saved)), grid...  9.62 us
  transfers between devices with their start and end apart: 19, of which 10 were waited for; matrix products, arithmetic and copies ran while one was open for 12% of the time, Pallas kernels for 22%

profile of v1, /device:TPU:0, one launch (start us, length us, event | category | flops | bytes accessed | tf_op | source)
XLA Modules:
  0.0 256.1 jit_solution(5810255840296468712)
XLA Ops:
  7.9 8.6 %all-to-all-start.1 = ((bf16[32,16,2048]{2,1,0:T(8,128)(2,1)}), bf16[32,16,2048]{2,1,0:T(8,128)(2,1)S(1)}, u32[]{:S(2)}, u32[]{:S(2)}) async-start(bf16[32,16,2048]{2,1,0:T(8,128)(2,1)} %bitcast.48), calls=%async_computation.1 | async-start | bytes 4194304 | tf_op jit(solution)/shard_map/all_to_all | solution.py:565
  22.4 24.2 %all-to-all-done.1 = bf16[32,16,2048]{2,1,0:T(8,128)(2,1)S(1)} async-done(((bf16[32,16,2048]{2,1,0:T(8,128)(2,1)}), bf16[32,16,2048]{2,1,0:T(8,128)(2,1)S(1)}, u32[]{:S(2)}, u32[]{:S(2)}) %all-to-all-start.1) | async-done | bytes 2097184 | tf_op jit(solution)/shard_map/all_to_all | solution.py:565
  47.9 4.8 %all-to-all-start = ((bf16[32,24,2048]{2,1,0:T(8,128)(2,1)}), bf16[32,24,2048]{2,1,0:T(8,128)(2,1)}, u32[]{:S(2)}, u32[]{:S(2)}) async-start(bf16[32,24,2048]{2,1,0:T(8,128)(2,1)} %bitcast.47), calls=%async_computation | async-start | bytes 6291456 | tf_op jit(solution)/shard_map/all_to_all | solution.py:565
  54.5 5.8 %expert_forward.3 = (bf16[512,512]{1,0:T(8,128)(2,1)S(1)}, f32[512,1024]{1,0:T(8,128)S(1)}) custom-call(bf16[512,2048]{1,0:T(8,128)(2,1)S(1)} %bitcast.43, bf16[2048,512]{1,0:T(8,128)(2,1)} %bitcast.35, bf16[2048,512]{1,0:T(8,128)(2,1)} %bitcast.39), custom_call_target="tpu_custom_call" | custom-call | tf_op jit(solution)/shard_map/expert_forward/pallas_call | solution.py:119
  62.5 7.4 %expert_backward.3 = (bf16[512,1024]{1,0:T(8,128)(2,1)S(1)}, bf16[512,512]{1,0:T(8,128)(2,1)S(1)}, bf16[512,512]{1,0:T(8,128)(2,1)S(1)}, bf16[256,512]{1,0:T(8,1...) custom-call(s32[1]{0:T(128)} %bitcast.3.rank_ref, bf16[512,2048]{1,0:T(8,128)(2,1)S(1)} %bitcast.45, ...), custom_call_target="tpu_custom_call" | custom-call | tf_op jit(solution)/shard_map/expert_backward/pallas_call | solution.py:207
  74.4 6.6 %expert_forward.2 = (bf16[768,512]{1,0:T(8,128)(2,1)S(1)}, f32[768,1024]{1,0:T(8,128)}) custom-call(bf16[768,2048]{1,0:T(8,128)(2,1)} %bitcast.54, bf16[2048,512]{1,0:T(8,128)(2,1)S(1)} %bitcast.38, bf16[2048,512]{1,0:T(8,128)(2,1)S(1)} %bitcast.42), custom_call_target="tpu_custom_call" | custom-call | tf_op jit(solution)/shard_map/expert_forward/pallas_call | solution.py:119
  82.0 12.8 %all-to-all-done = bf16[32,24,2048]{2,1,0:T(8,128)(2,1)} async-done(((bf16[32,24,2048]{2,1,0:T(8,128)(2,1)}), bf16[32,24,2048]{2,1,0:T(8,128)(2,1)}, u32[]{:S(2)}, u32[]{:S(2)}) %all-to-all-start) | async-done | bytes 3145760 | tf_op jit(solution)/shard_map/all_to_all | solution.py:565
  94.7 9.1 %expert_backward.2 = (bf16[768,1024]{1,0:T(8,128)(2,1)S(1)}, bf16[768,512]{1,0:T(8,128)(2,1)S(1)}, bf16[768,512]{1,0:T(8,128)(2,1)S(1)}, bf16[384,512]{1,0:T(8,1...) custom-call(s32[1]{0:T(128)} %bitcast.3.rank_ref, bf16[768,2048]{1,0:T(8,128)(2,1)} %bitcast.7.got_ref.refs_2_, ...), custom_call_target="tpu_custom_call" | custom-call | tf_op jit(solution)/shard_map/expert_backward/pallas_call | solution.py:207
  110.5 9.9 %collective-permute-done.6 = bf16[512,512]{1,0:T(8,128)(2,1)S(1)} collective-permute-done((bf16[512,512]{1,0:T(8,128)(2,1)S(1)}, bf16[512,512]{1,0:T(8,128)(2,1)S(1)}, u32[]{:S(2)}, u32[]{:S(2)}) %collective-permute-start.6) | collective-permute-done | bytes 524320 | tf_op jit(solution)/shard_map/ppermute | solution.py:288
  120.5 3.0 %collective-permute-start.7 = (bf16[256,512]{1,0:T(8,128)(2,1)S(1)}, bf16[256,512]{1,0:T(8,128)(2,1)S(1)}, u32[]{:S(2)}, u32[]{:S(2)}) collective-permute-start(bf16[256,512]{1,0:T(8,128)(2,1)S(1)} %add_convert_fusion.7), channel_id=1, source_target_pairs={{0,3},{1,0},{2,1},{3,2},{4,7},{5,4},{6,5},{7,6},{8,11},{9,8},{10,9... | collective-permute-start | bytes 786440 | tf_op jit(solution)/shard_map/ppermute | solution.py:293
  127.0 10.3 %collective-permute-done.2 = bf16[768,512]{1,0:T(8,128)(2,1)S(1)} collective-permute-done((bf16[768,512]{1,0:T(8,128)(2,1)S(1)}, bf16[768,512]{1,0:T(8,128)(2,1)S(1)}, u32[]{:S(2)}, u32[]{:S(2)}) %collective-permute-start.2) | collective-permute-done | bytes 786464 | tf_op jit(solution)/shard_map/ppermute | solution.py:288
  144.9 3.9 %all-to-all-start.3 = ((bf16[32,16,512]{2,1,0:T(8,128)(2,1)}), bf16[32,16,512]{2,1,0:T(8,128)(2,1)S(1)}, u32[]{:S(2)}, u32[]{:S(2)}) async-start(bf16[32,16,512]{2,1,0:T(8,128)(2,1)} %bitcast.19), calls=%async_computation.3 | async-start | bytes 1048576 | tf_op jit(solution)/shard_map/all_to_all | solution.py:606
  152.2 8.2 %all-to-all-done.3 = bf16[32,16,512]{2,1,0:T(8,128)(2,1)S(1)} async-done(((bf16[32,16,512]{2,1,0:T(8,128)(2,1)}), bf16[32,16,512]{2,1,0:T(8,128)(2,1)S(1)}, u32[]{:S(2)}, u32[]{:S(2)}) %all-to-all-start.3) | async-done | bytes 524320 | tf_op jit(solution)/shard_map/all_to_all | solution.py:606
  160.4 3.9 %all-to-all-start.2 = ((bf16[32,24,512]{2,1,0:T(8,128)(2,1)}), bf16[32,24,512]{2,1,0:T(8,128)(2,1)S(1)}, u32[]{:S(2)}, u32[]{:S(2)}) async-start(bf16[32,24,512]{2,1,0:T(8,128)(2,1)} %bitcast.63), calls=%async_computation.2 | async-start | bytes 1572864 | tf_op jit(solution)/shard_map/all_to_all | solution.py:606
  168.3 10.6 %all-to-all-done.2 = bf16[32,24,512]{2,1,0:T(8,128)(2,1)S(1)} async-done(((bf16[32,24,512]{2,1,0:T(8,128)(2,1)}), bf16[32,24,512]{2,1,0:T(8,128)(2,1)S(1)}, u32[]{:S(2)}, u32[]{:S(2)}) %all-to-all-start.2) | async-done | bytes 786464 | tf_op jit(solution)/shard_map/all_to_all | solution.py:606
  184.1 7.9 %collective-permute-done.8.z1 = bf16[384,512]{1,0:T(8,128)(2,1)S(1)} collective-permute-done((bf16[384,512]{1,0:T(8,128)(2,1)S(1)}, bf16[384,512]{1,0:T(8,128)(2,1)S(1)}, u32[]{:S(2)}, u32[]{:S(2)}) %collective-permute-start.8) | collective-permute-done | bytes 393248 | tf_op jit(solution)/shard_map/ppermute | solution.py:613
  196.6 3.7 %multiply_convert_fusion = (bf16[384,512]{1,0:T(8,128)(2,1)S(1)}, bf16[384,512]{1,0:T(8,128)(2,1)S(1)}, f32[384,512]{1,0:T(8,128)}, f32[384,512]{1,0:T(8,128)}) fusion(bf16[384,512]{1,0:T(8,128)(2,1)S(1)} %copy-done.20, f32[384,512]{1,0:T(8,128)S(1)} %copy-done.53, bf16[384,512]{1,0:T(8,128)(2,1)} %param.24, f32[384,256]{1,0:T(8,128)} %fusion.13, ...), kind=kLoop, calls=%fused_computation.23 | loop fusion | flops 6881280 | bytes 6295040 | tf_op jit(solution)/shard_map/convert_element_type | solution.py:589
  208.2 4.1 %state_grads.1 = (bf16[384,512]{1,0:T(8,128)(2,1)}, f32[384,512]{1,0:T(8,128)S(1)}, f32[32,16,128]{2,1,0:T(8,128)}) custom-call(s32[1]{0:T(128)} %bitcast.3.rank_ref, bf16[384,512]{1,0:T(8,128)(2,1)S(1)} %combine.1.z0, bf16[384,512]{1,0:T(8,128)(2,1)S(1)} %collective-permute-done.8.z1, bf16[384,512]{1,0:T(8,128)(2,1)S(1)} %collective-permute-done.9.z2, ...), custom_call_target="tpu_custom_call" | custom-call | tf_op jit(solution)/shard_map/state_grads/pallas_call | solution.py:388
  213.2 4.5 %all-to-all-start.5 = ((f32[32,16,128]{2,1,0:T(8,128)}), f32[32,16,128]{2,1,0:T(8,128)S(1)}, u32[]{:S(2)}, u32[]{:S(2)}) async-start(f32[32,16,128]{2,1,0:T(8,128)} %get-tuple-element.56), calls=%async_computation.5 | async-start | bytes 524288 | tf_op jit(solution)/shard_map/all_to_all | solution.py:631
  217.8 3.1 %add_convert_fusion = bf16[1024,512]{1,0:T(8,128)(2,1)} fusion(bf16[1024,512]{1,0:T(8,128)(2,1)} %collective-permute-done.12, bf16[1024,512]{1,0:T(8,128)(2,1)} %copy-done.23), kind=kLoop, calls=%fused_computation.1 | loop fusion | flops 2097152 | bytes 3145728 | tf_op jit(solution)/shard_map/convert_element_type | solution.py:634
  220.8 5.7 %all-to-all-done.5.got_ref = f32[32,16,128]{2,1,0:T(8,128)S(1)} async-done(((f32[32,16,128]{2,1,0:T(8,128)}), f32[32,16,128]{2,1,0:T(8,128)S(1)}, u32[]{:S(2)}, u32[]{:S(2)}) %all-to-all-start.5) | async-done | bytes 262176 | tf_op jit(solution)/shard_map/all_to_all | solution.py:631
  226.5 4.3 %all-to-all-start.4 = ((bf16[16,64,512]{2,1,0:T(8,128)(2,1)}), bf16[16,64,512]{2,1,0:T(8,128)(2,1)}, u32[]{:S(2)}, u32[]{:S(2)}) async-start(bf16[16,64,512]{2,1,0:T(8,128)(2,1)} %bitcast.62), calls=%async_computation.4 | async-start | bytes 2097152 | tf_op jit(solution)/shard_map/all_to_all | solution.py:637
  233.5 9.6 %gate_up_grads.1 = (bf16[2048,512]{1,0:T(8,128)(2,1)}, bf16[2048,512]{1,0:T(8,128)(2,1)}) custom-call(bf16[768,2048]{1,0:T(8,128)(2,1)} %bitcast.55, bf16[512,2048]{1,0:T(8,128)(2,1)S(1)} %bitcast.44, bf16[768,1024]{1,0:T(8,128)(2,1)S(1)} %copy-done.19, bf16[512,1024]{1,0:T(8,128)(2,1)S(1)} %copy-done.22), custom_call_target="tpu_custom_call" | custom-call | tf_op jit(solution)/shard_map/gate_up_grads/pallas_call | solution.py:250
  243.2 6.1 %down_grads.1 = bf16[512,2048]{1,0:T(8,128)(2,1)} custom-call(bf16[768,512]{1,0:T(8,128)(2,1)S(1)} %copy-done.32, bf16[512,512]{1,0:T(8,128)(2,1)S(1)} %copy-done.36, bf16[768,2048]{1,0:T(8,128)(2,1)} %bitcast.7.got_ref.refs_2_, bf16[512,2048]{1,0:T(8,128)(2,1)S(1)} %bitcast.46), custom_call_target="tpu_custom_call" | custom-call | tf_op jit(solution)/shard_map/down_grads/pallas_call | solution.py:269
  (174 shorter events, 76.5 us)
Async XLA Ops:
  7.9 38.6 %all-to-all-start.1 = ((bf16[32,16,2048]{2,1,0:T(8,128)(2,1)}), bf16[32,16,2048]{2,1,0:T(8,128)(2,1)S(1)}, u32[]{:S(2)}, u32[]{:S(2)}) async-start(bf16[32,16,2048]{2,1,0:T(8,128)(2,1)} %bitcast.48), calls=%async_computation.1 | async-start | bytes 4194304 | tf_op jit(solution)/shard_map/all_to_all | solution.py:565
  47.9 46.8 %all-to-all-start = ((bf16[32,24,2048]{2,1,0:T(8,128)(2,1)}), bf16[32,24,2048]{2,1,0:T(8,128)(2,1)}, u32[]{:S(2)}, u32[]{:S(2)}) async-start(bf16[32,24,2048]{2,1,0:T(8,128)(2,1)} %bitcast.47), calls=%async_computation | async-start | bytes 6291456 | tf_op jit(solution)/shard_map/all_to_all | solution.py:565
  70.9 38.0 %collective-permute-start.4 = (bf16[512,512]{1,0:T(8,128)(2,1)S(1)}, bf16[512,512]{1,0:T(8,128)(2,1)}, u32[]{:S(2)}, u32[]{:S(2)}) collective-permute-start(bf16[512,512]{1,0:T(8,128)(2,1)S(1)} %get-tuple-element.50), channel_id=1, source_target_pairs={{0,1},{1,2},{2,3},{3,0},{4,5},{5,6},{6,7},{7,4},{8,9},{9,10},{10,1... | collective-permute-start | bytes 1572872 | tf_op jit(solution)/shard_map/ppermute | solution.py:287
  103.9 40.2 %copy-start.18 = (bf16[768,1024]{1,0:T(8,128)(2,1)}, bf16[768,1024]{1,0:T(8,128)(2,1)S(1)}, u32[]{:S(2)}) copy-start(bf16[768,1024]{1,0:T(8,128)(2,1)S(1)} %get-tuple-element.35.refs_2_) | copy-start | bytes 4718596
  103.9 21.9 %collective-permute-start = (bf16[768,512]{1,0:T(8,128)(2,1)S(1)}, bf16[768,512]{1,0:T(8,128)(2,1)S(1)}, u32[]{:S(2)}, u32[]{:S(2)}) collective-permute-start(bf16[768,512]{1,0:T(8,128)(2,1)S(1)} %get-tuple-element.45), channel_id=1, source_target_pairs={{0,1},{1,2},{2,3},{3,0},{4,5},{5,6},{6,7},{7,4},{8,9},{9,10},{10,1... | collective-permute-start | bytes 2359304 | tf_op jit(solution)/shard_map/ppermute | solution.py:287
  105.6 14.8 %collective-permute-start.6 = (bf16[512,512]{1,0:T(8,128)(2,1)S(1)}, bf16[512,512]{1,0:T(8,128)(2,1)S(1)}, u32[]{:S(2)}, u32[]{:S(2)}) collective-permute-start(bf16[512,512]{1,0:T(8,128)(2,1)S(1)} %get-tuple-element.51), channel_id=1, source_target_pairs={{0,3},{1,0},{2,1},{3,2},{4,7},{5,4},{6,5},{7,6},{8,11},{9,8},{10,9... | collective-permute-start | bytes 1572872 | tf_op jit(solution)/shard_map/ppermute | solution.py:288
  107.4 29.9 %collective-permute-start.2 = (bf16[768,512]{1,0:T(8,128)(2,1)S(1)}, bf16[768,512]{1,0:T(8,128)(2,1)S(1)}, u32[]{:S(2)}, u32[]{:S(2)}) collective-permute-start(bf16[768,512]{1,0:T(8,128)(2,1)S(1)} %get-tuple-element.46), channel_id=1, source_target_pairs={{0,3},{1,0},{2,1},{3,2},{4,7},{5,4},{6,5},{7,6},{8,11},{9,8},{10,9... | collective-permute-start | bytes 2359304 | tf_op jit(solution)/shard_map/ppermute | solution.py:288
  110.0 31.2 %collective-permute-start.5 = (bf16[256,512]{1,0:T(8,128)(2,1)S(1)}, bf16[256,512]{1,0:T(8,128)(2,1)S(1)}, u32[]{:S(2)}, u32[]{:S(2)}) collective-permute-start(bf16[256,512]{1,0:T(8,128)(2,1)S(1)} %add_convert_fusion.9), channel_id=1, source_target_pairs={{0,1},{1,2},{2,3},{3,0},{4,5},{5,6},{6,7},{7,4},{8,9},{9,10},{10,1... | collective-permute-start | bytes 786440 | tf_op jit(solution)/shard_map/ppermute | solution.py:292
  120.5 22.4 %collective-permute-start.7 = (bf16[256,512]{1,0:T(8,128)(2,1)S(1)}, bf16[256,512]{1,0:T(8,128)(2,1)S(1)}, u32[]{:S(2)}, u32[]{:S(2)}) collective-permute-start(bf16[256,512]{1,0:T(8,128)(2,1)S(1)} %add_convert_fusion.7), channel_id=1, source_target_pairs={{0,3},{1,0},{2,1},{3,2},{4,7},{5,4},{6,5},{7,6},{8,11},{9,8},{10,9... | collective-permute-start | bytes 786440 | tf_op jit(solution)/shard_map/ppermute | solution.py:293
  125.8 18.3 %copy-start.50 = (bf16[768,512]{1,0:T(8,128)(2,1)}, bf16[768,512]{1,0:T(8,128)(2,1)S(1)}, u32[]{:S(2)}) copy-start(bf16[768,512]{1,0:T(8,128)(2,1)S(1)} %collective-permute-done) | copy-start | bytes 2359300
  126.7 22.1 %collective-permute-start.1 = (bf16[384,512]{1,0:T(8,128)(2,1)}, bf16[384,512]{1,0:T(8,128)(2,1)S(1)}, u32[]{:S(2)}, u32[]{:S(2)}) collective-permute-start(bf16[384,512]{1,0:T(8,128)(2,1)} %add_convert_fusion.5), channel_id=1, source_target_pairs={{0,1},{1,2},{2,3},{3,0},{4,5},{5,6},{6,7},{7,4},{8,9},{9,10},{10,1... | collective-permute-start | bytes 1179656 | tf_op jit(solution)/shard_map/ppermute | solution.py:292
  138.2 10.6 %collective-permute-start.3 = (bf16[384,512]{1,0:T(8,128)(2,1)}, bf16[384,512]{1,0:T(8,128)(2,1)}, u32[]{:S(2)}, u32[]{:S(2)}) collective-permute-start(bf16[384,512]{1,0:T(8,128)(2,1)} %add_convert_fusion.3), channel_id=1, source_target_pairs={{0,3},{1,0},{2,1},{3,2},{4,7},{5,4},{6,5},{7,6},{8,11},{9,8},{10,9... | collective-permute-start | bytes 1179656 | tf_op jit(solution)/shard_map/ppermute | solution.py:293
  144.9 15.5 %all-to-all-start.3 = ((bf16[32,16,512]{2,1,0:T(8,128)(2,1)}), bf16[32,16,512]{2,1,0:T(8,128)(2,1)S(1)}, u32[]{:S(2)}, u32[]{:S(2)}) async-start(bf16[32,16,512]{2,1,0:T(8,128)(2,1)} %bitcast.19), calls=%async_computation.3 | async-start | bytes 1048576 | tf_op jit(solution)/shard_map/all_to_all | solution.py:606
  160.4 18.4 %all-to-all-start.2 = ((bf16[32,24,512]{2,1,0:T(8,128)(2,1)}), bf16[32,24,512]{2,1,0:T(8,128)(2,1)S(1)}, u32[]{:S(2)}, u32[]{:S(2)}) async-start(bf16[32,24,512]{2,1,0:T(8,128)(2,1)} %bitcast.63), calls=%async_computation.2 | async-start | bytes 1572864 | tf_op jit(solution)/shard_map/all_to_all | solution.py:606
  167.3 29.2 %copy-start.20 = (bf16[384,512]{1,0:T(8,128)(2,1)S(1)}, bf16[384,512]{1,0:T(8,128)(2,1)}, u32[]{:S(2)}) copy-start(bf16[384,512]{1,0:T(8,128)(2,1)} %branch_ref.1) | copy-start | bytes 1179652
  167.3 29.2 %copy-start.56 = (f32[384]{0:T(512)S(1)}, f32[384]{0:T(512)}, u32[]{:S(2)}) copy-start(f32[384]{0:T(512)} %param.29) | copy-start | bytes 4612
  178.9 17.7 %copy-start.54 = (f32[384,512]{1,0:T(8,128)S(1)}, f32[384,512]{1,0:T(8,128)}, u32[]{:S(2)}) copy-start(f32[384,512]{1,0:T(8,128)} %param.26) | copy-start | bytes 2359300
  179.6 12.3 %collective-permute-start.8 = (bf16[384,512]{1,0:T(8,128)(2,1)S(1)}, bf16[384,512]{1,0:T(8,128)(2,1)S(1)}, u32[]{:S(2)}, u32[]{:S(2)}) collective-permute-start(bf16[384,512]{1,0:T(8,128)(2,1)S(1)} %combine.1.z0), channel_id=1, source_target_pairs={{0,1},{1,2},{2,3},{3,0},{4,5},{5,6},{6,7},{7,4},{8,9},{9,10},{10,1... | collective-permute-start | bytes 1179656 | tf_op jit(solution)/shard_map/ppermute | solution.py:613
  181.2 11.7 %collective-permute-start.9 = (bf16[384,512]{1,0:T(8,128)(2,1)S(1)}, bf16[384,512]{1,0:T(8,128)(2,1)S(1)}, u32[]{:S(2)}, u32[]{:S(2)}) collective-permute-start(bf16[384,512]{1,0:T(8,128)(2,1)S(1)} %combine.1.z0), channel_id=1, source_target_pairs={{0,3},{1,0},{2,1},{3,2},{4,7},{5,4},{6,5},{7,6},{8,11},{9,8},{10,9... | collective-permute-start | bytes 1179656 | tf_op jit(solution)/shard_map/ppermute | solution.py:614
  192.6 7.7 %collective-permute-start.10 = (bf16[192,512]{1,0:T(8,128)(2,1)}, bf16[192,512]{1,0:T(8,128)(2,1)S(1)}, u32[]{:S(2)}, u32[]{:S(2)}) collective-permute-start(bf16[192,512]{1,0:T(8,128)(2,1)} %slice.104), channel_id=1, source_target_pairs={{0,1},{1,2},{2,3},{3,0},{4,5},{5,6},{6,7},{7,4},{8,9},{9,10},{10,1... | collective-permute-start | bytes 589832 | tf_op jit(solution)/shard_map/ppermute | solution.py:615
  193.6 6.7 %collective-permute-start.11 = (bf16[192,512]{1,0:T(8,128)(2,1)}, bf16[192,512]{1,0:T(8,128)(2,1)S(1)}, u32[]{:S(2)}, u32[]{:S(2)}) collective-permute-start(bf16[192,512]{1,0:T(8,128)(2,1)} %slice.105), channel_id=1, source_target_pairs={{0,3},{1,0},{2,1},{3,2},{4,7},{5,4},{6,5},{7,6},{8,11},{9,8},{10,9... | collective-permute-start | bytes 589832 | tf_op jit(solution)/shard_map/ppermute | solution.py:616
  202.7 15.1 %collective-permute-start.12 = (bf16[1024,512]{1,0:T(8,128)(2,1)}, bf16[1024,512]{1,0:T(8,128)(2,1)}, u32[]{:S(2)}, u32[]{:S(2)}) collective-permute-start(bf16[1024,512]{1,0:T(8,128)(2,1)} %get-tuple-element.54), channel_id=1, source_target_pairs={{0,4},{4,0},{8,12},{12,8},{16,20},{20,16},{24,28},{28,24},{32,36},... | collective-permute-start | bytes 3145736 | tf_op jit(solution)/shard_map/ppermute | solution.py:633
  213.2 13.3 %all-to-all-start.5 = ((f32[32,16,128]{2,1,0:T(8,128)}), f32[32,16,128]{2,1,0:T(8,128)S(1)}, u32[]{:S(2)}, u32[]{:S(2)}) async-start(f32[32,16,128]{2,1,0:T(8,128)} %get-tuple-element.56), calls=%async_computation.5 | async-start | bytes 524288 | tf_op jit(solution)/shard_map/all_to_all | solution.py:631
  226.5 27.5 %all-to-all-start.4 = ((bf16[16,64,512]{2,1,0:T(8,128)(2,1)}), bf16[16,64,512]{2,1,0:T(8,128)(2,1)}, u32[]{:S(2)}, u32[]{:S(2)}) async-start(bf16[16,64,512]{2,1,0:T(8,128)(2,1)} %bitcast.62), calls=%async_computation.4 | async-start | bytes 2097152 | tf_op jit(solution)/shard_map/all_to_all | solution.py:637
  (55 other events, 333.8 us)

commit v2 on v1

v2 whole, which is shorter than its diff:
```python
import functools

import jax
import jax.numpy as jnp
from jax import lax
from jax.experimental import pallas as pl
from jax.experimental.pallas import tpu as pltpu
from jax.sharding import PartitionSpec as P


gate_scale_factor = 8.0
clamp_limit = 7.0
glu_alpha = 1.702

BF = jnp.bfloat16
F32 = jnp.float32

SLOT_GROUPS = (24, 16)

ROWS_ROWS = (((1,), (1,)), ((), ()))
COLS_COLS = (((0,), (0,)), ((), ()))


def params(limit_mib):
    return pltpu.CompilerParams(vmem_limit_bytes=limit_mib * 1024 * 1024)


def hbm(shape, dtype=BF):
    return pltpu.HBM(shape, dtype)


def in_hbm(*arrays):
    return tuple(pltpu.with_memory_space_constraint(a, pltpu.HBM) for a in arrays)


def iota(shape, dim):
    return lax.broadcasted_iota(jnp.int32, shape, dim)


def placed_row(expert, slot, experts):
    base, row = 0, None
    for size in SLOT_GROUPS:
        here = base * experts + expert * size + (slot - base)
        row = here if row is None else jnp.where(slot >= base, here, row)
        base += size
    return row


def slots_kernel(idx_ref, idx_t_ref, col_ref, row_ref, *, experts):
    tokens, top = idx_ref.shape
    a, b = iota((tokens, tokens), 0), iota((tokens, tokens), 1)
    hot = [idx_ref[:, k : k + 1] == iota((tokens, experts), 1) for k in range(top)]
    both = sum(h.astype(F32) for h in hot).astype(BF)
    before = jnp.dot((b < a).astype(F32).astype(BF), both, preferred_element_type=F32)
    for k in range(top):
        rank = jnp.sum(jnp.where(hot[k], before, 0.0), axis=1, keepdims=True).astype(jnp.int32)
        col_ref[:, k : k + 1] = idx_ref[:, k : k + 1] * sum(SLOT_GROUPS) + rank
    hot = [idx_t_ref[k : k + 1, :] == iota((experts, tokens), 0) for k in range(top)]
    both = sum(h.astype(F32) for h in hot).astype(BF)
    before = jnp.dot(both, (a < b).astype(F32).astype(BF), preferred_element_type=F32)
    for k in range(top):
        rank = jnp.sum(jnp.where(hot[k], before, 0.0), axis=0, keepdims=True).astype(jnp.int32)
        row_ref[k : k + 1, :] = placed_row(idx_t_ref[k : k + 1, :], rank, experts)


def slot_rows(chosen, experts):
    tokens, top = chosen.shape
    return pl.pallas_call(
        functools.partial(slots_kernel, experts=experts),
        out_shape=(
            jax.ShapeDtypeStruct((tokens, top), jnp.int32),
            jax.ShapeDtypeStruct((top, tokens), jnp.int32),
        ),
        compiler_params=params(8),
        name="slots",
    )(chosen, chosen.T)


def dispatch_kernel(row_ref, weight_ref, cot_ref, out_ref, *, first):
    rows, tokens = out_ref.shape[0], cot_ref.shape[0]
    at = first + pl.program_id(0) * rows + iota((rows, tokens), 0)
    weight = jnp.zeros((rows, tokens), F32)
    for k in range(row_ref.shape[0]):
        weight = jnp.where(row_ref[k : k + 1, :] == at, weight_ref[k : k + 1, :], weight)
    picked = jnp.dot((weight > 0.0).astype(F32).astype(BF), cot_ref[...], preferred_element_type=F32)
    out_ref[...] = (picked * jnp.sum(weight, axis=1, keepdims=True)).astype(BF)


def dispatch(row, weight_t, cot, first, count):
    _, width = cot.shape
    block = 256
    return pl.pallas_call(
        functools.partial(dispatch_kernel, first=first),
        grid=(count // block,),
        in_specs=[
            pl.BlockSpec(row.shape, lambda i: (0, 0)),
            pl.BlockSpec(weight_t.shape, lambda i: (0, 0)),
            pl.BlockSpec(cot.shape, lambda i: (0, 0)),
        ],
        out_specs=pl.BlockSpec((block, width), lambda i: (i, 0)),
        out_shape=hbm((count, width)),
        compiler_params=params(10),
        name="dispatch",
    )(row, weight_t, cot)


def hold_kernel(*refs):
    count = len(refs) // 2
    sems = refs[-1]
    copies = [
        pltpu.make_async_copy(refs[i], refs[count + i], sems.at[i]) for i in range(count)
    ]
    for copy in copies:
        copy.start()
    for copy in copies:
        copy.wait()


def held(*arrays):
    return pl.pallas_call(
        hold_kernel,
        in_specs=[pl.BlockSpec(memory_space=pl.ANY)] * len(arrays),
        out_specs=tuple([pl.BlockSpec(memory_space=pltpu.VMEM)] * len(arrays)),
        out_shape=tuple(pltpu.VMEM(a.shape, a.dtype) for a in arrays),
        scratch_shapes=[pltpu.SemaphoreType.DMA((len(arrays),))],
        compiler_params=params(4),
        name="fetch",
    )(*in_hbm(*arrays))


def forward_kernel(x_ref, gate_ref, up_ref, act_ref, slope_ref):
    x = x_ref[...]
    hidden = gate_ref.shape[1]
    gate_pre = jnp.dot(x, gate_ref[...], preferred_element_type=F32)
    up_pre = jnp.dot(x, up_ref[...], preferred_element_type=F32)
    glu = jnp.minimum(gate_pre, clamp_limit)
    lin = jnp.clip(up_pre, -clamp_limit, clamp_limit) + 1.0
    sig = 1.0 / (1.0 + jnp.exp(-glu_alpha * glu))
    silu = glu * sig
    act_ref[...] = (silu * lin).astype(BF)
    slope = lin * (sig + glu_alpha * silu * (1.0 - sig))
    slope_ref[:, :hidden] = jnp.where(gate_pre < clamp_limit, slope, 0.0)
    slope_ref[:, hidden:] = jnp.where(jnp.abs(up_pre) < clamp_limit, silu, 0.0)


def expert_forward(x, w_gate, w_up):
    rows, width = x.shape
    hidden = w_gate.shape[1]
    block = 256
    whole = pl.BlockSpec(memory_space=pltpu.VMEM)
    return pl.pallas_call(
        forward_kernel,
        grid=(rows // block,),
        in_specs=[pl.BlockSpec((block, width), lambda i: (i, 0)), whole, whole],
        out_specs=(
            pl.BlockSpec((block, hidden), lambda i: (i, 0)),
            pl.BlockSpec((block, 2 * hidden), lambda i: (i, 0)),
        ),
        out_shape=(hbm((rows, hidden)), hbm((rows, 2 * hidden), F32)),
        compiler_params=params(16),
        name="expert_forward",
    )(x, w_gate, w_up)


def turned_columns(rank, ref_count, part, n_tp):
    if ref_count == 1:
        return [0]
    start = lambda ahead: lax.rem(rank + ahead, n_tp) * part
    half = part // 2
    starts = [start(0), start(1), start(2), start(2) + half, start(3)]
    return [pl.multiple_of(at, half) for at in starts]


def backward_kernel(rank_ref, *refs, count, n_tp):
    got_refs, refs = refs[:count], refs[count:]
    slope_ref, down_ref, gate_ref, up_ref = refs[:4]
    both_ref, up1_ref, dn1_ref, up2_ref, dn2_ref, mine_ref = refs[4:]
    width = mine_ref.shape[1]
    half = width // 2
    hidden = down_ref.shape[0]
    d_act = None
    for got_ref, at in zip(got_refs, turned_columns(rank_ref[0], count, width, n_tp)):
        columns = down_ref[:, pl.ds(at, got_ref.shape[1])]
        term = lax.dot_general(got_ref[...], columns, ROWS_ROWS, preferred_element_type=F32)
        d_act = term if d_act is None else d_act + term
    d_gate = (d_act * slope_ref[:, :hidden]).astype(BF)
    d_up = (d_act * slope_ref[:, hidden:]).astype(BF)
    both_ref[:, :hidden] = d_gate
    both_ref[:, hidden:] = d_up

    def term(ahead):
        at = pl.multiple_of(lax.rem(rank_ref[0] + ahead, n_tp) * width, width)
        both = lax.dot_general(
            d_gate, gate_ref[pl.ds(at, width), :], ROWS_ROWS, preferred_element_type=F32
        )
        both = both + lax.dot_general(
            d_up, up_ref[pl.ds(at, width), :], ROWS_ROWS, preferred_element_type=F32
        )
        return both.astype(BF)

    away = term(2)
    up1_ref[:, :half] = away[:, :half]
    dn1_ref[:, :half] = away[:, half:]
    above = term(1)
    up1_ref[:, half:] = above[:, half:]
    up2_ref[...] = above[:, :half]
    below = term(3)
    dn1_ref[:, half:] = below[:, :half]
    dn2_ref[...] = below[:, half:]
    mine_ref[...] = term(0)


def expert_backward(rank, gots, slope, w_down, w_gate, w_up, n_tp):
    rows = gots[0].shape[0]
    hidden, width = w_down.shape
    part = width // n_tp
    block = 256
    by_rows = lambda cols: pl.BlockSpec((block, cols), lambda i: (i, 0))
    whole = pl.BlockSpec(memory_space=pltpu.VMEM)
    outs = (2 * hidden, part, part, part // 2, part // 2, part)
    return pl.pallas_call(
        functools.partial(backward_kernel, count=len(gots), n_tp=n_tp),
        grid=(rows // block,),
        in_specs=[pl.BlockSpec(memory_space=pltpu.SMEM)]
        + [by_rows(g.shape[1]) for g in gots]
        + [
            by_rows(2 * hidden),
            whole,
            whole,
            whole,
        ],
        out_specs=tuple(by_rows(c) for c in outs),
        out_shape=tuple(hbm((rows, c)) for c in outs),
        compiler_params=params(16),
        name="expert_backward",
    )(rank, *gots, slope, w_down, w_gate, w_up)


def summed_products(lefts, rights):
    total = None
    for left, right in zip(lefts, rights):
        term = lax.dot_general(left[...], right[...], COLS_COLS, preferred_element_type=F32)
        total = term if total is None else total + term
    return total


def gate_up_kernel(*refs, groups):
    gate_ref, up_ref = refs[2 * groups :]
    total = summed_products(refs[:groups], refs[groups : 2 * groups])
    hidden = gate_ref.shape[1]
    gate_ref[...] = total[:, :hidden].astype(BF)
    up_ref[...] = total[:, hidden:].astype(BF)


def gate_up_grads(saved, both):
    width, hidden = saved[0].shape[1], both[0].shape[1] // 2
    block = 256
    out = pl.BlockSpec((block, hidden), lambda i: (i, 0))
    return pl.pallas_call(
        functools.partial(gate_up_kernel, groups=len(saved)),
        grid=(width // block,),
        in_specs=[pl.BlockSpec((x.shape[0], block), lambda i: (0, i)) for x in saved]
        + [pl.BlockSpec(g.shape, lambda i: (0, 0)) for g in both],
        out_specs=(out, out),
        out_shape=(jax.ShapeDtypeStruct((width, hidden), BF),) * 2,
        compiler_params=params(16),
        name="gate_up_grads",
    )(*saved, *both)


def down_kernel(rank_ref, first_act, second_act, *refs, n_tp):
    pieces, second, out_ref = refs[:-2], refs[-2], refs[-1]
    part = second.shape[1] // n_tp
    for piece, at in zip(pieces, turned_columns(rank_ref[0], len(pieces), part, n_tp)):
        columns = pl.ds(at, piece.shape[1])
        total = lax.dot_general(first_act[...], piece[...], COLS_COLS, preferred_element_type=F32)
        total = total + lax.dot_general(
            second_act[...], second[:, columns], COLS_COLS, preferred_element_type=F32
        )
        out_ref[:, columns] = total.astype(BF)


def down_grads(rank, acts, received, n_tp):
    pieces, (second,) = received
    arrays = (*acts, *pieces, second)
    whole = lambda *shape: pl.BlockSpec(shape, lambda i: (0, 0))
    out = (acts[0].shape[1], second.shape[1])
    return pl.pallas_call(
        functools.partial(down_kernel, n_tp=n_tp),
        grid=(1,),
        in_specs=[pl.BlockSpec(memory_space=pltpu.SMEM)] + [whole(*a.shape) for a in arrays],
        out_specs=whole(*out),
        out_shape=hbm(out),
        compiler_params=params(32),
        name="down_grads",
    )(rank, *in_hbm(*arrays))


def ring(n, step):
    return [(i, (i + step) % n) for i in range(n)]


def gathered_over_tp(x, n_tp):
    half = x.shape[1] // 2
    below = lax.ppermute(x, "tp", ring(n_tp, 1))
    above = lax.ppermute(x, "tp", ring(n_tp, -1))
    left, right = below[:, :half], above[:, half:]
    left = lax.ppermute(left, "tp", ring(n_tp, 1))
    right = lax.ppermute(right, "tp", ring(n_tp, -1))
    return below, above, left, right


def summed_over_tp(up1, dn1, up2, dn2, mine, n_tp):
    half = up2.shape[1]
    from_below = lax.ppermute(up1, "tp", ring(n_tp, 1))
    from_above = lax.ppermute(dn1, "tp", ring(n_tp, -1))
    add = lambda a, b: (a.astype(F32) + b.astype(F32)).astype(BF)
    up2 = add(up2, from_below[:, :half])
    dn2 = add(dn2, from_above[:, :half])
    left = lax.ppermute(up2, "tp", ring(n_tp, 1))
    right = lax.ppermute(dn2, "tp", ring(n_tp, -1))
    far = jnp.concatenate([left, right], axis=1).astype(F32)
    near = jnp.concatenate([from_above[:, half:], from_below[:, half:]], axis=1).astype(F32)
    return (mine.astype(F32) + far + near).astype(BF)


def combine_kernel(col_ref, cot_ref, back_ref, out_ref):
    tokens, top = col_ref.shape
    at = iota((tokens, back_ref.shape[0]), 1)
    hit = col_ref[:, 0:1] == at
    for k in range(1, top):
        hit = hit | (col_ref[:, k : k + 1] == at)
    total = jnp.dot(hit.astype(F32).astype(BF), back_ref[...], preferred_element_type=F32)
    out_ref[...] = (cot_ref[...].astype(F32) + total).astype(BF)


def combine(col, cot_part, back):
    return pl.pallas_call(
        combine_kernel,
        out_shape=jax.ShapeDtypeStruct(cot_part.shape, BF),
        compiler_params=params(16),
        name="combine",
    )(col, cot_part, back)


def pieces_of(rank_ref, z_refs, n_tp):
    z0, z_below, z_above, z_top, z_bottom = z_refs
    me = rank_ref[0]
    away = jnp.concatenate([z_top[...], z_bottom[...]], axis=1)
    order = ((0, z0[...]), (n_tp - 1, z_below[...]), (1, z_above[...]), (2, away))
    width = z0.shape[1]
    return [(pl.multiple_of(lax.rem(me + a, n_tp) * width, width), z) for a, z in order]


def state_kernel(
    rank_ref,
    z0,
    z1,
    z2,
    z3,
    z4,
    w_hbm,
    mixed_ref,
    branch_ref,
    decay_ref,
    later_ref,
    earlier_ref,
    branch_grad_ref,
    state_ref,
    carry_ref,
    w_ref,
    sem,
    *,
    n_tp,
):
    copy = pltpu.make_async_copy(w_hbm, w_ref, sem)
    copy.start()
    copy.wait()
    total = None
    for at, z in pieces_of(rank_ref, (z0, z1, z2, z3, z4), n_tp):
        term = jnp.dot(z, w_ref[pl.ds(at, z.shape[1]), :], preferred_element_type=F32)
        total = term if total is None else total + term
    branch_grad_ref[...] = (total * mixed_ref[...].astype(F32)).astype(BF)
    state = total * branch_ref[...].astype(F32)
    state_ref[...] = state
    scaled = state * decay_ref[...]
    ahead = jnp.sum(scaled * earlier_ref[...], axis=0, keepdims=True)
    behind = jnp.sum(scaled * later_ref[...], axis=0, keepdims=True)
    last = slice(state.shape[0] - 1, state.shape[0])
    through = decay_ref[last, :] * earlier_ref[last, :]
    lanes = carry_ref.shape[2]
    count = ahead.shape[1] // lanes
    tile = jnp.concatenate(
        [
            v[:, b * lanes : (b + 1) * lanes]
            for v in (ahead, behind, through, through)
            for b in range(count)
        ],
        axis=0,
    )
    carry_ref[...] = jnp.broadcast_to(tile[None], carry_ref.shape)


def state_grads(rank, zs, w_out, mixed, branch, decay, later_prod, earlier_prod, n_sp, n_tp):
    tokens, channels = mixed.shape
    full = lambda *shape: pl.BlockSpec(shape, lambda i: (0,) * len(shape))
    held = full(tokens, channels)
    carry = (n_sp, 16, channels // 4)
    return pl.pallas_call(
        functools.partial(state_kernel, n_tp=n_tp),
        grid=(1,),
        in_specs=[pl.BlockSpec(memory_space=pltpu.SMEM)]
        + [full(*z.shape) for z in zs]
        + [pl.BlockSpec(memory_space=pl.ANY)]
        + [held] * 5,
        out_specs=(held, held, full(*carry)),
        out_shape=(hbm((tokens, channels)), hbm((tokens, channels), F32), hbm(carry, F32)),
        scratch_shapes=[pltpu.VMEM(w_out.shape, BF), pltpu.SemaphoreType.DMA(())],
        compiler_params=params(32),
        name="state_grads",
    )(rank, *zs, *in_hbm(w_out, mixed, branch, decay, later_prod, earlier_prod))


def proj_kernel(rank_ref, core_ref, z_ref, own, above, left, right, below, keep_ref, send_ref, *, n_tp, size):
    z = z_ref[...]
    me = rank_ref[0]
    same = lax.rem(me + core_ref[0], 2) == 0

    def term(ahead):
        if ahead == 2:
            channels = jnp.concatenate([left[...], right[...]], axis=1)
        else:
            channels = {0: own, 1: above, 3: below}[ahead][...]
        return lax.dot_general(z, channels, COLS_COLS, preferred_element_type=F32).astype(BF)

    for a, b in ((0, 1), (2, 3)):
        first, second = term(a), term(b)
        at = [lax.rem(me + ahead, n_tp) // 2 for ahead in (a, b)]
        kept = jnp.where(same, at[0], at[1]) * size
        sent = jnp.where(same, at[1], at[0]) * size
        for i in range(first.shape[0] // size):
            rows = slice(i * size, (i + 1) * size)
            base = i * (n_tp // 2) * size
            keep_ref[pl.ds(pl.multiple_of(base + kept, size), size), :] = jnp.where(
                same, first[rows], second[rows]
            )
            send_ref[pl.ds(pl.multiple_of(base + sent, size), size), :] = jnp.where(
                same, second[rows], first[rows]
            )


def proj_terms(rank, core, z, gateds, n_tp, n_sp):
    features, channels = z.shape[1], gateds[0].shape[1]
    size = features * n_tp // n_sp
    half = jax.ShapeDtypeStruct((features * n_tp // 2, channels), BF)
    return pl.pallas_call(
        functools.partial(proj_kernel, n_tp=n_tp, size=size),
        in_specs=[pl.BlockSpec(memory_space=pltpu.SMEM)] * 2
        + [pl.BlockSpec(memory_space=pltpu.VMEM)] * 6,
        out_shape=(half, half),
        compiler_params=params(20),
        name="proj_terms",
    )(rank, core, z, *gateds)


def carried_in(me, got_ref):
    count, half = got_ref.shape[0], got_ref.shape[1] // 2
    carry = lambda q: got_ref[q, :half, :]
    through = lambda q: got_ref[q, half:, :]
    zero = jnp.zeros((half, got_ref.shape[2]), F32)
    ahead, behind = zero, zero
    for q in range(count):
        p = count - 1 - q
        ahead = jnp.where(p > me, carry(p) + through(p) * ahead, ahead)
        behind = jnp.where(q < me, carry(q) + through(q) * behind, behind)
    return ahead[: half // 2], behind[half // 2 :]


def final_kernel(
    me_ref,
    got_ref,
    state_ref,
    decay_ref,
    h_later,
    h_earlier,
    q_ref,
    r_ref,
    rec_w,
    inp_w,
    out_ref,
    later_ref,
    earlier_ref,
):
    rows = state_ref.shape[0]
    ahead, behind = carried_in(me_ref[0], got_ref)
    spread = lambda v: jnp.concatenate([v[b : b + 1] for b in range(v.shape[0])], axis=1)

    def step(i, carry):
        ahead, behind = carry
        t = rows - 1 - i
        later = state_ref[pl.ds(t, 1), :] + ahead
        later_ref[pl.ds(t, 1), :] = later
        earlier = state_ref[pl.ds(i, 1), :] + behind
        earlier_ref[pl.ds(i, 1), :] = earlier
        return (later * decay_ref[pl.ds(t, 1), :], earlier * decay_ref[pl.ds(i, 1), :])

    lax.fori_loop(0, rows, step, (spread(ahead), spread(behind)), unroll=8)
    later, earlier = later_ref[...], earlier_ref[...]
    total = later + earlier
    rec_pre = (later * h_later[...] + earlier * h_earlier[...]).astype(BF)
    inp_pre = (total * q_ref[...]).astype(BF)
    direct = total * r_ref[...]
    size = rec_w.shape[1]
    for b in range(rec_w.shape[0]):
        cols = slice(b * size, (b + 1) * size)
        term = lax.dot_general(rec_pre[:, cols], rec_w[b], ROWS_ROWS, preferred_element_type=F32)
        term = term + lax.dot_general(
            inp_pre[:, cols], inp_w[b], ROWS_ROWS, preferred_element_type=F32
        )
        out_ref[:, cols] = (direct[:, cols] + term).astype(BF)


def final_grads(me, got, arrays, rec_w, inp_w):
    tokens, channels = arrays[0].shape
    rows = pl.BlockSpec((tokens, channels), lambda i: (0, 0))
    fixed = lambda a: pl.BlockSpec(a.shape, lambda i: (0,) * a.ndim)
    return pl.pallas_call(
        final_kernel,
        grid=(1,),
        in_specs=[pl.BlockSpec(memory_space=pltpu.SMEM), fixed(got)]
        + [rows] * len(arrays)
        + [fixed(rec_w), fixed(inp_w)],
        out_specs=rows,
        out_shape=hbm((tokens, channels)),
        scratch_shapes=[pltpu.VMEM((tokens, channels), F32)] * 2,
        compiler_params=params(32),
        name="final_grads",
    )(me, got, *in_hbm(*arrays, rec_w, inp_w))


def blockwise(rows, weights):
    size = weights.shape[1]
    return jnp.concatenate(
        [
            jnp.dot(rows[:, b * size : (b + 1) * size], weights[b], preferred_element_type=F32)
            for b in range(weights.shape[0])
        ],
        axis=1,
    )


def shards(
    output_cotangent,
    chosen_expert_index,
    chosen_expert_weight,
    expert_slot_tokens,
    expert_gate_matrix,
    expert_up_matrix,
    expert_down_matrix,
    output_projection_matrix,
    recurrence_input,
    branch_activation_values,
    forward_scan_state,
    reverse_scan_state,
    channel_decay_rate,
    position_extra_log_decay,
    recurrence_gate_weights,
    input_gate_weights,
):
    n_sp = lax.axis_size("sp")
    n_tp = lax.axis_size("tp")
    tokens, model_width = output_cotangent.shape
    experts = n_sp * expert_gate_matrix.shape[0]
    capacity = expert_slot_tokens.shape[1] // n_sp
    slots = expert_slot_tokens.shape[1]
    part = model_width // n_tp
    rank = lax.axis_index("tp").astype(jnp.int32).reshape(1)
    place = lax.axis_index("sp").astype(jnp.int32).reshape(1)
    bounds, at = [], 0
    for size in SLOT_GROUPS:
        bounds.append((at, size))
        at += size

    col, row = slot_rows(chosen_expert_index, experts)
    weight_t = chosen_expert_weight.T
    cot_part = lax.dynamic_slice_in_dim(output_cotangent, rank[0] * part, part, 1)
    w_gate, w_up, w_down = expert_gate_matrix[0], expert_up_matrix[0], expert_down_matrix[0]
    received = []
    for g, (base, size) in enumerate(bounds):
        cot = output_cotangent if g else cot_part
        out = dispatch(row, weight_t, cot, base * experts, size * experts)
        got = lax.all_to_all(out.reshape(experts, size, -1), "sp", 0, 0, tiled=True)
        got = got.reshape(n_sp * size, -1)
        if g:
            received.append((got,))
        else:
            below, above, left, right = gathered_over_tp(got, n_tp)
            received.append((got, above, left, right, below))
    w_down, w_gate_held, w_up_held = held(w_down, w_gate, w_up)

    by_source = expert_slot_tokens.reshape(n_sp, capacity, model_width)
    saved, acts, slopes = [], [], []
    for g, (base, size) in enumerate(bounds):
        x = by_source[:, base : base + size].reshape(n_sp * size, model_width)
        if g:
            w_gate, w_up = w_gate_held, w_up_held
        act, slope = expert_forward(x, w_gate, w_up)
        saved.append(x)
        acts.append(act)
        slopes.append(slope)

    rec = jax.nn.sigmoid(blockwise(recurrence_input, recurrence_gate_weights))
    inp = jax.nn.sigmoid(blockwise(recurrence_input, input_gate_weights))
    rate = -gate_scale_factor * channel_decay_rate[None, :]
    log_decay = rec * rate + position_extra_log_decay[:, None]
    decay = jnp.exp(log_decay)
    scale_in = jnp.sqrt(-jnp.expm1(2.0 * log_decay))
    inputs = recurrence_input.astype(F32)
    xin = scale_in * inp * inputs
    mixed = (
        (decay * forward_scan_state + xin) + (decay * reverse_scan_state + xin)
    ).astype(BF)
    gated = (mixed.astype(F32) * branch_activation_values.astype(F32)).astype(BF)
    lower = (iota((tokens, tokens), 1) <= iota((tokens, tokens), 0)).astype(F32)
    running = jnp.dot(lower, log_decay, precision=lax.Precision.HIGHEST)
    later_prod = jnp.exp(running[-1:] - running)
    earlier_prod = jnp.exp(running - log_decay)
    rec_slope = rate * rec * (1.0 - rec)
    shared = inp * inputs * decay * decay / scale_in
    h_later = (forward_scan_state * decay - shared) * rec_slope
    h_earlier = (reverse_scan_state * decay - shared) * rec_slope
    q = scale_in * inputs * inp * (1.0 - inp)
    r = scale_in * inp

    boths, sums = [], []
    for g, (base, size) in enumerate(bounds):
        both, *terms = expert_backward(
            rank, received[g], slopes[g], w_down, w_gate, w_up, n_tp
        )
        sums.append(summed_over_tp(*terms, n_tp).reshape(n_sp, size, part))
        boths.append(both)
    back = lax.all_to_all(jnp.concatenate(sums, axis=1), "sp", 0, 0, tiled=True)
    gate_grad, up_grad = gate_up_grads(saved, boths)
    down_grad = down_grads(rank, acts, received, n_tp)

    below, above, left, right = gathered_over_tp(gated, n_tp)
    gateds = (gated, above, left, right, below)

    z0 = combine(col, cot_part, back.reshape(slots, part))
    zs = (z0, *gathered_over_tp(z0, n_tp))

    keep, send = proj_terms(rank, place % 2, z0, gateds, n_tp, n_sp)
    other = lax.ppermute(send, "sp", [(i, i ^ 1) for i in range(n_sp)])
    terms = (keep.astype(F32) + other.astype(F32)).astype(BF)
    terms = terms.reshape(n_sp // 2, model_width // n_sp, -1)
    groups = [list(range(c, n_sp, 2)) for c in range(2)]
    terms = lax.all_to_all(terms, "sp", 0, 0, axis_index_groups=groups, tiled=True)
    proj_grad = jnp.sum(terms.astype(F32), axis=0)
    spread = n_sp // n_tp
    moves = [
        (s * n_tp + x, (x * spread + s // n_tp) * n_tp + s % n_tp)
        for s in range(n_sp)
        for x in range(n_tp)
    ]
    proj_grad = lax.ppermute(proj_grad, ("sp", "tp"), moves)

    branch_grad, state, carry = state_grads(
        rank,
        zs,
        output_projection_matrix,
        mixed,
        branch_activation_values,
        decay,
        later_prod,
        earlier_prod,
        n_sp,
        n_tp,
    )
    carried = lax.all_to_all(carry, "sp", 0, 0, tiled=True)
    input_grad = final_grads(
        place,
        carried,
        (state, decay, h_later, h_earlier, q, r),
        recurrence_gate_weights,
        input_gate_weights,
    )
    return (gate_grad[None], up_grad[None], down_grad[None], proj_grad, branch_grad, input_grad)


def solution(mesh):
    in_specs = (
        P("sp", None),
        P("sp", None),
        P("sp", None),
        P("sp", None, None),
        P("sp", None, "tp"),
        P("sp", None, "tp"),
        P("sp", "tp", None),
        P(None, "tp"),
        P("sp", "tp"),
        P("sp", "tp"),
        P("sp", "tp"),
        P("sp", "tp"),
        P("tp"),
        P("sp"),
        P("tp", None, None),
        P("tp", None, None),
    )
    out_specs = (
        P("sp", None, "tp"),
        P("sp", None, "tp"),
        P("sp", "tp", None),
        P("sp", "tp"),
        P("sp", "tp"),
        P("sp", "tp"),
    )
    return jax.shard_map(shards, mesh=mesh, in_specs=in_specs, out_specs=out_specs, check_vma=False)
```

time: 259 us -> 267 us (1.031)
  the two profiles are of different devices: /device:TPU:0 before, /device:TPU:13 now
where the time goes in v2:
time: 267 us; the launch traced here: 266 us
  waiting for transfers between devices  81.6 us (31%)
  starting transfers between devices  70.5 us (26%)
  Pallas kernels  64.2 us (24%)
  local copies, waits for them, and re-layouts  29.3 us (11%)
  other arithmetic  12.9 us (5%)
  matrix products  6.01 us (2%)
    ppermute x3, waiting for transfers between devices, gathered_over_tp(): below = lax.ppermute(x, 'tp', ring(n_tp, 1))  30.9 us
    unnamed x110, local copies, waits for them, and re-layouts  20.9 us
    ppermute x2, waiting for transfers between devices, summed_over_tp(): from_above = lax.ppermute(dn1, 'tp', ring(n_tp, -1))  18 us
    all_to_all x2, starting transfers between devices, shards(): got = lax.all_to_all(out.reshape(experts, size, -1), 'sp', 0, 0, tiled=True)  14.5 us
    pallas_call x2, Pallas kernels, expert_backward(): pl.pallas_call(functools.partial(backward_kernel, count=len(gots), n_tp=n...  13.8 us
    ppermute x2, waiting for transfers between devices, summed_over_tp(): right = lax.ppermute(dn2, 'tp', ring(n_tp, -1))  12.3 us
    all_to_all x2, waiting for transfers between devices, shards(): got = lax.all_to_all(out.reshape(experts, size, -1), 'sp', 0, 0, tiled=True)  11 us
    all_to_all x1, starting transfers between devices, shards(): back = lax.all_to_all(jnp.concatenate(sums, axis=1), 'sp', 0, 0, tiled=True)  10.4 us
  transfers between devices with their start and end apart: 27, of which 13 were waited for; matrix products, arithmetic and copies ran while one was open for 9% of the time, Pallas kernels for 22%

profile of v2, /device:TPU:13, one launch (start us, length us, event | category | flops | bytes accessed | tf_op | source)
XLA Modules:
  0.0 265.8 jit_solution(13686530905471941870)
XLA Ops:
  7.2 8.8 %all-to-all-start = ((bf16[32,24,512]{2,1,0:T(8,128)(2,1)}), bf16[32,24,512]{2,1,0:T(8,128)(2,1)S(1)}, u32[]{:S(2)}, u32[]{:S(2)}) async-start(bf16[32,24,512]{2,1,0:T(8,128)(2,1)} %bitcast.53), calls=%async_computation | async-start | bytes 1572864 | tf_op jit(solution)/shard_map/all_to_all | solution.py:592
  18.6 11.0 %all-to-all-done = bf16[32,24,512]{2,1,0:T(8,128)(2,1)S(1)} async-done(((bf16[32,24,512]{2,1,0:T(8,128)(2,1)}), bf16[32,24,512]{2,1,0:T(8,128)(2,1)S(1)}, u32[]{:S(2)}, u32[]{:S(2)}) %all-to-all-start) | async-done | bytes 786464 | tf_op jit(solution)/shard_map/all_to_all | solution.py:592
  29.5 5.7 %all-to-all-start.1 = ((bf16[32,16,2048]{2,1,0:T(8,128)(2,1)}), bf16[32,16,2048]{2,1,0:T(8,128)(2,1)}, u32[]{:S(2)}, u32[]{:S(2)}) async-start(bf16[32,16,2048]{2,1,0:T(8,128)(2,1)} %bitcast.49), calls=%async_computation.1 | async-start | bytes 4194304 | tf_op jit(solution)/shard_map/all_to_all | solution.py:592
  36.7 17.3 %collective-permute-done.1.refs_4_ = bf16[768,512]{1,0:T(8,128)(2,1)S(1)} collective-permute-done((bf16[768,512]{1,0:T(8,128)(2,1)S(1)}, bf16[768,512]{1,0:T(8,128)(2,1)S(1)}, u32[]{:S(2)}, u32[]{:S(2)}) %collective-permute-start.1) | collective-permute-done | bytes 786464 | tf_op jit(solution)/shard_map/ppermute | solution.py:305
  59.0 3.6 %fetch.1 = (bf16[512,2048]{1,0:T(8,128)(2,1)S(1)}, bf16[2048,512]{1,0:T(8,128)(2,1)S(1)}, bf16[2048,512]{1,0:T(8,128)(2,1)S(1)}) custom-call(bf16[512,2048]{1,0:T(8,128)(2,1)} %bitcast.55, bf16[2048,512]{1,0:T(8,128)(2,1)} %bitcast.38, bf16[2048,512]{1,0:T(8,128)(2,1)} %bitcast.40), custom_call_target="tpu_custom_call" | custom-call | tf_op jit(solution)/shard_map/fetch/pallas_call | solution.py:120
  63.9 3.9 %expert_forward.3 = (bf16[512,512]{1,0:T(8,128)(2,1)}, f32[512,1024]{1,0:T(8,128)}) custom-call(bf16[512,2048]{1,0:T(8,128)(2,1)S(1)} %bitcast.36, bf16[2048,512]{1,0:T(8,128)(2,1)S(1)} %get-tuple-element.37.refs_7_.gate_ref.refs_3_, bf16[2048,512]{1,0:T(8,128)(2,1)S(1)} %get-tuple-element.38.refs_8_.up_ref.refs_4_), custom_call_target="tpu_custom_call" | custom-call | tf_op jit(solution)/shard_map/expert_forward/pallas_call | solution.py:151
  74.0 6.1 %expert_backward.3 = (bf16[512,1024]{1,0:T(8,128)(2,1)}, bf16[512,512]{1,0:T(8,128)(2,1)}, bf16[512,512]{1,0:T(8,128)(2,1)}, bf16[512,256]{1,0:T(8,128)(2,1)}, b...) custom-call(s32[1]{0:T(128)} %bitcast.3.rank_ref, bf16[512,2048]{1,0:T(8,128)(2,1)} %bitcast.12.refs_0_.refs_5_, ...), custom_call_target="tpu_custom_call" | custom-call | tf_op jit(solution)/shard_map/expert_backward/pallas_call | solution.py:221
  85.3 5.3 %expert_forward.2 = (bf16[768,512]{1,0:T(8,128)(2,1)}, f32[768,1024]{1,0:T(8,128)}) custom-call(bf16[768,2048]{1,0:T(8,128)(2,1)S(1)} %bitcast.34, bf16[2048,512]{1,0:T(8,128)(2,1)S(1)} %bitcast.39, bf16[2048,512]{1,0:T(8,128)(2,1)S(1)} %bitcast.41), custom_call_target="tpu_custom_call" | custom-call | tf_op jit(solution)/shard_map/expert_forward/pallas_call | solution.py:151
  92.5 7.7 %expert_backward.2 = (bf16[768,1024]{1,0:T(8,128)(2,1)}, bf16[768,512]{1,0:T(8,128)(2,1)}, bf16[768,512]{1,0:T(8,128)(2,1)}, bf16[768,256]{1,0:T(8,128)(2,1)}, b...) custom-call(s32[1]{0:T(128)} %bitcast.3.rank_ref, bf16[768,512]{1,0:T(8,128)(2,1)S(1)} %bitcast.45, ...), custom_call_target="tpu_custom_call" | custom-call | tf_op jit(solution)/shard_map/expert_backward/pallas_call | solution.py:221
  106.5 7.4 %collective-permute-done.10 = bf16[512,512]{1,0:T(8,128)(2,1)S(1)} collective-permute-done((bf16[512,512]{1,0:T(8,128)(2,1)S(1)}, bf16[512,512]{1,0:T(8,128)(2,1)S(1)}, u32[]{:S(2)}, u32[]{:S(2)}) %collective-permute-start.10) | collective-permute-done | bytes 524320 | tf_op jit(solution)/shard_map/ppermute | solution.py:316
  120.2 10.6 %collective-permute-done.6 = bf16[768,512]{1,0:T(8,128)(2,1)S(1)} collective-permute-done((bf16[768,512]{1,0:T(8,128)(2,1)}, bf16[768,512]{1,0:T(8,128)(2,1)S(1)}, u32[]{:S(2)}, u32[]{:S(2)}) %collective-permute-start.6) | collective-permute-done | bytes 786464 | tf_op jit(solution)/shard_map/ppermute | solution.py:316
  132.3 4.1 %collective-permute-done.11 = bf16[512,256]{1,0:T(8,128)(2,1)S(1)} collective-permute-done((bf16[512,256]{1,0:T(8,128)(2,1)S(1)}, bf16[512,256]{1,0:T(8,128)(2,1)S(1)}, u32[]{:S(2)}, u32[]{:S(2)}) %collective-permute-start.11) | collective-permute-done | bytes 262176 | tf_op jit(solution)/shard_map/ppermute | solution.py:321
  136.6 8.2 %collective-permute-done.7 = bf16[768,256]{1,0:T(8,128)(2,1)S(1)} collective-permute-done((bf16[768,256]{1,0:T(8,128)(2,1)S(1)}, bf16[768,256]{1,0:T(8,128)(2,1)S(1)}, u32[]{:S(2)}, u32[]{:S(2)}) %collective-permute-start.7) | collective-permute-done | bytes 393248 | tf_op jit(solution)/shard_map/ppermute | solution.py:321
  146.3 10.4 %all-to-all-start.2 = ((bf16[32,40,512]{2,1,0:T(8,128)(2,1)}), bf16[32,40,512]{2,1,0:T(8,128)(2,1)}, u32[]{:S(2)}, u32[]{:S(2)}) async-start(bf16[32,40,512]{2,1,0:T(8,128)(2,1)} %pad_maximum_fusion), calls=%async_computation.2 | async-start | bytes 2621440 | tf_op jit(solution)/shard_map/all_to_all | solution.py:642
  156.7 4.7 %multiply_convert_fusion = (bf16[384,512]{1,0:T(8,128)(2,1)S(1)}, bf16[384,512]{1,0:T(8,128)(2,1)}, f32[384,512]{1,0:T(8,128)}, f32[384,512]{1,0:T(8,128)}) fusion(bf16[384,512]{1,0:T(8,128)(2,1)} %branch_ref.1, f32[384,512]{1,0:T(8,128)} %param.27, bf16[384,512]{1,0:T(8,128)(2,1)} %param.24, f32[384,256]{1,0:T(8,128)} %fusion.13, f32[384,256]{1,0:T(8,128)} %fusion.17, ...), kind=kLoop, calls=%fused_computation.25 | loop fusion | flops 6881280 | bytes 6295040 | tf_op jit(solution)/shard_map/convert_element_type | solution.py:623
  163.6 8.2 %collective-permute-done.13.below = bf16[384,512]{1,0:T(8,128)(2,1)S(1)} collective-permute-done((bf16[384,512]{1,0:T(8,128)(2,1)S(1)}, bf16[384,512]{1,0:T(8,128)(2,1)S(1)}, u32[]{:S(2)}, u32[]{:S(2)}) %collective-permute-start.13) | collective-permute-done | bytes 393248 | tf_op jit(solution)/shard_map/ppermute | solution.py:305
  188.3 6.8 %all-to-all-start.3 = ((bf16[16,64,512]{2,1,0:T(8,128)(2,1)}), bf16[16,64,512]{2,1,0:T(8,128)(2,1)}, u32[]{:S(2)}, u32[]{:S(2)}) async-start(bf16[16,64,512]{2,1,0:T(8,128)(2,1)} %bitcast.52), calls=%async_computation.3 | async-start | bytes 2097152 | tf_op jit(solution)/shard_map/all_to_all | solution.py:657
  200.0 5.3 %collective-permute-done.18.z1 = bf16[384,512]{1,0:T(8,128)(2,1)S(1)} collective-permute-done((bf16[384,512]{1,0:T(8,128)(2,1)S(1)}, bf16[384,512]{1,0:T(8,128)(2,1)S(1)}, u32[]{:S(2)}, u32[]{:S(2)}) %collective-permute-start.18) | collective-permute-done | bytes 393248 | tf_op jit(solution)/shard_map/ppermute | solution.py:305
  212.6 5.7 %state_grads.1 = (bf16[384,512]{1,0:T(8,128)(2,1)}, f32[384,512]{1,0:T(8,128)}, f32[32,16,128]{2,1,0:T(8,128)}) custom-call(s32[1]{0:T(128)} %bitcast.3.rank_ref, bf16[384,512]{1,0:T(8,128)(2,1)S(1)} %copy-done.19, bf16[384,512]{1,0:T(8,128)(2,1)S(1)} %collective-permute-done.18.z1, bf16[384,512]{1,0:T(8,128)(2,1)S(1)} %collective-permute-done.19.z2, ...), custom_call_target="tpu_custom_call" | custom-call | tf_op jit(solution)/shard_map/state_grads/pallas_call | solution.py:409
  218.3 10.1 %all-to-all-start.4 = ((f32[32,16,128]{2,1,0:T(8,128)}), f32[32,16,128]{2,1,0:T(8,128)S(1)}, u32[]{:S(2)}, u32[]{:S(2)}) async-start(f32[32,16,128]{2,1,0:T(8,128)} %get-tuple-element.60), calls=%async_computation.4 | async-start | bytes 524288 | tf_op jit(solution)/shard_map/all_to_all | solution.py:679
  230.4 7.0 %collective-permute-start.17 = (f32[64,512]{1,0:T(8,128)}, f32[64,512]{1,0:T(8,128)}, u32[]{:S(2)}, u32[]{:S(2)}) collective-permute-start(f32[64,512]{1,0:T(8,128)} %convert_reduce_fusion), channel_id=1, source_target_pairs={{0,0},{1,32},{2,64},{3,96},{4,1},{5,33},{6,65},{7,97},{8,2},{9,34}... | collective-permute-start | bytes 393224 | tf_op jit(solution)/shard_map/ppermute | solution.py:665
  241.7 8.5 %gate_up_grads.1 = (bf16[2048,512]{1,0:T(8,128)(2,1)}, bf16[2048,512]{1,0:T(8,128)(2,1)}) custom-call(bf16[768,2048]{1,0:T(8,128)(2,1)S(1)} %bitcast.35, bf16[512,2048]{1,0:T(8,128)(2,1)S(1)} %bitcast.37, bf16[768,1024]{1,0:T(8,128)(2,1)S(1)} %copy-done.23, bf16[512,1024]{1,0:T(8,128)(2,1)S(1)} %copy-done.26), custom_call_target="tpu_custom_call" | custom-call | tf_op jit(solution)/shard_map/gate_up_grads/pallas_call | solution.py:259
  250.1 7.2 %down_grads.1 = bf16[512,2048]{1,0:T(8,128)(2,1)} custom-call(s32[1]{0:T(128)} %bitcast.3.rank_ref, bf16[768,512]{1,0:T(8,128)(2,1)} %get-tuple-element.44.first_act, bf16[512,512]{1,0:T(8,128)(2,1)} %get-tuple-element.45.second_act, bf16[768,512]{1,0:T(8,128)(2,1)} %bitcast.44, bf16[768,512]{1,0:T(8,128)(2,1)} %copy-done.16, ...), custom_call_target="tpu_custom_call" | custom-call | tf_op jit(solution)/shard_map/down_grads/pallas_call | solution.py:288
  257.3 6.9 %final_grads.1 = bf16[384,512]{1,0:T(8,128)(2,1)} custom-call(s32[1]{0:T(128)} %bitcast.16.me_ref, f32[32,16,128]{2,1,0:T(8,128)S(1)} %all-to-all-done.4.got_ref, f32[384,512]{1,0:T(8,128)} %get-tuple-element.61.state_ref, f32[384,512]{1,0:T(8,128)} %get-tuple-element.69.decay_ref, f32[384,512]{1,0:T(8,128)} %get-tuple-element.65.h_later, ...), custom_call_target="tpu_custom_call" | custom-call | tf_op jit(solution)/shard_map/final_grads/pallas_call | solution.py:527
  (187 shorter events, 84.2 us)
Async XLA Ops:
  7.2 22.3 %all-to-all-start = ((bf16[32,24,512]{2,1,0:T(8,128)(2,1)}), bf16[32,24,512]{2,1,0:T(8,128)(2,1)S(1)}, u32[]{:S(2)}, u32[]{:S(2)}) async-start(bf16[32,24,512]{2,1,0:T(8,128)(2,1)} %bitcast.53), calls=%async_computation | async-start | bytes 1572864 | tf_op jit(solution)/shard_map/all_to_all | solution.py:592
  29.5 39.7 %all-to-all-start.1 = ((bf16[32,16,2048]{2,1,0:T(8,128)(2,1)}), bf16[32,16,2048]{2,1,0:T(8,128)(2,1)}, u32[]{:S(2)}, u32[]{:S(2)}) async-start(bf16[32,16,2048]{2,1,0:T(8,128)(2,1)} %bitcast.49), calls=%async_computation.1 | async-start | bytes 4194304 | tf_op jit(solution)/shard_map/all_to_all | solution.py:592
  35.2 18.9 %collective-permute-start.1 = (bf16[768,512]{1,0:T(8,128)(2,1)S(1)}, bf16[768,512]{1,0:T(8,128)(2,1)S(1)}, u32[]{:S(2)}, u32[]{:S(2)}) collective-permute-start(bf16[768,512]{1,0:T(8,128)(2,1)S(1)} %bitcast.42), channel_id=1, source_target_pairs={{0,1},{1,2},{2,3},{3,0},{4,5},{5,6},{6,7},{7,4},{8,9},{9,10},{10,1... | collective-permute-start | bytes 2359304 | tf_op jit(solution)/shard_map/ppermute | solution.py:305
  36.2 19.6 %collective-permute-start = (bf16[768,512]{1,0:T(8,128)(2,1)S(1)}, bf16[768,512]{1,0:T(8,128)(2,1)S(1)}, u32[]{:S(2)}, u32[]{:S(2)}) collective-permute-start(bf16[768,512]{1,0:T(8,128)(2,1)S(1)} %bitcast.43), channel_id=1, source_target_pairs={{0,3},{1,0},{2,1},{3,2},{4,7},{5,4},{6,5},{7,6},{8,11},{9,8},{10,9... | collective-permute-start | bytes 2359304 | tf_op jit(solution)/shard_map/ppermute | solution.py:306
  54.9 35.6 %collective-permute-start.2 = (bf16[768,256]{1,0:T(8,128)(2,1)}, bf16[768,256]{1,0:T(8,128)(2,1)}, u32[]{:S(2)}, u32[]{:S(2)}) collective-permute-start(bf16[768,256]{1,0:T(8,128)(2,1)} %slice.96), channel_id=1, source_target_pairs={{0,1},{1,2},{2,3},{3,0},{4,5},{5,6},{6,7},{7,4},{8,9},{9,10},{10,1... | collective-permute-start | bytes 1179656 | tf_op jit(solution)/shard_map/ppermute | solution.py:308
  56.6 33.9 %collective-permute-start.3 = (bf16[768,256]{1,0:T(8,128)(2,1)}, bf16[768,256]{1,0:T(8,128)(2,1)}, u32[]{:S(2)}, u32[]{:S(2)}) collective-permute-start(bf16[768,256]{1,0:T(8,128)(2,1)} %slice.97), channel_id=1, source_target_pairs={{0,3},{1,0},{2,1},{3,2},{4,7},{5,4},{6,5},{7,6},{8,11},{9,8},{10,9... | collective-permute-start | bytes 1179656 | tf_op jit(solution)/shard_map/ppermute | solution.py:309
  80.1 24.6 %collective-permute-start.8 = (bf16[512,512]{1,0:T(8,128)(2,1)}, bf16[512,512]{1,0:T(8,128)(2,1)S(1)}, u32[]{:S(2)}, u32[]{:S(2)}) collective-permute-start(bf16[512,512]{1,0:T(8,128)(2,1)} %get-tuple-element.54), channel_id=1, source_target_pairs={{0,1},{1,2},{2,3},{3,0},{4,5},{5,6},{6,7},{7,4},{8,9},{9,10},{10,1... | collective-permute-start | bytes 1572872 | tf_op jit(solution)/shard_map/ppermute | solution.py:315
  100.3 17.7 %collective-permute-start.4 = (bf16[768,512]{1,0:T(8,128)(2,1)}, bf16[768,512]{1,0:T(8,128)(2,1)S(1)}, u32[]{:S(2)}, u32[]{:S(2)}) collective-permute-start(bf16[768,512]{1,0:T(8,128)(2,1)} %get-tuple-element.49), channel_id=1, source_target_pairs={{0,1},{1,2},{2,3},{3,0},{4,5},{5,6},{6,7},{7,4},{8,9},{9,10},{10,1... | collective-permute-start | bytes 2359304 | tf_op jit(solution)/shard_map/ppermute | solution.py:315
  102.8 11.1 %collective-permute-start.10 = (bf16[512,512]{1,0:T(8,128)(2,1)S(1)}, bf16[512,512]{1,0:T(8,128)(2,1)S(1)}, u32[]{:S(2)}, u32[]{:S(2)}) collective-permute-start(bf16[512,512]{1,0:T(8,128)(2,1)S(1)} %copy-done.53), channel_id=1, source_target_pairs={{0,3},{1,0},{2,1},{3,2},{4,7},{5,4},{6,5},{7,6},{8,11},{9,8},{10,9... | collective-permute-start | bytes 1572872 | tf_op jit(solution)/shard_map/ppermute | solution.py:316
  103.7 27.0 %collective-permute-start.6 = (bf16[768,512]{1,0:T(8,128)(2,1)}, bf16[768,512]{1,0:T(8,128)(2,1)S(1)}, u32[]{:S(2)}, u32[]{:S(2)}) collective-permute-start(bf16[768,512]{1,0:T(8,128)(2,1)} %get-tuple-element.51), channel_id=1, source_target_pairs={{0,3},{1,0},{2,1},{3,2},{4,7},{5,4},{6,5},{7,6},{8,11},{9,8},{10,9... | collective-permute-start | bytes 2359304 | tf_op jit(solution)/shard_map/ppermute | solution.py:316
  104.8 27.5 %collective-permute-start.9 = (bf16[512,256]{1,0:T(8,128)(2,1)S(1)}, bf16[512,256]{1,0:T(8,128)(2,1)S(1)}, u32[]{:S(2)}, u32[]{:S(2)}) collective-permute-start(bf16[512,256]{1,0:T(8,128)(2,1)S(1)} %add_convert_fusion.7), channel_id=1, source_target_pairs={{0,1},{1,2},{2,3},{3,0},{4,5},{5,6},{6,7},{7,4},{8,9},{9,10},{10,1... | collective-permute-start | bytes 786440 | tf_op jit(solution)/shard_map/ppermute | solution.py:320
  114.0 22.4 %collective-permute-start.11 = (bf16[512,256]{1,0:T(8,128)(2,1)S(1)}, bf16[512,256]{1,0:T(8,128)(2,1)S(1)}, u32[]{:S(2)}, u32[]{:S(2)}) collective-permute-start(bf16[512,256]{1,0:T(8,128)(2,1)S(1)} %add_convert_fusion.6), channel_id=1, source_target_pairs={{0,3},{1,0},{2,1},{3,2},{4,7},{5,4},{6,5},{7,6},{8,11},{9,8},{10,9... | collective-permute-start | bytes 786440 | tf_op jit(solution)/shard_map/ppermute | solution.py:321
  118.0 18.5 %collective-permute-start.5 = (bf16[768,256]{1,0:T(8,128)(2,1)S(1)}, bf16[768,256]{1,0:T(8,128)(2,1)S(1)}, u32[]{:S(2)}, u32[]{:S(2)}) collective-permute-start(bf16[768,256]{1,0:T(8,128)(2,1)S(1)} %add_convert_fusion.5), channel_id=1, source_target_pairs={{0,1},{1,2},{2,3},{3,0},{4,5},{5,6},{6,7},{7,4},{8,9},{9,10},{10,1... | collective-permute-start | bytes 1179656 | tf_op jit(solution)/shard_map/ppermute | solution.py:320
  130.9 13.9 %collective-permute-start.7 = (bf16[768,256]{1,0:T(8,128)(2,1)S(1)}, bf16[768,256]{1,0:T(8,128)(2,1)S(1)}, u32[]{:S(2)}, u32[]{:S(2)}) collective-permute-start(bf16[768,256]{1,0:T(8,128)(2,1)S(1)} %add_convert_fusion.4), channel_id=1, source_target_pairs={{0,3},{1,0},{2,1},{3,2},{4,7},{5,4},{6,5},{7,6},{8,11},{9,8},{10,9... | collective-permute-start | bytes 1179656 | tf_op jit(solution)/shard_map/ppermute | solution.py:321
  146.3 29.3 %all-to-all-start.2 = ((bf16[32,40,512]{2,1,0:T(8,128)(2,1)}), bf16[32,40,512]{2,1,0:T(8,128)(2,1)}, u32[]{:S(2)}, u32[]{:S(2)}) async-start(bf16[32,40,512]{2,1,0:T(8,128)(2,1)} %pad_maximum_fusion), calls=%async_computation.2 | async-start | bytes 2621440 | tf_op jit(solution)/shard_map/all_to_all | solution.py:642
  161.4 10.4 %collective-permute-start.13 = (bf16[384,512]{1,0:T(8,128)(2,1)S(1)}, bf16[384,512]{1,0:T(8,128)(2,1)S(1)}, u32[]{:S(2)}, u32[]{:S(2)}) collective-permute-start(bf16[384,512]{1,0:T(8,128)(2,1)S(1)} %get-tuple-element.62.own), channel_id=1, source_target_pairs={{0,1},{1,2},{2,3},{3,0},{4,5},{5,6},{6,7},{7,4},{8,9},{9,10},{10,1... | collective-permute-start | bytes 1179656 | tf_op jit(solution)/shard_map/ppermute | solution.py:305
  162.7 11.1 %collective-permute-start.12 = (bf16[384,512]{1,0:T(8,128)(2,1)S(1)}, bf16[384,512]{1,0:T(8,128)(2,1)S(1)}, u32[]{:S(2)}, u32[]{:S(2)}) collective-permute-start(bf16[384,512]{1,0:T(8,128)(2,1)S(1)} %get-tuple-element.62.own), channel_id=1, source_target_pairs={{0,3},{1,0},{2,1},{3,2},{4,7},{5,4},{6,5},{7,6},{8,11},{9,8},{10,9... | collective-permute-start | bytes 1179656 | tf_op jit(solution)/shard_map/ppermute | solution.py:306
  172.5 6.2 %collective-permute-start.14 = (bf16[384,256]{1,0:T(8,128)(2,1)}, bf16[384,256]{1,0:T(8,128)(2,1)}, u32[]{:S(2)}, u32[]{:S(2)}) collective-permute-start(bf16[384,256]{1,0:T(8,128)(2,1)} %slice.106), channel_id=1, source_target_pairs={{0,1},{1,2},{2,3},{3,0},{4,5},{5,6},{6,7},{7,4},{8,9},{9,10},{10,1... | collective-permute-start | bytes 589832 | tf_op jit(solution)/shard_map/ppermute | solution.py:308
  188.3 30.0 %all-to-all-start.3 = ((bf16[16,64,512]{2,1,0:T(8,128)(2,1)}), bf16[16,64,512]{2,1,0:T(8,128)(2,1)}, u32[]{:S(2)}, u32[]{:S(2)}) async-start(bf16[16,64,512]{2,1,0:T(8,128)(2,1)} %bitcast.52), calls=%async_computation.3 | async-start | bytes 2097152 | tf_op jit(solution)/shard_map/all_to_all | solution.py:657
  195.2 10.2 %collective-permute-start.18 = (bf16[384,512]{1,0:T(8,128)(2,1)S(1)}, bf16[384,512]{1,0:T(8,128)(2,1)S(1)}, u32[]{:S(2)}, u32[]{:S(2)}) collective-permute-start(bf16[384,512]{1,0:T(8,128)(2,1)S(1)} %copy-done.19), channel_id=1, source_target_pairs={{0,1},{1,2},{2,3},{3,0},{4,5},{5,6},{6,7},{7,4},{8,9},{9,10},{10,1... | collective-permute-start | bytes 1179656 | tf_op jit(solution)/shard_map/ppermute | solution.py:305
  197.8 9.9 %collective-permute-start.19 = (bf16[384,512]{1,0:T(8,128)(2,1)S(1)}, bf16[384,512]{1,0:T(8,128)(2,1)S(1)}, u32[]{:S(2)}, u32[]{:S(2)}) collective-permute-start(bf16[384,512]{1,0:T(8,128)(2,1)S(1)} %copy-done.19), channel_id=1, source_target_pairs={{0,3},{1,0},{2,1},{3,2},{4,7},{5,4},{6,5},{7,6},{8,11},{9,8},{10,9... | collective-permute-start | bytes 1179656 | tf_op jit(solution)/shard_map/ppermute | solution.py:306
  205.4 5.7 %collective-permute-start.20 = (bf16[384,256]{1,0:T(8,128)(2,1)S(1)}, bf16[384,256]{1,0:T(8,128)(2,1)S(1)}, u32[]{:S(2)}, u32[]{:S(2)}) collective-permute-start(bf16[384,256]{1,0:T(8,128)(2,1)S(1)} %slice.108), channel_id=1, source_target_pairs={{0,1},{1,2},{2,3},{3,0},{4,5},{5,6},{6,7},{7,4},{8,9},{9,10},{10,1... | collective-permute-start | bytes 589832 | tf_op jit(solution)/shard_map/ppermute | solution.py:308
  218.3 39.0 %all-to-all-start.4 = ((f32[32,16,128]{2,1,0:T(8,128)}), f32[32,16,128]{2,1,0:T(8,128)S(1)}, u32[]{:S(2)}, u32[]{:S(2)}) async-start(f32[32,16,128]{2,1,0:T(8,128)} %get-tuple-element.60), calls=%async_computation.4 | async-start | bytes 524288 | tf_op jit(solution)/shard_map/all_to_all | solution.py:679
  230.4 33.8 %collective-permute-start.17 = (f32[64,512]{1,0:T(8,128)}, f32[64,512]{1,0:T(8,128)}, u32[]{:S(2)}, u32[]{:S(2)}) collective-permute-start(f32[64,512]{1,0:T(8,128)} %convert_reduce_fusion), channel_id=1, source_target_pairs={{0,0},{1,32},{2,64},{3,96},{4,1},{5,33},{6,65},{7,97},{8,2},{9,34}... | collective-permute-start | bytes 393224 | tf_op jit(solution)/shard_map/ppermute | solution.py:665
  (59 other events, 400.1 us)

commit v3 on v2

--- a/solution.py
+++ b/solution.py
@@ -46,7 +46,7 @@
     return row
 
 
-def slots_kernel(idx_ref, idx_t_ref, col_ref, row_ref, *, experts):
+def slots_kernel(idx_ref, col_ref, *, experts):
     tokens, top = idx_ref.shape
     a, b = iota((tokens, tokens), 0), iota((tokens, tokens), 1)
     hot = [idx_ref[:, k : k + 1] == iota((tokens, experts), 1) for k in range(top)]
@@ -55,84 +55,103 @@
     for k in range(top):
         rank = jnp.sum(jnp.where(hot[k], before, 0.0), axis=1, keepdims=True).astype(jnp.int32)
         col_ref[:, k : k + 1] = idx_ref[:, k : k + 1] * sum(SLOT_GROUPS) + rank
-    hot = [idx_t_ref[k : k + 1, :] == iota((experts, tokens), 0) for k in range(top)]
-    both = sum(h.astype(F32) for h in hot).astype(BF)
-    before = jnp.dot(both, (a < b).astype(F32).astype(BF), preferred_element_type=F32)
-    for k in range(top):
-        rank = jnp.sum(jnp.where(hot[k], before, 0.0), axis=0, keepdims=True).astype(jnp.int32)
-        row_ref[k : k + 1, :] = placed_row(idx_t_ref[k : k + 1, :], rank, experts)
-
-
-def slot_rows(chosen, experts):
-    tokens, top = chosen.shape
+
+
+def slot_columns(chosen, experts):
     return pl.pallas_call(
         functools.partial(slots_kernel, experts=experts),
-        out_shape=(
-            jax.ShapeDtypeStruct((tokens, top), jnp.int32),
-            jax.ShapeDtypeStruct((top, tokens), jnp.int32),
-        ),
+        out_shape=jax.ShapeDtypeStruct(chosen.shape, jnp.int32),
         compiler_params=params(8),
         name="slots",
-    )(chosen, chosen.T)
-
-
-def dispatch_kernel(row_ref, weight_ref, cot_ref, out_ref, *, first):
+    )(chosen)
+
+
+def dispatch_kernel(idx_ref, weight_ref, cot_ref, out_ref, row_ref, *, first, experts):
     rows, tokens = out_ref.shape[0], cot_ref.shape[0]
+    top = idx_ref.shape[0]
+
+    @pl.when(pl.program_id(0) == 0)
+    def _():
+        a, b = iota((tokens, tokens), 0), iota((tokens, tokens), 1)
+        hot = [idx_ref[k : k + 1, :] == iota((experts, tokens), 0) for k in range(top)]
+        both = sum(h.astype(F32) for h in hot).astype(BF)
+        before = jnp.dot(both, (a < b).astype(F32).astype(BF), preferred_element_type=F32)
+        for k in range(top):
+            rank = jnp.sum(jnp.where(hot[k], before, 0.0), axis=0, keepdims=True)
+            row_ref[k : k + 1, :] = placed_row(
+                idx_ref[k : k + 1, :], rank.astype(jnp.int32), experts
+            )
+
     at = first + pl.program_id(0) * rows + iota((rows, tokens), 0)
     weight = jnp.zeros((rows, tokens), F32)
-    for k in range(row_ref.shape[0]):
+    for k in range(top):
         weight = jnp.where(row_ref[k : k + 1, :] == at, weight_ref[k : k + 1, :], weight)
     picked = jnp.dot((weight > 0.0).astype(F32).astype(BF), cot_ref[...], preferred_element_type=F32)
     out_ref[...] = (picked * jnp.sum(weight, axis=1, keepdims=True)).astype(BF)
 
 
-def dispatch(row, weight_t, cot, first, count):
+def dispatch(chosen_t, weight_t, cot, first, count, experts):
     _, width = cot.shape
     block = 256
     return pl.pallas_call(
-        functools.partial(dispatch_kernel, first=first),
+        functools.partial(dispatch_kernel, first=first, experts=experts),
         grid=(count // block,),
         in_specs=[
-            pl.BlockSpec(row.shape, lambda i: (0, 0)),
+            pl.BlockSpec(chosen_t.shape, lambda i: (0, 0)),
             pl.BlockSpec(weight_t.shape, lambda i: (0, 0)),
             pl.BlockSpec(cot.shape, lambda i: (0, 0)),
         ],
         out_specs=pl.BlockSpec((block, width), lambda i: (i, 0)),
         out_shape=hbm((count, width)),
+        scratch_shapes=[pltpu.VMEM(chosen_t.shape, jnp.int32)],
         compiler_params=params(10),
         name="dispatch",
-    )(row, weight_t, cot)
-
-
-def hold_kernel(*refs):
-    count = len(refs) // 2
-    sems = refs[-1]
-    copies = [
-        pltpu.make_async_copy(refs[i], refs[count + i], sems.at[i]) for i in range(count)
+    )(chosen_t, weight_t, cot)
+
+
+def weight_copies(rank, down, gate, up, down_to, cat_to, sems, n_tp, cat_only=False):
+    hidden, part = gate.shape[1], down.shape[1] // n_tp
+    copies = []
+    for m in range(n_tp):
+        at = pl.multiple_of(lax.rem(rank + m, n_tp) * part, part)
+        copies.append((down.at[:, pl.ds(at, part)], down_to.at[:, m * part : (m + 1) * part]))
+    copies.append((gate, cat_to.at[:, :hidden]))
+    copies.append((up, cat_to.at[:, hidden:]))
+    first = n_tp if cat_only else 0
+    return [
+        pltpu.make_async_copy(a, b, sems.at[first + i])
+        for i, (a, b) in enumerate(copies[first:])
     ]
+
+
+def fetch_kernel(rank_ref, down, gate, up, down_to, cat_to, sems, *, n_tp):
+    copies = weight_copies(rank_ref[0], down, gate, up, down_to, cat_to, sems, n_tp)
     for copy in copies:
         copy.start()
     for copy in copies:
         copy.wait()
 
 
-def held(*arrays):
-    return pl.pallas_call(
-        hold_kernel,
-        in_specs=[pl.BlockSpec(memory_space=pl.ANY)] * len(arrays),
-        out_specs=tuple([pl.BlockSpec(memory_space=pltpu.VMEM)] * len(arrays)),
-        out_shape=tuple(pltpu.VMEM(a.shape, a.dtype) for a in arrays),
-        scratch_shapes=[pltpu.SemaphoreType.DMA((len(arrays),))],
+def fetched_weights(rank, w_down, w_gate, w_up, n_tp):
+    width, hidden = w_gate.shape
+    return pl.pallas_call(
+        functools.partial(fetch_kernel, n_tp=n_tp),
+        in_specs=[pl.BlockSpec(memory_space=pltpu.SMEM)]
+        + [pl.BlockSpec(memory_space=pl.ANY)] * 3,
+        out_specs=(pl.BlockSpec(memory_space=pltpu.VMEM),) * 2,
+        out_shape=(pltpu.VMEM(w_down.shape, BF), pltpu.VMEM((width, 2 * hidden), BF)),
+        scratch_shapes=[pltpu.SemaphoreType.DMA((n_tp + 2,))],
         compiler_params=params(4),
         name="fetch",
-    )(*in_hbm(*arrays))
-
-
-def forward_kernel(x_ref, gate_ref, up_ref, act_ref, slope_ref):
+    )(rank, *in_hbm(w_down, w_gate, w_up))
+
+
+def forward_kernel(x_ref, *refs):
+    weights, (act_ref, slope_ref) = refs[:-2], refs[-2:]
     x = x_ref[...]
-    hidden = gate_ref.shape[1]
-    gate_pre = jnp.dot(x, gate_ref[...], preferred_element_type=F32)
-    up_pre = jnp.dot(x, up_ref[...], preferred_element_type=F32)
+    hidden = act_ref.shape[1]
+    pre = [jnp.dot(x, w[...], preferred_element_type=F32) for w in weights]
+    gate_pre, up_pre = pre if len(pre) == 2 else (pre[0][:, :hidden], pre[0][:, hidden:])
     glu = jnp.minimum(gate_pre, clamp_limit)
     lin = jnp.clip(up_pre, -clamp_limit, clamp_limit) + 1.0
     sig = 1.0 / (1.0 + jnp.exp(-glu_alpha * glu))
@@ -143,60 +162,65 @@
     slope_ref[:, hidden:] = jnp.where(jnp.abs(up_pre) < clamp_limit, silu, 0.0)
 
 
-def expert_forward(x, w_gate, w_up):
+def expert_forward(x, weights, hidden):
     rows, width = x.shape
-    hidden = w_gate.shape[1]
-    block = 256
+    block = 384 if rows % 384 == 0 else 256
     whole = pl.BlockSpec(memory_space=pltpu.VMEM)
     return pl.pallas_call(
         forward_kernel,
         grid=(rows // block,),
-        in_specs=[pl.BlockSpec((block, width), lambda i: (i, 0)), whole, whole],
+        in_specs=[pl.BlockSpec((block, width), lambda i: (i, 0))] + [whole] * len(weights),
         out_specs=(
             pl.BlockSpec((block, hidden), lambda i: (i, 0)),
             pl.BlockSpec((block, 2 * hidden), lambda i: (i, 0)),
         ),
         out_shape=(hbm((rows, hidden)), hbm((rows, 2 * hidden), F32)),
-        compiler_params=params(16),
+        compiler_params=params(24),
         name="expert_forward",
-    )(x, w_gate, w_up)
-
-
-def turned_columns(rank, ref_count, part, n_tp):
-    if ref_count == 1:
-        return [0]
-    start = lambda ahead: lax.rem(rank + ahead, n_tp) * part
-    half = part // 2
-    starts = [start(0), start(1), start(2), start(2) + half, start(3)]
-    return [pl.multiple_of(at, half) for at in starts]
-
-
-def backward_kernel(rank_ref, *refs, count, n_tp):
+    )(x, *weights)
+
+
+def backward_kernel(rank_ref, *refs, count, fetched, n_tp):
     got_refs, refs = refs[:count], refs[count:]
-    slope_ref, down_ref, gate_ref, up_ref = refs[:4]
-    both_ref, up1_ref, dn1_ref, up2_ref, dn2_ref, mine_ref = refs[4:]
+    slope_ref, refs = refs[0], refs[1:]
+    sources, refs = (refs[:3], refs[3:]) if fetched else ((), refs)
+    weights, refs = ((), refs) if fetched else (refs[:2], refs[2:])
+    both_ref, up1_ref, dn1_ref, up2_ref, dn2_ref, mine_ref = refs[:6]
+    first = pl.program_id(0) == 0
+    if fetched:
+        weights, sems = refs[6:8], refs[8]
+
+        @pl.when(first)
+        def _():
+            copies = weight_copies(0, *sources, *weights, sems, n_tp)
+            for copy in copies:
+                copy.start()
+            for copy in copies[:n_tp]:
+                copy.wait()
+
+    down_ref, cat_ref = weights
     width = mine_ref.shape[1]
     half = width // 2
     hidden = down_ref.shape[0]
-    d_act = None
-    for got_ref, at in zip(got_refs, turned_columns(rank_ref[0], count, width, n_tp)):
-        columns = down_ref[:, pl.ds(at, got_ref.shape[1])]
-        term = lax.dot_general(got_ref[...], columns, ROWS_ROWS, preferred_element_type=F32)
-        d_act = term if d_act is None else d_act + term
-    d_gate = (d_act * slope_ref[:, :hidden]).astype(BF)
-    d_up = (d_act * slope_ref[:, hidden:]).astype(BF)
-    both_ref[:, :hidden] = d_gate
-    both_ref[:, hidden:] = d_up
+    got = [ref[...] for ref in got_refs]
+    got = got[0] if len(got) == 1 else jnp.concatenate(got, axis=1)
+    d_act = lax.dot_general(got, down_ref[...], ROWS_ROWS, preferred_element_type=F32)
+    both_ref[:, :hidden] = (d_act * slope_ref[:, :hidden]).astype(BF)
+    both_ref[:, hidden:] = (d_act * slope_ref[:, hidden:]).astype(BF)
+    if fetched:
+
+        @pl.when(first)
+        def _():
+            for copy in weight_copies(0, *sources, *weights, sems, n_tp, True):
+                copy.wait()
+
+    both = both_ref[...]
 
     def term(ahead):
         at = pl.multiple_of(lax.rem(rank_ref[0] + ahead, n_tp) * width, width)
-        both = lax.dot_general(
-            d_gate, gate_ref[pl.ds(at, width), :], ROWS_ROWS, preferred_element_type=F32
-        )
-        both = both + lax.dot_general(
-            d_up, up_ref[pl.ds(at, width), :], ROWS_ROWS, preferred_element_type=F32
-        )
-        return both.astype(BF)
+        return lax.dot_general(
+            both, cat_ref[pl.ds(at, width), :], ROWS_ROWS, preferred_element_type=F32
+        ).astype(BF)
 
     away = term(2)
     up1_ref[:, :half] = away[:, :half]
@@ -210,30 +234,35 @@
     mine_ref[...] = term(0)
 
 
-def expert_backward(rank, gots, slope, w_down, w_gate, w_up, n_tp):
+def expert_backward(rank, gots, slope, weights, n_tp):
     rows = gots[0].shape[0]
-    hidden, width = w_down.shape
+    hidden, width = weights[0].shape
     part = width // n_tp
-    block = 256
+    fetched = len(weights) == 3
+    block = 384 if rows % 384 == 0 and not fetched else 256
     by_rows = lambda cols: pl.BlockSpec((block, cols), lambda i: (i, 0))
-    whole = pl.BlockSpec(memory_space=pltpu.VMEM)
+    whole = pl.BlockSpec(memory_space=pl.ANY if fetched else pltpu.VMEM)
+    scratch = [
+        pltpu.VMEM((hidden, width), BF),
+        pltpu.VMEM((width, 2 * hidden), BF),
+        pltpu.SemaphoreType.DMA((n_tp + 2,)),
+    ]
+    if fetched:
+        slope, *weights = in_hbm(slope, *weights)
     outs = (2 * hidden, part, part, part // 2, part // 2, part)
     return pl.pallas_call(
-        functools.partial(backward_kernel, count=len(gots), n_tp=n_tp),
+        functools.partial(backward_kernel, count=len(gots), fetched=fetched, n_tp=n_tp),
         grid=(rows // block,),
         in_specs=[pl.BlockSpec(memory_space=pltpu.SMEM)]
         + [by_rows(g.shape[1]) for g in gots]
-        + [
-            by_rows(2 * hidden),
-            whole,
-            whole,
-            whole,
-        ],
+        + [by_rows(2 * hidden)]
+        + [whole] * len(weights),
         out_specs=tuple(by_rows(c) for c in outs),
         out_shape=tuple(hbm((rows, c)) for c in outs),
-        compiler_params=params(16),
+        scratch_shapes=scratch if fetched else [],
+        compiler_params=params(24),
         name="expert_backward",
-    )(rank, *gots, slope, w_down, w_gate, w_up)
+    )(rank, *gots, slope, *weights)
 
 
 def summed_products(lefts, rights):
@@ -254,7 +283,7 @@
 
 def gate_up_grads(saved, both):
     width, hidden = saved[0].shape[1], both[0].shape[1] // 2
-    block = 256
+    block = 512
     out = pl.BlockSpec((block, hidden), lambda i: (i, 0))
     return pl.pallas_call(
         functools.partial(gate_up_kernel, groups=len(saved)),
@@ -263,34 +292,54 @@
         + [pl.BlockSpec(g.shape, lambda i: (0, 0)) for g in both],
         out_specs=(out, out),
         out_shape=(jax.ShapeDtypeStruct((width, hidden), BF),) * 2,
-        compiler_params=params(16),
+        compiler_params=params(32),
         name="gate_up_grads",
-    )(*saved, *both)
-
-
-def down_kernel(rank_ref, first_act, second_act, *refs, n_tp):
-    pieces, second, out_ref = refs[:-2], refs[-2], refs[-1]
+    )(*in_hbm(*saved, *both))
+
+
+def down_kernel(rank_ref, first_act, second_act, second, *refs, count, n_tp):
+    pieces, refs = refs[:count], refs[count:]
+    out_ref, act0, act1, rows0, rows1, turned0, turned1, sems = refs
     part = second.shape[1] // n_tp
-    for piece, at in zip(pieces, turned_columns(rank_ref[0], len(pieces), part, n_tp)):
-        columns = pl.ds(at, piece.shape[1])
-        total = lax.dot_general(first_act[...], piece[...], COLS_COLS, preferred_element_type=F32)
-        total = total + lax.dot_general(
-            second_act[...], second[:, columns], COLS_COLS, preferred_element_type=F32
-        )
+    half = part // 2
+    pairs = [(first_act, act0), (second_act, act1), (second, rows1)]
+    for i, piece in enumerate(pieces):
+        ahead, side = (0, 0) if i == 0 else ((i + 1) // 2, (i + 1) % 2)
+        at = lax.rem(rank_ref[0] + ahead, n_tp) * part + side * half
+        columns = pl.ds(pl.multiple_of(at, half), piece.shape[1])
+        pairs.append((piece, rows0.at[:, columns]))
+    copies = [pltpu.make_async_copy(a, b, sems.at[i]) for i, (a, b) in enumerate(pairs)]
+    for copy in copies:
+        copy.start()
+    for copy in copies[:2]:
+        copy.wait()
+    turned0[...] = act0[...].T
+    turned1[...] = act1[...].T
+    for copy in copies[2:]:
+        copy.wait()
+    for m in range(n_tp):
+        columns = slice(m * part, (m + 1) * part)
+        total = jnp.dot(turned0[...], rows0[:, columns], preferred_element_type=F32)
+        total = total + jnp.dot(turned1[...], rows1[:, columns], preferred_element_type=F32)
         out_ref[:, columns] = total.astype(BF)
 
 
 def down_grads(rank, acts, received, n_tp):
     pieces, (second,) = received
-    arrays = (*acts, *pieces, second)
-    whole = lambda *shape: pl.BlockSpec(shape, lambda i: (0, 0))
-    out = (acts[0].shape[1], second.shape[1])
-    return pl.pallas_call(
-        functools.partial(down_kernel, n_tp=n_tp),
+    arrays = (*acts, second, *pieces)
+    hidden, width = acts[0].shape[1], second.shape[1]
+    counts = [a.shape[0] for a in acts]
+    return pl.pallas_call(
+        functools.partial(down_kernel, count=len(pieces), n_tp=n_tp),
         grid=(1,),
-        in_specs=[pl.BlockSpec(memory_space=pltpu.SMEM)] + [whole(*a.shape) for a in arrays],
-        out_specs=whole(*out),
-        out_shape=hbm(out),
+        in_specs=[pl.BlockSpec(memory_space=pltpu.SMEM)]
+        + [pl.BlockSpec(memory_space=pl.ANY)] * len(arrays),
+        out_specs=pl.BlockSpec((hidden, width), lambda i: (0, 0)),
+        out_shape=hbm((hidden, width)),
+        scratch_shapes=[pltpu.VMEM((n, hidden), BF) for n in counts]
+        + [pltpu.VMEM((n, width), BF) for n in counts]
+        + [pltpu.VMEM((hidden, n), BF) for n in counts]
+        + [pltpu.SemaphoreType.DMA((len(arrays),))],
         compiler_params=params(32),
         name="down_grads",
     )(rank, *in_hbm(*arrays))
@@ -308,6 +357,19 @@
     left = lax.ppermute(left, "tp", ring(n_tp, 1))
     right = lax.ppermute(right, "tp", ring(n_tp, -1))
     return below, above, left, right
+
+
+def gathered_early(x, n_tp):
+    half = x.shape[1] // 2
+    left, right = x[:, :half], x[:, half:]
+    up, down = ring(n_tp, 1), ring(n_tp, -1)
+    below_left = lax.ppermute(left, "tp", up)
+    above_right = lax.ppermute(right, "tp", down)
+    below_right = lax.ppermute(right, "tp", up)
+    above_left = lax.ppermute(left, "tp", down)
+    away_left = lax.ppermute(below_left, "tp", up)
+    away_right = lax.ppermute(above_right, "tp", down)
+    return (x, above_left, above_right, away_left, away_right, below_left, below_right)
 
 
 def summed_over_tp(up1, dn1, up2, dn2, mine, n_tp):
@@ -476,21 +538,16 @@
     return ahead[: half // 2], behind[half // 2 :]
 
 
-def final_kernel(
-    me_ref,
-    got_ref,
-    state_ref,
-    decay_ref,
-    h_later,
-    h_earlier,
-    q_ref,
-    r_ref,
-    rec_w,
-    inp_w,
-    out_ref,
-    later_ref,
-    earlier_ref,
-):
+def final_kernel(me_ref, got_ref, *refs):
+    sources, out_ref = refs[:8], refs[8]
+    later_ref, earlier_ref = refs[9:11]
+    holds, sems = refs[11:19], refs[19]
+    copies = [pltpu.make_async_copy(a, b, sems.at[i]) for i, (a, b) in enumerate(zip(sources, holds))]
+    for copy in copies:
+        copy.start()
+    for copy in copies[:2]:
+        copy.wait()
+    state_ref, decay_ref, h_later, h_earlier, q_ref, r_ref, rec_w, inp_w = holds
     rows = state_ref.shape[0]
     ahead, behind = carried_in(me_ref[0], got_ref)
     spread = lambda v: jnp.concatenate([v[b : b + 1] for b in range(v.shape[0])], axis=1)
@@ -505,6 +562,8 @@
         return (later * decay_ref[pl.ds(t, 1), :], earlier * decay_ref[pl.ds(i, 1), :])
 
     lax.fori_loop(0, rows, step, (spread(ahead), spread(behind)), unroll=8)
+    for copy in copies[2:]:
+        copy.wait()
     later, earlier = later_ref[...], earlier_ref[...]
     total = later + earlier
     rec_pre = (later * h_later[...] + earlier * h_earlier[...]).astype(BF)
@@ -522,20 +581,23 @@
 
 def final_grads(me, got, arrays, rec_w, inp_w):
     tokens, channels = arrays[0].shape
-    rows = pl.BlockSpec((tokens, channels), lambda i: (0, 0))
-    fixed = lambda a: pl.BlockSpec(a.shape, lambda i: (0,) * a.ndim)
+    sources = (*arrays, rec_w, inp_w)
     return pl.pallas_call(
         final_kernel,
         grid=(1,),
-        in_specs=[pl.BlockSpec(memory_space=pltpu.SMEM), fixed(got)]
-        + [rows] * len(arrays)
-        + [fixed(rec_w), fixed(inp_w)],
-        out_specs=rows,
+        in_specs=[
+            pl.BlockSpec(memory_space=pltpu.SMEM),
+            pl.BlockSpec(got.shape, lambda i: (0, 0, 0)),
+        ]
+        + [pl.BlockSpec(memory_space=pl.ANY)] * len(sources),
+        out_specs=pl.BlockSpec((tokens, channels), lambda i: (0, 0)),
         out_shape=hbm((tokens, channels)),
-        scratch_shapes=[pltpu.VMEM((tokens, channels), F32)] * 2,
-        compiler_params=params(32),
+        scratch_shapes=[pltpu.VMEM((tokens, channels), F32)] * 2
+        + [pltpu.VMEM(a.shape, a.dtype) for a in sources]
+        + [pltpu.SemaphoreType.DMA((len(sources),))],
+        compiler_params=params(24),
         name="final_grads",
-    )(me, got, *in_hbm(*arrays, rec_w, inp_w))
+    )(me, got, *in_hbm(*sources))
 
 
 def blockwise(rows, weights):
@@ -573,6 +635,7 @@
     experts = n_sp * expert_gate_matrix.shape[0]
     capacity = expert_slot_tokens.shape[1] // n_sp
     slots = expert_slot_tokens.shape[1]
+    hidden = expert_gate_matrix.shape[2]
     part = model_width // n_tp
     rank = lax.axis_index("tp").astype(jnp.int32).reshape(1)
     place = lax.axis_index("sp").astype(jnp.int32).reshape(1)
@@ -581,30 +644,26 @@
         bounds.append((at, size))
         at += size
 
-    col, row = slot_rows(chosen_expert_index, experts)
-    weight_t = chosen_expert_weight.T
+    chosen_t, weight_t = chosen_expert_index.T, chosen_expert_weight.T
     cot_part = lax.dynamic_slice_in_dim(output_cotangent, rank[0] * part, part, 1)
     w_gate, w_up, w_down = expert_gate_matrix[0], expert_up_matrix[0], expert_down_matrix[0]
     received = []
     for g, (base, size) in enumerate(bounds):
         cot = output_cotangent if g else cot_part
-        out = dispatch(row, weight_t, cot, base * experts, size * experts)
+        out = dispatch(chosen_t, weight_t, cot, base * experts, size * experts, experts)
         got = lax.all_to_all(out.reshape(experts, size, -1), "sp", 0, 0, tiled=True)
         got = got.reshape(n_sp * size, -1)
         if g:
             received.append((got,))
         else:
-            below, above, left, right = gathered_over_tp(got, n_tp)
-            received.append((got, above, left, right, below))
-    w_down, w_gate_held, w_up_held = held(w_down, w_gate, w_up)
+            received.append(gathered_early(got, n_tp))
+    down_turned, w_cat = fetched_weights(rank, w_down, w_gate, w_up, n_tp)
 
     by_source = expert_slot_tokens.reshape(n_sp, capacity, model_width)
     saved, acts, slopes = [], [], []
     for g, (base, size) in enumerate(bounds):
         x = by_source[:, base : base + size].reshape(n_sp * size, model_width)
-        if g:
-            w_gate, w_up = w_gate_held, w_up_held
-        act, slope = expert_forward(x, w_gate, w_up)
+        act, slope = expert_forward(x, (w_cat,) if g else (w_gate, w_up), hidden)
         saved.append(x)
         acts.append(act)
         slopes.append(slope)
@@ -634,9 +693,8 @@
 
     boths, sums = [], []
     for g, (base, size) in enumerate(bounds):
-        both, *terms = expert_backward(
-            rank, received[g], slopes[g], w_down, w_gate, w_up, n_tp
-        )
+        weights = (w_down, w_gate, w_up) if g else (down_turned, w_cat)
+        both, *terms = expert_backward(rank, received[g], slopes[g], weights, n_tp)
         sums.append(summed_over_tp(*terms, n_tp).reshape(n_sp, size, part))
         boths.append(both)
     back = lax.all_to_all(jnp.concatenate(sums, axis=1), "sp", 0, 0, tiled=True)
@@ -646,6 +704,7 @@
     below, above, left, right = gathered_over_tp(gated, n_tp)
     gateds = (gated, above, left, right, below)
 
+    col = slot_columns(chosen_expert_index, experts)
     z0 = combine(col, cot_part, back.reshape(slots, part))
     zs = (z0, *gathered_over_tp(z0, n_tp))
 

time: 267 us -> 229 us (0.86)
  local copies, waits for them, and re-layouts: 29.3 us -> 10.1 us
  waiting for transfers between devices: 81.6 us -> 66.4 us
    unnamed x110 -> x74, local copies, waits for them, and re-layouts: 20.9 us -> 3.01 us
    ppermute x2, waiting for transfers between devices: 18 us -> 0.62 us  [summed_over_tp(): from_above = lax.ppermute(dn1, 'tp', ring(n_tp, -1))]
    ppermute x3 -> x2, waiting for transfers between devices: 30.9 us -> 14.5 us  [gathered_over_tp(): below = lax.ppermute(x, 'tp', ring(n_tp, 1))]
    ppermute x0 -> x6, waiting for transfers between devices: none -> 11.9 us  [the longest x1 7.46 us: gathered_early(): below_left = lax.ppermute(left, 'tp', up)]
    ppermute x2, waiting for transfers between devices: 0.01 us -> 9.42 us  [summed_over_tp(): left = lax.ppermute(up2, 'tp', ring(n_tp, 1))]
    ppermute x2, waiting for transfers between devices: 12.3 us -> 3.92 us  [summed_over_tp(): right = lax.ppermute(dn2, 'tp', ring(n_tp, -1))]
    ppermute x0 -> x6, starting transfers between devices: none -> 4.47 us  [the longest x1 1.21 us: gathered_early(): below_right = lax.ppermute(right, 'tp', up)]
    ppermute x2, waiting for transfers between devices: 3.59 us -> 7.4 us  [summed_over_tp(): from_below = lax.ppermute(up1, 'tp', ring(n_tp, 1))]
  transfers between devices with their start and end apart: 27 -> 29, of which waited for: 13 -> 16; matrix products, arithmetic and copies ran while one was open for 9% -> 8% of each run, Pallas kernels for 22% -> 26%
where the time goes in v3:
time: 229 us; the launch traced here: 228 us
  starting transfers between devices  71.8 us (31%)
  waiting for transfers between devices  66.4 us (29%)
  Pallas kernels  64.3 us (28%)
  other arithmetic  10.7 us (5%)
  local copies, waits for them, and re-layouts  10.1 us (4%)
  matrix products  3.37 us (1%)
    pallas_call x2, Pallas kernels, expert_backward(): pl.pallas_call(functools.partial(backward_kernel, count=len(gots), fetche...  15.6 us
    ppermute x2, waiting for transfers between devices, gathered_over_tp(): below = lax.ppermute(x, 'tp', ring(n_tp, 1))  14.5 us
    all_to_all x2, starting transfers between devices, shards(): got = lax.all_to_all(out.reshape(experts, size, -1), 'sp', 0, 0, tiled=True)  14.5 us
    all_to_all x2, waiting for transfers between devices, shards(): got = lax.all_to_all(out.reshape(experts, size, -1), 'sp', 0, 0, tiled=True)  10.7 us
    all_to_all x1, starting transfers between devices, shards(): back = lax.all_to_all(jnp.concatenate(sums, axis=1), 'sp', 0, 0, tiled=True)  10.3 us
    all_to_all x1, starting transfers between devices, shards(): carried = lax.all_to_all(carry, 'sp', 0, 0, tiled=True)  9.95 us
    ppermute x2, waiting for transfers between devices, summed_over_tp(): left = lax.ppermute(up2, 'tp', ring(n_tp, 1))  9.42 us
    pallas_call x1, Pallas kernels, gate_up_grads(): pl.pallas_call(functools.partial(gate_up_kernel, groups=len(saved)), grid...  9.24 us
  transfers between devices with their start and end apart: 29, of which 16 were waited for; matrix products, arithmetic and copies ran while one was open for 8% of the time, Pallas kernels for 26%

profile of v3, /device:TPU:13, one launch (start us, length us, event | category | flops | bytes accessed | tf_op | source)
XLA Modules:
  0.0 227.9 jit_solution(11984498599246240610)
XLA Ops:
  5.4 8.8 %all-to-all-start = ((bf16[32,24,512]{2,1,0:T(8,128)(2,1)}), bf16[32,24,512]{2,1,0:T(8,128)(2,1)S(1)}, u32[]{:S(2)}, u32[]{:S(2)}) async-start(bf16[32,24,512]{2,1,0:T(8,128)(2,1)} %bitcast.57), calls=%async_computation | async-start | bytes 1572864 | tf_op jit(solution)/shard_map/all_to_all | solution.py:654
  16.9 10.7 %all-to-all-done = bf16[32,24,512]{2,1,0:T(8,128)(2,1)S(1)} async-done(((bf16[32,24,512]{2,1,0:T(8,128)(2,1)}), bf16[32,24,512]{2,1,0:T(8,128)(2,1)S(1)}, u32[]{:S(2)}, u32[]{:S(2)}) %all-to-all-start) | async-done | bytes 786464 | tf_op jit(solution)/shard_map/all_to_all | solution.py:654
  27.7 5.7 %all-to-all-start.1 = ((bf16[32,16,2048]{2,1,0:T(8,128)(2,1)}), bf16[32,16,2048]{2,1,0:T(8,128)(2,1)}, u32[]{:S(2)}, u32[]{:S(2)}) async-start(bf16[32,16,2048]{2,1,0:T(8,128)(2,1)} %bitcast.54), calls=%async_computation.1 | async-start | bytes 4194304 | tf_op jit(solution)/shard_map/all_to_all | solution.py:654
  36.4 7.5 %collective-permute-done.2.refs_5_ = bf16[768,256]{1,0:T(8,128)(2,1)S(1)} collective-permute-done((bf16[768,256]{1,0:T(8,128)(2,1)S(1)}, bf16[768,256]{1,0:T(8,128)(2,1)S(1)}, u32[]{:S(2)}, u32[]{:S(2)}) %collective-permute-start.2) | collective-permute-done | bytes 393248 | tf_op jit(solution)/shard_map/ppermute | solution.py:366
  48.5 5.3 %expert_forward.2 = (bf16[768,512]{1,0:T(8,128)(2,1)}, f32[768,1024]{1,0:T(8,128)}) custom-call(bf16[768,2048]{1,0:T(8,128)(2,1)S(1)} %bitcast.34, bf16[2048,512]{1,0:T(8,128)(2,1)S(1)} %bitcast.38, bf16[2048,512]{1,0:T(8,128)(2,1)S(1)} %bitcast.41), custom_call_target="tpu_custom_call" | custom-call | tf_op jit(solution)/shard_map/expert_forward/pallas_call | solution.py:169
  53.8 3.1 %fetch.1 = (bf16[512,2048]{1,0:T(8,128)(2,1)S(1)}, bf16[2048,1024]{1,0:T(8,128)(2,1)S(1)}) custom-call(s32[1]{0:T(128)} %bitcast.3.rank_ref, bf16[512,2048]{1,0:T(8,128)(2,1)} %bitcast.52, bf16[2048,512]{1,0:T(8,128)(2,1)} %bitcast.36, bf16[2048,512]{1,0:T(8,128)(2,1)} %bitcast.39), custom_call_target="tpu_custom_call" | custom-call | tf_op jit(solution)/shard_map/fetch/pallas_call | solution.py:137
  57.0 3.8 %collective-permute-done.3.refs_3_ = bf16[768,256]{1,0:T(8,128)(2,1)S(1)} collective-permute-done((bf16[768,256]{1,0:T(8,128)(2,1)S(1)}, bf16[768,256]{1,0:T(8,128)(2,1)S(1)}, u32[]{:S(2)}, u32[]{:S(2)}) %collective-permute-start.3) | collective-permute-done | bytes 393248 | tf_op jit(solution)/shard_map/ppermute | solution.py:370
  61.4 6.6 %expert_backward.2 = (bf16[768,1024]{1,0:T(8,128)(2,1)}, bf16[768,512]{1,0:T(8,128)(2,1)}, bf16[768,512]{1,0:T(8,128)(2,1)}, bf16[768,256]{1,0:T(8,128)(2,1)}, b...) custom-call(s32[1]{0:T(128)} %bitcast.3.rank_ref, bf16[768,512]{1,0:T(8,128)(2,1)S(1)} %bitcast.46, ...), custom_call_target="tpu_custom_call" | custom-call | tf_op jit(solution)/shard_map/expert_backward/pallas_call | solution.py:253
  72.2 3.9 %expert_forward.3 = (bf16[512,512]{1,0:T(8,128)(2,1)}, f32[512,1024]{1,0:T(8,128)}) custom-call(bf16[512,2048]{1,0:T(8,128)(2,1)S(1)} %bitcast.42, bf16[2048,1024]{1,0:T(8,128)(2,1)S(1)} %get-tuple-element.33.refs_9_.refs_0_), custom_call_target="tpu_custom_call" | custom-call | tf_op jit(solution)/shard_map/expert_forward/pallas_call | solution.py:169
  77.1 9.0 %expert_backward.3 = (bf16[512,1024]{1,0:T(8,128)(2,1)}, bf16[512,512]{1,0:T(8,128)(2,1)}, bf16[512,512]{1,0:T(8,128)(2,1)}, bf16[512,256]{1,0:T(8,128)(2,1)}, b...) custom-call(s32[1]{0:T(128)} %bitcast.3.rank_ref, bf16[512,2048]{1,0:T(8,128)(2,1)} %bitcast.12.refs_0_.second, ...), custom_call_target="tpu_custom_call" | custom-call | tf_op jit(solution)/shard_map/expert_backward/pallas_call | solution.py:253
  90.6 7.4 %collective-permute-done.10 = bf16[512,512]{1,0:T(8,128)(2,1)S(1)} collective-permute-done((bf16[512,512]{1,0:T(8,128)(2,1)}, bf16[512,512]{1,0:T(8,128)(2,1)S(1)}, u32[]{:S(2)}, u32[]{:S(2)}) %collective-permute-start.10) | collective-permute-done | bytes 524320 | tf_op jit(solution)/shard_map/ppermute | solution.py:377
  100.3 6.1 %collective-permute-done.7 = bf16[768,256]{1,0:T(8,128)(2,1)S(1)} collective-permute-done((bf16[768,256]{1,0:T(8,128)(2,1)S(1)}, bf16[768,256]{1,0:T(8,128)(2,1)S(1)}, u32[]{:S(2)}, u32[]{:S(2)}) %collective-permute-start.7) | collective-permute-done | bytes 393248 | tf_op jit(solution)/shard_map/ppermute | solution.py:382
  108.7 3.3 %collective-permute-done.11 = bf16[512,256]{1,0:T(8,128)(2,1)S(1)} collective-permute-done((bf16[512,256]{1,0:T(8,128)(2,1)S(1)}, bf16[512,256]{1,0:T(8,128)(2,1)S(1)}, u32[]{:S(2)}, u32[]{:S(2)}) %collective-permute-start.11) | collective-permute-done | bytes 262176 | tf_op jit(solution)/shard_map/ppermute | solution.py:382
  115.3 10.3 %all-to-all-start.2 = ((bf16[32,40,512]{2,1,0:T(8,128)(2,1)}), bf16[32,40,512]{2,1,0:T(8,128)(2,1)S(1)}, u32[]{:S(2)}, u32[]{:S(2)}) async-start(bf16[32,40,512]{2,1,0:T(8,128)(2,1)} %pad_maximum_fusion), calls=%async_computation.2 | async-start | bytes 2621440 | tf_op jit(solution)/shard_map/all_to_all | solution.py:700
  125.7 4.4 %multiply_convert_fusion = (bf16[384,512]{1,0:T(8,128)(2,1)S(1)}, bf16[384,512]{1,0:T(8,128)(2,1)}, f32[384,512]{1,0:T(8,128)}, f32[384,512]{1,0:T(8,128)}) fusion(bf16[384,512]{1,0:T(8,128)(2,1)} %branch_ref.1, f32[384,512]{1,0:T(8,128)} %param.27, bf16[384,512]{1,0:T(8,128)(2,1)S(1)} %copy-done.17, f32[384,256]{1,0:T(8,128)} %fusion.13, ...), kind=kLoop, calls=%fused_computation.25 | loop fusion | flops 6881280 | bytes 6295040 | tf_op jit(solution)/shard_map/convert_element_type | solution.py:682
  132.7 8.1 %collective-permute-done.15.below = bf16[384,512]{1,0:T(8,128)(2,1)S(1)} collective-permute-done((bf16[384,512]{1,0:T(8,128)(2,1)S(1)}, bf16[384,512]{1,0:T(8,128)(2,1)S(1)}, u32[]{:S(2)}, u32[]{:S(2)}) %collective-permute-start.15) | collective-permute-done | bytes 393248 | tf_op jit(solution)/shard_map/ppermute | solution.py:354
  158.0 6.7 %all-to-all-start.3 = ((bf16[16,64,512]{2,1,0:T(8,128)(2,1)}), bf16[16,64,512]{2,1,0:T(8,128)(2,1)S(1)}, u32[]{:S(2)}, u32[]{:S(2)}) async-start(bf16[16,64,512]{2,1,0:T(8,128)(2,1)} %bitcast.24), calls=%async_computation.3 | async-start | bytes 2097152 | tf_op jit(solution)/shard_map/all_to_all | solution.py:716
  168.5 6.5 %collective-permute-done.20.z1 = bf16[384,512]{1,0:T(8,128)(2,1)S(1)} collective-permute-done((bf16[384,512]{1,0:T(8,128)(2,1)S(1)}, bf16[384,512]{1,0:T(8,128)(2,1)S(1)}, u32[]{:S(2)}, u32[]{:S(2)}) %collective-permute-start.20) | collective-permute-done | bytes 393248 | tf_op jit(solution)/shard_map/ppermute | solution.py:354
  182.1 5.7 %state_grads.1 = (bf16[384,512]{1,0:T(8,128)(2,1)}, f32[384,512]{1,0:T(8,128)}, f32[32,16,128]{2,1,0:T(8,128)}) custom-call(s32[1]{0:T(128)} %bitcast.3.rank_ref, bf16[384,512]{1,0:T(8,128)(2,1)S(1)} %combine.1.z_ref.z0, bf16[384,512]{1,0:T(8,128)(2,1)S(1)} %collective-permute-done.20.z1, bf16[384,512]{1,0:T(8,128)(2,1)S(1)} %collective-permute-done.21.z2, ...), custom_call_target="tpu_custom_call" | custom-call | tf_op jit(solution)/shard_map/state_grads/pallas_call | solution.py:471
  187.8 10.0 %all-to-all-start.4 = ((f32[32,16,128]{2,1,0:T(8,128)}), f32[32,16,128]{2,1,0:T(8,128)S(1)}, u32[]{:S(2)}, u32[]{:S(2)}) async-start(f32[32,16,128]{2,1,0:T(8,128)} %get-tuple-element.54), calls=%async_computation.4 | async-start | bytes 524288 | tf_op jit(solution)/shard_map/all_to_all | solution.py:738
  197.9 7.0 %collective-permute-start.19 = (f32[64,512]{1,0:T(8,128)S(1)}, f32[64,512]{1,0:T(8,128)S(1)}, u32[]{:S(2)}, u32[]{:S(2)}) collective-permute-start(f32[64,512]{1,0:T(8,128)S(1)} %convert_reduce_fusion), channel_id=1, source_target_pairs={{0,0},{1,32},{2,64},{3,96},{4,1},{5,33},{6,65},{7,97},{8,2},{9,34}... | collective-permute-start | bytes 393224 | tf_op jit(solution)/shard_map/ppermute | solution.py:724
  205.0 9.2 %gate_up_grads.1 = (bf16[2048,512]{1,0:T(8,128)(2,1)}, bf16[2048,512]{1,0:T(8,128)(2,1)}) custom-call(bf16[768,2048]{1,0:T(8,128)(2,1)} %bitcast.35, bf16[512,2048]{1,0:T(8,128)(2,1)} %bitcast.43, bf16[768,1024]{1,0:T(8,128)(2,1)} %get-tuple-element.34.refs_2_, bf16[512,1024]{1,0:T(8,128)(2,1)} %get-tuple-element.36.refs_3_), custom_call_target="tpu_custom_call" | custom-call | tf_op jit(solution)/shard_map/gate_up_grads/pallas_call | solution.py:288
  214.2 7.1 %down_grads.1 = bf16[512,2048]{1,0:T(8,128)(2,1)} custom-call(s32[1]{0:T(128)} %bitcast.3.rank_ref, bf16[768,512]{1,0:T(8,128)(2,1)} %get-tuple-element.39.first_act, bf16[512,512]{1,0:T(8,128)(2,1)} %get-tuple-element.40.second_act, bf16[512,2048]{1,0:T(8,128)(2,1)} %bitcast.12.refs_0_.second, bf16[768,512]{1,0:T(8,128)(2,1)} %bitcast.45, ...), custom_call_target="tpu_custom_call" | custom-call | tf_op jit(solution)/shard_map/down_grads/pallas_call | solution.py:332
  221.3 5.9 %final_grads.1 = bf16[384,512]{1,0:T(8,128)(2,1)} custom-call(s32[1]{0:T(128)} %bitcast.16.me_ref, f32[32,16,128]{2,1,0:T(8,128)S(1)} %all-to-all-done.4.got_ref, f32[384,512]{1,0:T(8,128)} %get-tuple-element.55.refs_0_, f32[384,512]{1,0:T(8,128)} %get-tuple-element.63.decay_ref.refs_1_, f32[384,512]{1,0:T(8,128)} %get-tuple-element.59.refs_2_, ...), custom_call_target="tpu_custom_call" | custom-call | tf_op jit(solution)/shard_map/final_grads/pallas_call | solution.py:585
  (153 shorter events, 64.7 us)
Async XLA Ops:
  5.4 22.3 %all-to-all-start = ((bf16[32,24,512]{2,1,0:T(8,128)(2,1)}), bf16[32,24,512]{2,1,0:T(8,128)(2,1)S(1)}, u32[]{:S(2)}, u32[]{:S(2)}) async-start(bf16[32,24,512]{2,1,0:T(8,128)(2,1)} %bitcast.57), calls=%async_computation | async-start | bytes 1572864 | tf_op jit(solution)/shard_map/all_to_all | solution.py:654
  27.7 49.5 %all-to-all-start.1 = ((bf16[32,16,2048]{2,1,0:T(8,128)(2,1)}), bf16[32,16,2048]{2,1,0:T(8,128)(2,1)}, u32[]{:S(2)}, u32[]{:S(2)}) async-start(bf16[32,16,2048]{2,1,0:T(8,128)(2,1)} %bitcast.54), calls=%async_computation.1 | async-start | bytes 4194304 | tf_op jit(solution)/shard_map/all_to_all | solution.py:654
  33.4 10.5 %collective-permute-start.2 = (bf16[768,256]{1,0:T(8,128)(2,1)S(1)}, bf16[768,256]{1,0:T(8,128)(2,1)S(1)}, u32[]{:S(2)}, u32[]{:S(2)}) collective-permute-start(bf16[768,256]{1,0:T(8,128)(2,1)S(1)} %get-tuple-element.66), channel_id=1, source_target_pairs={{0,1},{1,2},{2,3},{3,0},{4,5},{5,6},{6,7},{7,4},{8,9},{9,10},{10,1... | collective-permute-start | bytes 1179656 | tf_op jit(solution)/shard_map/ppermute | solution.py:366
  34.4 10.4 %collective-permute-start.1 = (bf16[768,256]{1,0:T(8,128)(2,1)S(1)}, bf16[768,256]{1,0:T(8,128)(2,1)S(1)}, u32[]{:S(2)}, u32[]{:S(2)}) collective-permute-start(bf16[768,256]{1,0:T(8,128)(2,1)S(1)} %get-tuple-element.65), channel_id=1, source_target_pairs={{0,3},{1,0},{2,1},{3,2},{4,7},{5,4},{6,5},{7,6},{8,11},{9,8},{10,9... | collective-permute-start | bytes 1179656 | tf_op jit(solution)/shard_map/ppermute | solution.py:367
  35.0 22.0 %collective-permute-start = (bf16[768,256]{1,0:T(8,128)(2,1)S(1)}, bf16[768,256]{1,0:T(8,128)(2,1)S(1)}, u32[]{:S(2)}, u32[]{:S(2)}) collective-permute-start(bf16[768,256]{1,0:T(8,128)(2,1)S(1)} %get-tuple-element.66), channel_id=1, source_target_pairs={{0,3},{1,0},{2,1},{3,2},{4,7},{5,4},{6,5},{7,6},{8,11},{9,8},{10,9... | collective-permute-start | bytes 1179656 | tf_op jit(solution)/shard_map/ppermute | solution.py:369
  35.2 21.7 %collective-permute-start.5 = (bf16[768,256]{1,0:T(8,128)(2,1)S(1)}, bf16[768,256]{1,0:T(8,128)(2,1)S(1)}, u32[]{:S(2)}, u32[]{:S(2)}) collective-permute-start(bf16[768,256]{1,0:T(8,128)(2,1)S(1)} %get-tuple-element.65), channel_id=1, source_target_pairs={{0,1},{1,2},{2,3},{3,0},{4,5},{5,6},{6,7},{7,4},{8,9},{9,10},{10,1... | collective-permute-start | bytes 1179656 | tf_op jit(solution)/shard_map/ppermute | solution.py:368
  43.9 16.9 %collective-permute-start.3 = (bf16[768,256]{1,0:T(8,128)(2,1)S(1)}, bf16[768,256]{1,0:T(8,128)(2,1)S(1)}, u32[]{:S(2)}, u32[]{:S(2)}) collective-permute-start(bf16[768,256]{1,0:T(8,128)(2,1)S(1)} %collective-permute-done.2.refs_5_), channel_id=1, source_target_pairs={{0,1},{1,2},{2,3},{3,0},{4,5},{5,6},{6,7},{7,4},{8,9},{9,10},{10,1... | collective-permute-start | bytes 1179656 | tf_op jit(solution)/shard_map/ppermute | solution.py:370
  44.8 16.6 %collective-permute-start.4 = (bf16[768,256]{1,0:T(8,128)(2,1)S(1)}, bf16[768,256]{1,0:T(8,128)(2,1)S(1)}, u32[]{:S(2)}, u32[]{:S(2)}) collective-permute-start(bf16[768,256]{1,0:T(8,128)(2,1)S(1)} %collective-permute-done.1.refs_2_), channel_id=1, source_target_pairs={{0,3},{1,0},{2,1},{3,2},{4,7},{5,4},{6,5},{7,6},{8,11},{9,8},{10,9... | collective-permute-start | bytes 1179656 | tf_op jit(solution)/shard_map/ppermute | solution.py:371
  68.0 20.7 %collective-permute-start.6 = (bf16[768,512]{1,0:T(8,128)(2,1)}, bf16[768,512]{1,0:T(8,128)(2,1)S(1)}, u32[]{:S(2)}, u32[]{:S(2)}) collective-permute-start(bf16[768,512]{1,0:T(8,128)(2,1)} %get-tuple-element.43), channel_id=1, source_target_pairs={{0,1},{1,2},{2,3},{3,0},{4,5},{5,6},{6,7},{7,4},{8,9},{9,10},{10,1... | collective-permute-start | bytes 2359304 | tf_op jit(solution)/shard_map/ppermute | solution.py:377
  69.6 20.6 %collective-permute-start.8 = (bf16[768,512]{1,0:T(8,128)(2,1)}, bf16[768,512]{1,0:T(8,128)(2,1)S(1)}, u32[]{:S(2)}, u32[]{:S(2)}) collective-permute-start(bf16[768,512]{1,0:T(8,128)(2,1)} %get-tuple-element.45), channel_id=1, source_target_pairs={{0,3},{1,0},{2,1},{3,2},{4,7},{5,4},{6,5},{7,6},{8,11},{9,8},{10,9... | collective-permute-start | bytes 2359304 | tf_op jit(solution)/shard_map/ppermute | solution.py:378
  86.2 11.8 %collective-permute-start.10 = (bf16[512,512]{1,0:T(8,128)(2,1)}, bf16[512,512]{1,0:T(8,128)(2,1)S(1)}, u32[]{:S(2)}, u32[]{:S(2)}) collective-permute-start(bf16[512,512]{1,0:T(8,128)(2,1)} %get-tuple-element.48), channel_id=1, source_target_pairs={{0,1},{1,2},{2,3},{3,0},{4,5},{5,6},{6,7},{7,4},{8,9},{9,10},{10,1... | collective-permute-start | bytes 1572872 | tf_op jit(solution)/shard_map/ppermute | solution.py:377
  88.5 11.4 %collective-permute-start.12 = (bf16[512,512]{1,0:T(8,128)(2,1)}, bf16[512,512]{1,0:T(8,128)(2,1)S(1)}, u32[]{:S(2)}, u32[]{:S(2)}) collective-permute-start(bf16[512,512]{1,0:T(8,128)(2,1)} %get-tuple-element.50), channel_id=1, source_target_pairs={{0,3},{1,0},{2,1},{3,2},{4,7},{5,4},{6,5},{7,6},{8,11},{9,8},{10,9... | collective-permute-start | bytes 1572872 | tf_op jit(solution)/shard_map/ppermute | solution.py:378
  88.8 17.6 %collective-permute-start.7 = (bf16[768,256]{1,0:T(8,128)(2,1)S(1)}, bf16[768,256]{1,0:T(8,128)(2,1)S(1)}, u32[]{:S(2)}, u32[]{:S(2)}) collective-permute-start(bf16[768,256]{1,0:T(8,128)(2,1)S(1)} %add_convert_fusion.5), channel_id=1, source_target_pairs={{0,1},{1,2},{2,3},{3,0},{4,5},{5,6},{6,7},{7,4},{8,9},{9,10},{10,1... | collective-permute-start | bytes 1179656 | tf_op jit(solution)/shard_map/ppermute | solution.py:382
  90.4 18.0 %collective-permute-start.9 = (bf16[768,256]{1,0:T(8,128)(2,1)S(1)}, bf16[768,256]{1,0:T(8,128)(2,1)S(1)}, u32[]{:S(2)}, u32[]{:S(2)}) collective-permute-start(bf16[768,256]{1,0:T(8,128)(2,1)S(1)} %add_convert_fusion.4), channel_id=1, source_target_pairs={{0,3},{1,0},{2,1},{3,2},{4,7},{5,4},{6,5},{7,6},{8,11},{9,8},{10,9... | collective-permute-start | bytes 1179656 | tf_op jit(solution)/shard_map/ppermute | solution.py:383
  98.0 14.0 %collective-permute-start.11 = (bf16[512,256]{1,0:T(8,128)(2,1)S(1)}, bf16[512,256]{1,0:T(8,128)(2,1)S(1)}, u32[]{:S(2)}, u32[]{:S(2)}) collective-permute-start(bf16[512,256]{1,0:T(8,128)(2,1)S(1)} %add_convert_fusion.7), channel_id=1, source_target_pairs={{0,1},{1,2},{2,3},{3,0},{4,5},{5,6},{6,7},{7,4},{8,9},{9,10},{10,1... | collective-permute-start | bytes 786440 | tf_op jit(solution)/shard_map/ppermute | solution.py:382
  100.0 14.0 %collective-permute-start.13 = (bf16[512,256]{1,0:T(8,128)(2,1)S(1)}, bf16[512,256]{1,0:T(8,128)(2,1)S(1)}, u32[]{:S(2)}, u32[]{:S(2)}) collective-permute-start(bf16[512,256]{1,0:T(8,128)(2,1)S(1)} %add_convert_fusion.6), channel_id=1, source_target_pairs={{0,3},{1,0},{2,1},{3,2},{4,7},{5,4},{6,5},{7,6},{8,11},{9,8},{10,9... | collective-permute-start | bytes 786440 | tf_op jit(solution)/shard_map/ppermute | solution.py:383
  115.3 29.7 %all-to-all-start.2 = ((bf16[32,40,512]{2,1,0:T(8,128)(2,1)}), bf16[32,40,512]{2,1,0:T(8,128)(2,1)S(1)}, u32[]{:S(2)}, u32[]{:S(2)}) async-start(bf16[32,40,512]{2,1,0:T(8,128)(2,1)} %pad_maximum_fusion), calls=%async_computation.2 | async-start | bytes 2621440 | tf_op jit(solution)/shard_map/all_to_all | solution.py:700
  130.0 10.8 %collective-permute-start.15 = (bf16[384,512]{1,0:T(8,128)(2,1)S(1)}, bf16[384,512]{1,0:T(8,128)(2,1)S(1)}, u32[]{:S(2)}, u32[]{:S(2)}) collective-permute-start(bf16[384,512]{1,0:T(8,128)(2,1)S(1)} %get-tuple-element.56.own), channel_id=1, source_target_pairs={{0,1},{1,2},{2,3},{3,0},{4,5},{5,6},{6,7},{7,4},{8,9},{9,10},{10,1... | collective-permute-start | bytes 1179656 | tf_op jit(solution)/shard_map/ppermute | solution.py:354
  132.7 11.0 %collective-permute-start.14 = (bf16[384,512]{1,0:T(8,128)(2,1)S(1)}, bf16[384,512]{1,0:T(8,128)(2,1)S(1)}, u32[]{:S(2)}, u32[]{:S(2)}) collective-permute-start(bf16[384,512]{1,0:T(8,128)(2,1)S(1)} %get-tuple-element.56.own), channel_id=1, source_target_pairs={{0,3},{1,0},{2,1},{3,2},{4,7},{5,4},{6,5},{7,6},{8,11},{9,8},{10,9... | collective-permute-start | bytes 1179656 | tf_op jit(solution)/shard_map/ppermute | solution.py:355
  158.0 29.8 %all-to-all-start.3 = ((bf16[16,64,512]{2,1,0:T(8,128)(2,1)}), bf16[16,64,512]{2,1,0:T(8,128)(2,1)S(1)}, u32[]{:S(2)}, u32[]{:S(2)}) async-start(bf16[16,64,512]{2,1,0:T(8,128)(2,1)} %bitcast.24), calls=%async_computation.3 | async-start | bytes 2097152 | tf_op jit(solution)/shard_map/all_to_all | solution.py:716
  164.7 10.3 %collective-permute-start.20 = (bf16[384,512]{1,0:T(8,128)(2,1)S(1)}, bf16[384,512]{1,0:T(8,128)(2,1)S(1)}, u32[]{:S(2)}, u32[]{:S(2)}) collective-permute-start(bf16[384,512]{1,0:T(8,128)(2,1)S(1)} %combine.1.z_ref.z0), channel_id=1, source_target_pairs={{0,1},{1,2},{2,3},{3,0},{4,5},{5,6},{6,7},{7,4},{8,9},{9,10},{10,1... | collective-permute-start | bytes 1179656 | tf_op jit(solution)/shard_map/ppermute | solution.py:354
  167.4 9.8 %collective-permute-start.21 = (bf16[384,512]{1,0:T(8,128)(2,1)S(1)}, bf16[384,512]{1,0:T(8,128)(2,1)S(1)}, u32[]{:S(2)}, u32[]{:S(2)}) collective-permute-start(bf16[384,512]{1,0:T(8,128)(2,1)S(1)} %combine.1.z_ref.z0), channel_id=1, source_target_pairs={{0,3},{1,0},{2,1},{3,2},{4,7},{5,4},{6,5},{7,6},{8,11},{9,8},{10,9... | collective-permute-start | bytes 1179656 | tf_op jit(solution)/shard_map/ppermute | solution.py:355
  187.8 33.5 %all-to-all-start.4 = ((f32[32,16,128]{2,1,0:T(8,128)}), f32[32,16,128]{2,1,0:T(8,128)S(1)}, u32[]{:S(2)}, u32[]{:S(2)}) async-start(f32[32,16,128]{2,1,0:T(8,128)} %get-tuple-element.54), calls=%async_computation.4 | async-start | bytes 524288 | tf_op jit(solution)/shard_map/all_to_all | solution.py:738
  197.9 29.3 %collective-permute-start.19 = (f32[64,512]{1,0:T(8,128)S(1)}, f32[64,512]{1,0:T(8,128)S(1)}, u32[]{:S(2)}, u32[]{:S(2)}) collective-permute-start(f32[64,512]{1,0:T(8,128)S(1)} %convert_reduce_fusion), channel_id=1, source_target_pairs={{0,0},{1,32},{2,64},{3,96},{4,1},{5,33},{6,65},{7,97},{8,2},{9,34}... | collective-permute-start | bytes 393224 | tf_op jit(solution)/shard_map/ppermute | solution.py:724
  (42 other events, 458.9 us)

commit v4 on v3

--- a/solution.py
+++ b/solution.py
@@ -66,7 +66,7 @@
     )(chosen)
 
 
-def dispatch_kernel(idx_ref, weight_ref, cot_ref, out_ref, row_ref, *, first, experts):
+def dispatch_kernel(_, idx_ref, weight_ref, cot_ref, out_ref, row_ref, *, first, experts):
     rows, tokens = out_ref.shape[0], cot_ref.shape[0]
     top = idx_ref.shape[0]
 
@@ -90,23 +90,25 @@
     out_ref[...] = (picked * jnp.sum(weight, axis=1, keepdims=True)).astype(BF)
 
 
-def dispatch(chosen_t, weight_t, cot, first, count, experts):
-    _, width = cot.shape
+def dispatch(column, chosen_t, weight_t, cot, width, first, count, experts):
     block = 256
     return pl.pallas_call(
         functools.partial(dispatch_kernel, first=first, experts=experts),
-        grid=(count // block,),
-        in_specs=[
-            pl.BlockSpec(chosen_t.shape, lambda i: (0, 0)),
-            pl.BlockSpec(weight_t.shape, lambda i: (0, 0)),
-            pl.BlockSpec(cot.shape, lambda i: (0, 0)),
-        ],
-        out_specs=pl.BlockSpec((block, width), lambda i: (i, 0)),
+        grid_spec=pltpu.PrefetchScalarGridSpec(
+            num_scalar_prefetch=1,
+            grid=(count // block,),
+            in_specs=[
+                pl.BlockSpec(chosen_t.shape, lambda i, c: (0, 0)),
+                pl.BlockSpec(weight_t.shape, lambda i, c: (0, 0)),
+                pl.BlockSpec((cot.shape[0], width), lambda i, c: (0, c[0])),
+            ],
+            out_specs=pl.BlockSpec((block, width), lambda i, c: (i, 0)),
+            scratch_shapes=[pltpu.VMEM(chosen_t.shape, jnp.int32)],
+        ),
         out_shape=hbm((count, width)),
-        scratch_shapes=[pltpu.VMEM(chosen_t.shape, jnp.int32)],
-        compiler_params=params(10),
+        compiler_params=params(12),
         name="dispatch",
-    )(chosen_t, weight_t, cot)
+    )(column, chosen_t, weight_t, cot)
 
 
 def weight_copies(rank, down, gate, up, down_to, cat_to, sems, n_tp, cat_only=False):
@@ -566,9 +568,10 @@
         copy.wait()
     later, earlier = later_ref[...], earlier_ref[...]
     total = later + earlier
-    rec_pre = (later * h_later[...] + earlier * h_earlier[...]).astype(BF)
-    inp_pre = (total * q_ref[...]).astype(BF)
-    direct = total * r_ref[...]
+    h_later, h_earlier = h_later[...].astype(F32), h_earlier[...].astype(F32)
+    rec_pre = (later * h_later + earlier * h_earlier).astype(BF)
+    inp_pre = (total * q_ref[...].astype(F32)).astype(BF)
+    direct = total * r_ref[...].astype(F32)
     size = rec_w.shape[1]
     for b in range(rec_w.shape[0]):
         cols = slice(b * size, (b + 1) * size)
@@ -645,12 +648,21 @@
         at += size
 
     chosen_t, weight_t = chosen_expert_index.T, chosen_expert_weight.T
-    cot_part = lax.dynamic_slice_in_dim(output_cotangent, rank[0] * part, part, 1)
     w_gate, w_up, w_down = expert_gate_matrix[0], expert_up_matrix[0], expert_down_matrix[0]
     received = []
     for g, (base, size) in enumerate(bounds):
-        cot = output_cotangent if g else cot_part
-        out = dispatch(chosen_t, weight_t, cot, base * experts, size * experts, experts)
+        width = model_width if g else part
+        column = jnp.zeros_like(rank) if g else rank
+        out = dispatch(
+            column,
+            chosen_t,
+            weight_t,
+            output_cotangent if g else in_hbm(output_cotangent)[0],
+            width,
+            base * experts,
+            size * experts,
+            experts,
+        )
         got = lax.all_to_all(out.reshape(experts, size, -1), "sp", 0, 0, tiled=True)
         got = got.reshape(n_sp * size, -1)
         if g:
@@ -686,10 +698,10 @@
     earlier_prod = jnp.exp(running - log_decay)
     rec_slope = rate * rec * (1.0 - rec)
     shared = inp * inputs * decay * decay / scale_in
-    h_later = (forward_scan_state * decay - shared) * rec_slope
-    h_earlier = (reverse_scan_state * decay - shared) * rec_slope
-    q = scale_in * inputs * inp * (1.0 - inp)
-    r = scale_in * inp
+    h_later = ((forward_scan_state * decay - shared) * rec_slope).astype(BF)
+    h_earlier = ((reverse_scan_state * decay - shared) * rec_slope).astype(BF)
+    q = (scale_in * inputs * inp * (1.0 - inp)).astype(BF)
+    r = (scale_in * inp).astype(BF)
 
     boths, sums = [], []
     for g, (base, size) in enumerate(bounds):
@@ -704,6 +716,7 @@
     below, above, left, right = gathered_over_tp(gated, n_tp)
     gateds = (gated, above, left, right, below)
 
+    cot_part = lax.dynamic_slice_in_dim(output_cotangent, rank[0] * part, part, 1)
     col = slot_columns(chosen_expert_index, experts)
     z0 = combine(col, cot_part, back.reshape(slots, part))
     zs = (z0, *gathered_over_tp(z0, n_tp))

time: 229 us -> 230 us (level)
  waiting for transfers between devices: 66.4 us -> 62.6 us
  local copies, waits for them, and re-layouts: 10.1 us -> 13.5 us
    mul x1 -> x0, other arithmetic: 2.94 us -> none  [shards(): xin = scale_in * inp * inputs]
    convert_element_type x0 -> x1, other arithmetic: none -> 2.73 us  [shards(): r = (scale_in * inp).astype(BF)]
    unnamed x74 -> x76, local copies, waits for them, and re-layouts: 3.01 us -> 5.55 us
  transfers between devices with their start and end apart: 29 -> 29, of which waited for: 16 -> 16; matrix products, arithmetic and copies ran while one was open for 8% -> 8% of each run, Pallas kernels for 26% -> 27%
where the time goes in v4:
time: 230 us; the launch traced here: 229 us
  starting transfers between devices  71.5 us (31%)
  Pallas kernels  66.4 us (29%)
  waiting for transfers between devices  62.6 us (27%)
  local copies, waits for them, and re-layouts  13.5 us (6%)
  other arithmetic  11.3 us (5%)
  matrix products  2.6 us (1%)
    pallas_call x2, Pallas kernels, expert_backward(): pl.pallas_call(functools.partial(backward_kernel, count=len(gots), fetche...  15.7 us
    ppermute x2, waiting for transfers between devices, gathered_over_tp(): below = lax.ppermute(x, 'tp', ring(n_tp, 1))  14.5 us
    all_to_all x2, starting transfers between devices, shards(): got = lax.all_to_all(out.reshape(experts, size, -1), 'sp', 0, 0, tiled=True)  14.5 us
    all_to_all x2, waiting for transfers between devices, shards(): got = lax.all_to_all(out.reshape(experts, size, -1), 'sp', 0, 0, tiled=True)  10.7 us
    all_to_all x1, starting transfers between devices, shards(): back = lax.all_to_all(jnp.concatenate(sums, axis=1), 'sp', 0, 0, tiled=True)  10.1 us
    all_to_all x1, starting transfers between devices, shards(): carried = lax.all_to_all(carry, 'sp', 0, 0, tiled=True)  9.95 us
    pallas_call x1, Pallas kernels, gate_up_grads(): pl.pallas_call(functools.partial(gate_up_kernel, groups=len(saved)), grid...  9.23 us
    pallas_call x2, Pallas kernels, expert_forward(): pl.pallas_call(forward_kernel, grid=(rows // block,), in_specs=[pl.BlockS...  9.21 us
  transfers between devices with their start and end apart: 29, of which 16 were waited for; matrix products, arithmetic and copies ran while one was open for 8% of the time, Pallas kernels for 27%

profile of v4, /device:TPU:13, one launch (start us, length us, event | category | flops | bytes accessed | tf_op | source)
XLA Modules:
  0.0 229.1 jit_solution(9194632563195988942)
XLA Ops:
  2.1 3.2 %dispatch.2 = bf16[768,512]{1,0:T(8,128)(2,1)} custom-call(s32[1]{0:T(128)} %bitcast.3._.rank_ref, s32[2,384]{1,0:T(2,128)S(1)} %bitcast.48, f32[2,384]{1,0:T(2,128)S(1)} %bitcast.50, bf16[384,2048]{1,0:T(8,128)(2,1)} %cot_ref.3), custom_call_target="tpu_custom_call" | custom-call | tf_op jit(solution)/shard_map/dispatch/pallas_call | solution.py:95
  5.4 8.8 %all-to-all-start = ((bf16[32,24,512]{2,1,0:T(8,128)(2,1)}), bf16[32,24,512]{2,1,0:T(8,128)(2,1)S(1)}, u32[]{:S(2)}, u32[]{:S(2)}) async-start(bf16[32,24,512]{2,1,0:T(8,128)(2,1)} %bitcast.58), calls=%async_computation | async-start | bytes 1572864 | tf_op jit(solution)/shard_map/all_to_all | solution.py:666
  16.9 10.7 %all-to-all-done = bf16[32,24,512]{2,1,0:T(8,128)(2,1)S(1)} async-done(((bf16[32,24,512]{2,1,0:T(8,128)(2,1)}), bf16[32,24,512]{2,1,0:T(8,128)(2,1)S(1)}, u32[]{:S(2)}, u32[]{:S(2)}) %all-to-all-start) | async-done | bytes 786464 | tf_op jit(solution)/shard_map/all_to_all | solution.py:666
  27.6 5.7 %all-to-all-start.1 = ((bf16[32,16,2048]{2,1,0:T(8,128)(2,1)}), bf16[32,16,2048]{2,1,0:T(8,128)(2,1)}, u32[]{:S(2)}, u32[]{:S(2)}) async-start(bf16[32,16,2048]{2,1,0:T(8,128)(2,1)} %bitcast.54), calls=%async_computation.1 | async-start | bytes 4194304 | tf_op jit(solution)/shard_map/all_to_all | solution.py:666
  36.4 7.5 %collective-permute-done.2.refs_5_ = bf16[768,256]{1,0:T(8,128)(2,1)S(1)} collective-permute-done((bf16[768,256]{1,0:T(8,128)(2,1)S(1)}, bf16[768,256]{1,0:T(8,128)(2,1)S(1)}, u32[]{:S(2)}, u32[]{:S(2)}) %collective-permute-start.2) | collective-permute-done | bytes 393248 | tf_op jit(solution)/shard_map/ppermute | solution.py:368
  47.7 4.1 %fetch.1 = (bf16[512,2048]{1,0:T(8,128)(2,1)S(1)}, bf16[2048,1024]{1,0:T(8,128)(2,1)S(1)}) custom-call(s32[1]{0:T(128)} %bitcast.3._.rank_ref, bf16[512,2048]{1,0:T(8,128)(2,1)} %bitcast.52, bf16[2048,512]{1,0:T(8,128)(2,1)} %bitcast.36, bf16[2048,512]{1,0:T(8,128)(2,1)} %bitcast.39), custom_call_target="tpu_custom_call" | custom-call | tf_op jit(solution)/shard_map/fetch/pallas_call | solution.py:139
  52.9 5.3 %expert_forward.2 = (bf16[768,512]{1,0:T(8,128)(2,1)}, f32[768,1024]{1,0:T(8,128)}) custom-call(bf16[768,2048]{1,0:T(8,128)(2,1)S(1)} %bitcast.34, bf16[2048,512]{1,0:T(8,128)(2,1)S(1)} %bitcast.38, bf16[2048,512]{1,0:T(8,128)(2,1)S(1)} %bitcast.41), custom_call_target="tpu_custom_call" | custom-call | tf_op jit(solution)/shard_map/expert_forward/pallas_call | solution.py:171
  63.4 6.5 %expert_backward.2 = (bf16[768,1024]{1,0:T(8,128)(2,1)}, bf16[768,512]{1,0:T(8,128)(2,1)}, bf16[768,512]{1,0:T(8,128)(2,1)}, bf16[768,256]{1,0:T(8,128)(2,1)}, b...) custom-call(s32[1]{0:T(128)} %bitcast.3._.rank_ref, bf16[768,512]{1,0:T(8,128)(2,1)S(1)} %bitcast.46, ...), custom_call_target="tpu_custom_call" | custom-call | tf_op jit(solution)/shard_map/expert_backward/pallas_call | solution.py:255
  74.2 3.9 %expert_forward.3 = (bf16[512,512]{1,0:T(8,128)(2,1)}, f32[512,1024]{1,0:T(8,128)}) custom-call(bf16[512,2048]{1,0:T(8,128)(2,1)S(1)} %bitcast.42, bf16[2048,1024]{1,0:T(8,128)(2,1)S(1)} %get-tuple-element.33.refs_9_.refs_0_), custom_call_target="tpu_custom_call" | custom-call | tf_op jit(solution)/shard_map/expert_forward/pallas_call | solution.py:171
  78.3 9.1 %expert_backward.3 = (bf16[512,1024]{1,0:T(8,128)(2,1)}, bf16[512,512]{1,0:T(8,128)(2,1)}, bf16[512,512]{1,0:T(8,128)(2,1)}, bf16[512,256]{1,0:T(8,128)(2,1)}, b...) custom-call(s32[1]{0:T(128)} %bitcast.3._.rank_ref, bf16[512,2048]{1,0:T(8,128)(2,1)} %bitcast.12.refs_0_.second, ...), custom_call_target="tpu_custom_call" | custom-call | tf_op jit(solution)/shard_map/expert_backward/pallas_call | solution.py:255
  94.0 5.3 %collective-permute-done.10 = bf16[512,512]{1,0:T(8,128)(2,1)S(1)} collective-permute-done((bf16[512,512]{1,0:T(8,128)(2,1)}, bf16[512,512]{1,0:T(8,128)(2,1)S(1)}, u32[]{:S(2)}, u32[]{:S(2)}) %collective-permute-start.10) | collective-permute-done | bytes 524320 | tf_op jit(solution)/shard_map/ppermute | solution.py:379
  101.7 6.0 %collective-permute-done.7 = bf16[768,256]{1,0:T(8,128)(2,1)S(1)} collective-permute-done((bf16[768,256]{1,0:T(8,128)(2,1)S(1)}, bf16[768,256]{1,0:T(8,128)(2,1)S(1)}, u32[]{:S(2)}, u32[]{:S(2)}) %collective-permute-start.7) | collective-permute-done | bytes 393248 | tf_op jit(solution)/shard_map/ppermute | solution.py:384
  110.3 3.0 %collective-permute-done.11 = bf16[512,256]{1,0:T(8,128)(2,1)S(1)} collective-permute-done((bf16[512,256]{1,0:T(8,128)(2,1)S(1)}, bf16[512,256]{1,0:T(8,128)(2,1)S(1)}, u32[]{:S(2)}, u32[]{:S(2)}) %collective-permute-start.11) | collective-permute-done | bytes 262176 | tf_op jit(solution)/shard_map/ppermute | solution.py:384
  116.9 10.1 %all-to-all-start.2 = ((bf16[32,40,512]{2,1,0:T(8,128)(2,1)}), bf16[32,40,512]{2,1,0:T(8,128)(2,1)S(1)}, u32[]{:S(2)}, u32[]{:S(2)}) async-start(bf16[32,40,512]{2,1,0:T(8,128)(2,1)} %pad_maximum_fusion), calls=%async_computation.2 | async-start | bytes 2621440 | tf_op jit(solution)/shard_map/all_to_all | solution.py:712
  127.1 4.1 %multiply_convert_fusion.2 = (bf16[384,512]{1,0:T(8,128)(2,1)S(1)}, bf16[384,512]{1,0:T(8,128)(2,1)}, bf16[384,512]{1,0:T(8,128)(2,1)}, bf16[384,512]{1,0:T(8,128)(2,1)}) fusion(bf16[384,512]{1,0:T(8,128)(2,1)} %branch_ref.1, f32[384,512]{1,0:T(8,128)} %param.27, bf16[384,512]{1,0:T(8,128)(2,1)S(1)} %copy-done.17, f32[384,256]{1,0:T(8,128)S(1)} %fusion.14, ...), kind=kLoop, calls=%fused_computation.26 | loop fusion | flops 7274496 | bytes 5508608 | tf_op jit(solution)/shard_map/convert_element_type | solution.py:694
  133.9 8.1 %collective-permute-done.15.below = bf16[384,512]{1,0:T(8,128)(2,1)S(1)} collective-permute-done((bf16[384,512]{1,0:T(8,128)(2,1)S(1)}, bf16[384,512]{1,0:T(8,128)(2,1)S(1)}, u32[]{:S(2)}, u32[]{:S(2)}) %collective-permute-start.15) | collective-permute-done | bytes 393248 | tf_op jit(solution)/shard_map/ppermute | solution.py:356
  159.2 6.7 %all-to-all-start.3 = ((bf16[16,64,512]{2,1,0:T(8,128)(2,1)}), bf16[16,64,512]{2,1,0:T(8,128)(2,1)S(1)}, u32[]{:S(2)}, u32[]{:S(2)}) async-start(bf16[16,64,512]{2,1,0:T(8,128)(2,1)} %bitcast.57), calls=%async_computation.3 | async-start | bytes 2097152 | tf_op jit(solution)/shard_map/all_to_all | solution.py:729
  169.8 6.5 %collective-permute-done.20.z1 = bf16[384,512]{1,0:T(8,128)(2,1)S(1)} collective-permute-done((bf16[384,512]{1,0:T(8,128)(2,1)S(1)}, bf16[384,512]{1,0:T(8,128)(2,1)S(1)}, u32[]{:S(2)}, u32[]{:S(2)}) %collective-permute-start.20) | collective-permute-done | bytes 393248 | tf_op jit(solution)/shard_map/ppermute | solution.py:356
  183.4 5.7 %state_grads.1 = (bf16[384,512]{1,0:T(8,128)(2,1)}, f32[384,512]{1,0:T(8,128)}, f32[32,16,128]{2,1,0:T(8,128)}) custom-call(s32[1]{0:T(128)} %bitcast.3._.rank_ref, bf16[384,512]{1,0:T(8,128)(2,1)S(1)} %combine.1.z_ref.z0, bf16[384,512]{1,0:T(8,128)(2,1)S(1)} %collective-permute-done.20.z1, bf16[384,512]{1,0:T(8,128)(2,1)S(1)} %collective-permute-done.21.z2, ...), custom_call_target="tpu_custom_call" | custom-call | tf_op jit(solution)/shard_map/state_grads/pallas_call | solution.py:473
  189.1 10.0 %all-to-all-start.4 = ((f32[32,16,128]{2,1,0:T(8,128)}), f32[32,16,128]{2,1,0:T(8,128)S(1)}, u32[]{:S(2)}, u32[]{:S(2)}) async-start(f32[32,16,128]{2,1,0:T(8,128)} %get-tuple-element.54), calls=%async_computation.4 | async-start | bytes 524288 | tf_op jit(solution)/shard_map/all_to_all | solution.py:751
  199.2 7.0 %collective-permute-start.19 = (f32[64,512]{1,0:T(8,128)S(1)}, f32[64,512]{1,0:T(8,128)S(1)}, u32[]{:S(2)}, u32[]{:S(2)}) collective-permute-start(f32[64,512]{1,0:T(8,128)S(1)} %convert_reduce_fusion), channel_id=1, source_target_pairs={{0,0},{1,32},{2,64},{3,96},{4,1},{5,33},{6,65},{7,97},{8,2},{9,34}... | collective-permute-start | bytes 393224 | tf_op jit(solution)/shard_map/ppermute | solution.py:737
  206.2 9.2 %gate_up_grads.1 = (bf16[2048,512]{1,0:T(8,128)(2,1)}, bf16[2048,512]{1,0:T(8,128)(2,1)}) custom-call(bf16[768,2048]{1,0:T(8,128)(2,1)} %bitcast.35, bf16[512,2048]{1,0:T(8,128)(2,1)} %bitcast.43, bf16[768,1024]{1,0:T(8,128)(2,1)} %get-tuple-element.34.refs_2_, bf16[512,1024]{1,0:T(8,128)(2,1)} %get-tuple-element.36.refs_3_), custom_call_target="tpu_custom_call" | custom-call | tf_op jit(solution)/shard_map/gate_up_grads/pallas_call | solution.py:290
  215.4 7.1 %down_grads.1 = bf16[512,2048]{1,0:T(8,128)(2,1)} custom-call(s32[1]{0:T(128)} %bitcast.3._.rank_ref, bf16[768,512]{1,0:T(8,128)(2,1)} %get-tuple-element.39.first_act, bf16[512,512]{1,0:T(8,128)(2,1)} %get-tuple-element.40.second_act, bf16[512,2048]{1,0:T(8,128)(2,1)} %bitcast.12.refs_0_.second, bf16[768,512]{1,0:T(8,128)(2,1)} %bitcast.45, ...), custom_call_target="tpu_custom_call" | custom-call | tf_op jit(solution)/shard_map/down_grads/pallas_call | solution.py:334
  222.6 5.9 %final_grads.1 = bf16[384,512]{1,0:T(8,128)(2,1)} custom-call(s32[1]{0:T(128)} %bitcast.16.me_ref, f32[32,16,128]{2,1,0:T(8,128)S(1)} %all-to-all-done.4.got_ref, f32[384,512]{1,0:T(8,128)} %get-tuple-element.55.refs_0_, f32[384,512]{1,0:T(8,128)} %get-tuple-element.63.decay_ref.refs_1_, bf16[384,512]{1,0:T(8,128)(2,1)} %get-tuple-element.59.refs_2_, ...), custom_call_target="tpu_custom_call" | custom-call | tf_op jit(solution)/shard_map/final_grads/pallas_call | solution.py:588
  (155 shorter events, 68.4 us)
Async XLA Ops:
  5.4 22.3 %all-to-all-start = ((bf16[32,24,512]{2,1,0:T(8,128)(2,1)}), bf16[32,24,512]{2,1,0:T(8,128)(2,1)S(1)}, u32[]{:S(2)}, u32[]{:S(2)}) async-start(bf16[32,24,512]{2,1,0:T(8,128)(2,1)} %bitcast.58), calls=%async_computation | async-start | bytes 1572864 | tf_op jit(solution)/shard_map/all_to_all | solution.py:666
  27.6 50.7 %all-to-all-start.1 = ((bf16[32,16,2048]{2,1,0:T(8,128)(2,1)}), bf16[32,16,2048]{2,1,0:T(8,128)(2,1)}, u32[]{:S(2)}, u32[]{:S(2)}) async-start(bf16[32,16,2048]{2,1,0:T(8,128)(2,1)} %bitcast.54), calls=%async_computation.1 | async-start | bytes 4194304 | tf_op jit(solution)/shard_map/all_to_all | solution.py:666
  33.4 10.5 %collective-permute-start.2 = (bf16[768,256]{1,0:T(8,128)(2,1)S(1)}, bf16[768,256]{1,0:T(8,128)(2,1)S(1)}, u32[]{:S(2)}, u32[]{:S(2)}) collective-permute-start(bf16[768,256]{1,0:T(8,128)(2,1)S(1)} %get-tuple-element.66), channel_id=1, source_target_pairs={{0,1},{1,2},{2,3},{3,0},{4,5},{5,6},{6,7},{7,4},{8,9},{9,10},{10,1... | collective-permute-start | bytes 1179656 | tf_op jit(solution)/shard_map/ppermute | solution.py:368
  34.4 10.4 %collective-permute-start.1 = (bf16[768,256]{1,0:T(8,128)(2,1)S(1)}, bf16[768,256]{1,0:T(8,128)(2,1)S(1)}, u32[]{:S(2)}, u32[]{:S(2)}) collective-permute-start(bf16[768,256]{1,0:T(8,128)(2,1)S(1)} %get-tuple-element.65), channel_id=1, source_target_pairs={{0,3},{1,0},{2,1},{3,2},{4,7},{5,4},{6,5},{7,6},{8,11},{9,8},{10,9... | collective-permute-start | bytes 1179656 | tf_op jit(solution)/shard_map/ppermute | solution.py:369
  34.9 23.3 %collective-permute-start = (bf16[768,256]{1,0:T(8,128)(2,1)S(1)}, bf16[768,256]{1,0:T(8,128)(2,1)S(1)}, u32[]{:S(2)}, u32[]{:S(2)}) collective-permute-start(bf16[768,256]{1,0:T(8,128)(2,1)S(1)} %get-tuple-element.66), channel_id=1, source_target_pairs={{0,3},{1,0},{2,1},{3,2},{4,7},{5,4},{6,5},{7,6},{8,11},{9,8},{10,9... | collective-permute-start | bytes 1179656 | tf_op jit(solution)/shard_map/ppermute | solution.py:371
  35.2 23.0 %collective-permute-start.5 = (bf16[768,256]{1,0:T(8,128)(2,1)S(1)}, bf16[768,256]{1,0:T(8,128)(2,1)S(1)}, u32[]{:S(2)}, u32[]{:S(2)}) collective-permute-start(bf16[768,256]{1,0:T(8,128)(2,1)S(1)} %get-tuple-element.65), channel_id=1, source_target_pairs={{0,1},{1,2},{2,3},{3,0},{4,5},{5,6},{6,7},{7,4},{8,9},{9,10},{10,1... | collective-permute-start | bytes 1179656 | tf_op jit(solution)/shard_map/ppermute | solution.py:370
  43.9 16.9 %collective-permute-start.3 = (bf16[768,256]{1,0:T(8,128)(2,1)S(1)}, bf16[768,256]{1,0:T(8,128)(2,1)S(1)}, u32[]{:S(2)}, u32[]{:S(2)}) collective-permute-start(bf16[768,256]{1,0:T(8,128)(2,1)S(1)} %collective-permute-done.2.refs_5_), channel_id=1, source_target_pairs={{0,1},{1,2},{2,3},{3,0},{4,5},{5,6},{6,7},{7,4},{8,9},{9,10},{10,1... | collective-permute-start | bytes 1179656 | tf_op jit(solution)/shard_map/ppermute | solution.py:372
  44.8 16.6 %collective-permute-start.4 = (bf16[768,256]{1,0:T(8,128)(2,1)S(1)}, bf16[768,256]{1,0:T(8,128)(2,1)S(1)}, u32[]{:S(2)}, u32[]{:S(2)}) collective-permute-start(bf16[768,256]{1,0:T(8,128)(2,1)S(1)} %collective-permute-done.1.refs_2_), channel_id=1, source_target_pairs={{0,3},{1,0},{2,1},{3,2},{4,7},{5,4},{6,5},{7,6},{8,11},{9,8},{10,9... | collective-permute-start | bytes 1179656 | tf_op jit(solution)/shard_map/ppermute | solution.py:373
  69.9 20.0 %collective-permute-start.6 = (bf16[768,512]{1,0:T(8,128)(2,1)}, bf16[768,512]{1,0:T(8,128)(2,1)S(1)}, u32[]{:S(2)}, u32[]{:S(2)}) collective-permute-start(bf16[768,512]{1,0:T(8,128)(2,1)} %get-tuple-element.43), channel_id=1, source_target_pairs={{0,1},{1,2},{2,3},{3,0},{4,5},{5,6},{6,7},{7,4},{8,9},{9,10},{10,1... | collective-permute-start | bytes 2359304 | tf_op jit(solution)/shard_map/ppermute | solution.py:379
  71.5 20.1 %collective-permute-start.8 = (bf16[768,512]{1,0:T(8,128)(2,1)}, bf16[768,512]{1,0:T(8,128)(2,1)}, u32[]{:S(2)}, u32[]{:S(2)}) collective-permute-start(bf16[768,512]{1,0:T(8,128)(2,1)} %get-tuple-element.45), channel_id=1, source_target_pairs={{0,3},{1,0},{2,1},{3,2},{4,7},{5,4},{6,5},{7,6},{8,11},{9,8},{10,9... | collective-permute-start | bytes 2359304 | tf_op jit(solution)/shard_map/ppermute | solution.py:380
  87.5 11.8 %collective-permute-start.10 = (bf16[512,512]{1,0:T(8,128)(2,1)}, bf16[512,512]{1,0:T(8,128)(2,1)S(1)}, u32[]{:S(2)}, u32[]{:S(2)}) collective-permute-start(bf16[512,512]{1,0:T(8,128)(2,1)} %get-tuple-element.48), channel_id=1, source_target_pairs={{0,1},{1,2},{2,3},{3,0},{4,5},{5,6},{6,7},{7,4},{8,9},{9,10},{10,1... | collective-permute-start | bytes 1572872 | tf_op jit(solution)/shard_map/ppermute | solution.py:379
  89.8 11.7 %collective-permute-start.12 = (bf16[512,512]{1,0:T(8,128)(2,1)}, bf16[512,512]{1,0:T(8,128)(2,1)S(1)}, u32[]{:S(2)}, u32[]{:S(2)}) collective-permute-start(bf16[512,512]{1,0:T(8,128)(2,1)} %get-tuple-element.50), channel_id=1, source_target_pairs={{0,3},{1,0},{2,1},{3,2},{4,7},{5,4},{6,5},{7,6},{8,11},{9,8},{10,9... | collective-permute-start | bytes 1572872 | tf_op jit(solution)/shard_map/ppermute | solution.py:380
  90.1 17.6 %collective-permute-start.7 = (bf16[768,256]{1,0:T(8,128)(2,1)S(1)}, bf16[768,256]{1,0:T(8,128)(2,1)S(1)}, u32[]{:S(2)}, u32[]{:S(2)}) collective-permute-start(bf16[768,256]{1,0:T(8,128)(2,1)S(1)} %add_convert_fusion.5), channel_id=1, source_target_pairs={{0,1},{1,2},{2,3},{3,0},{4,5},{5,6},{6,7},{7,4},{8,9},{9,10},{10,1... | collective-permute-start | bytes 1179656 | tf_op jit(solution)/shard_map/ppermute | solution.py:384
  92.8 17.1 %collective-permute-start.9 = (bf16[768,256]{1,0:T(8,128)(2,1)S(1)}, bf16[768,256]{1,0:T(8,128)(2,1)S(1)}, u32[]{:S(2)}, u32[]{:S(2)}) collective-permute-start(bf16[768,256]{1,0:T(8,128)(2,1)S(1)} %add_convert_fusion.4), channel_id=1, source_target_pairs={{0,3},{1,0},{2,1},{3,2},{4,7},{5,4},{6,5},{7,6},{8,11},{9,8},{10,9... | collective-permute-start | bytes 1179656 | tf_op jit(solution)/shard_map/ppermute | solution.py:385
  99.3 14.0 %collective-permute-start.11 = (bf16[512,256]{1,0:T(8,128)(2,1)S(1)}, bf16[512,256]{1,0:T(8,128)(2,1)S(1)}, u32[]{:S(2)}, u32[]{:S(2)}) collective-permute-start(bf16[512,256]{1,0:T(8,128)(2,1)S(1)} %add_convert_fusion.7), channel_id=1, source_target_pairs={{0,1},{1,2},{2,3},{3,0},{4,5},{5,6},{6,7},{7,4},{8,9},{9,10},{10,1... | collective-permute-start | bytes 786440 | tf_op jit(solution)/shard_map/ppermute | solution.py:384
  101.6 14.0 %collective-permute-start.13 = (bf16[512,256]{1,0:T(8,128)(2,1)S(1)}, bf16[512,256]{1,0:T(8,128)(2,1)S(1)}, u32[]{:S(2)}, u32[]{:S(2)}) collective-permute-start(bf16[512,256]{1,0:T(8,128)(2,1)S(1)} %add_convert_fusion.6), channel_id=1, source_target_pairs={{0,3},{1,0},{2,1},{3,2},{4,7},{5,4},{6,5},{7,6},{8,11},{9,8},{10,9... | collective-permute-start | bytes 786440 | tf_op jit(solution)/shard_map/ppermute | solution.py:385
  116.9 30.4 %all-to-all-start.2 = ((bf16[32,40,512]{2,1,0:T(8,128)(2,1)}), bf16[32,40,512]{2,1,0:T(8,128)(2,1)S(1)}, u32[]{:S(2)}, u32[]{:S(2)}) async-start(bf16[32,40,512]{2,1,0:T(8,128)(2,1)} %pad_maximum_fusion), calls=%async_computation.2 | async-start | bytes 2621440 | tf_op jit(solution)/shard_map/all_to_all | solution.py:712
  131.2 10.8 %collective-permute-start.15 = (bf16[384,512]{1,0:T(8,128)(2,1)S(1)}, bf16[384,512]{1,0:T(8,128)(2,1)S(1)}, u32[]{:S(2)}, u32[]{:S(2)}) collective-permute-start(bf16[384,512]{1,0:T(8,128)(2,1)S(1)} %get-tuple-element.56.own), channel_id=1, source_target_pairs={{0,1},{1,2},{2,3},{3,0},{4,5},{5,6},{6,7},{7,4},{8,9},{9,10},{10,1... | collective-permute-start | bytes 1179656 | tf_op jit(solution)/shard_map/ppermute | solution.py:356
  133.9 11.0 %collective-permute-start.14 = (bf16[384,512]{1,0:T(8,128)(2,1)S(1)}, bf16[384,512]{1,0:T(8,128)(2,1)S(1)}, u32[]{:S(2)}, u32[]{:S(2)}) collective-permute-start(bf16[384,512]{1,0:T(8,128)(2,1)S(1)} %get-tuple-element.56.own), channel_id=1, source_target_pairs={{0,3},{1,0},{2,1},{3,2},{4,7},{5,4},{6,5},{7,6},{8,11},{9,8},{10,9... | collective-permute-start | bytes 1179656 | tf_op jit(solution)/shard_map/ppermute | solution.py:357
  159.2 29.8 %all-to-all-start.3 = ((bf16[16,64,512]{2,1,0:T(8,128)(2,1)}), bf16[16,64,512]{2,1,0:T(8,128)(2,1)S(1)}, u32[]{:S(2)}, u32[]{:S(2)}) async-start(bf16[16,64,512]{2,1,0:T(8,128)(2,1)} %bitcast.57), calls=%async_computation.3 | async-start | bytes 2097152 | tf_op jit(solution)/shard_map/all_to_all | solution.py:729
  165.9 10.3 %collective-permute-start.20 = (bf16[384,512]{1,0:T(8,128)(2,1)S(1)}, bf16[384,512]{1,0:T(8,128)(2,1)S(1)}, u32[]{:S(2)}, u32[]{:S(2)}) collective-permute-start(bf16[384,512]{1,0:T(8,128)(2,1)S(1)} %combine.1.z_ref.z0), channel_id=1, source_target_pairs={{0,1},{1,2},{2,3},{3,0},{4,5},{5,6},{6,7},{7,4},{8,9},{9,10},{10,1... | collective-permute-start | bytes 1179656 | tf_op jit(solution)/shard_map/ppermute | solution.py:356
  168.7 9.8 %collective-permute-start.21 = (bf16[384,512]{1,0:T(8,128)(2,1)S(1)}, bf16[384,512]{1,0:T(8,128)(2,1)S(1)}, u32[]{:S(2)}, u32[]{:S(2)}) collective-permute-start(bf16[384,512]{1,0:T(8,128)(2,1)S(1)} %combine.1.z_ref.z0), channel_id=1, source_target_pairs={{0,3},{1,0},{2,1},{3,2},{4,7},{5,4},{6,5},{7,6},{8,11},{9,8},{10,9... | collective-permute-start | bytes 1179656 | tf_op jit(solution)/shard_map/ppermute | solution.py:357
  189.1 33.5 %all-to-all-start.4 = ((f32[32,16,128]{2,1,0:T(8,128)}), f32[32,16,128]{2,1,0:T(8,128)S(1)}, u32[]{:S(2)}, u32[]{:S(2)}) async-start(f32[32,16,128]{2,1,0:T(8,128)} %get-tuple-element.54), calls=%async_computation.4 | async-start | bytes 524288 | tf_op jit(solution)/shard_map/all_to_all | solution.py:751
  199.2 29.3 %collective-permute-start.19 = (f32[64,512]{1,0:T(8,128)S(1)}, f32[64,512]{1,0:T(8,128)S(1)}, u32[]{:S(2)}, u32[]{:S(2)}) collective-permute-start(f32[64,512]{1,0:T(8,128)S(1)} %convert_reduce_fusion), channel_id=1, source_target_pairs={{0,0},{1,32},{2,64},{3,96},{4,1},{5,33},{6,65},{7,97},{8,2},{9,34}... | collective-permute-start | bytes 393224 | tf_op jit(solution)/shard_map/ppermute | solution.py:737
  (43 other events, 510.1 us)

commit v5 on v4

--- a/solution.py
+++ b/solution.py
@@ -416,34 +416,20 @@
     return [(pl.multiple_of(lax.rem(me + a, n_tp) * width, width), z) for a, z in order]
 
 
-def state_kernel(
-    rank_ref,
-    z0,
-    z1,
-    z2,
-    z3,
-    z4,
-    w_hbm,
-    mixed_ref,
-    branch_ref,
-    decay_ref,
-    later_ref,
-    earlier_ref,
-    branch_grad_ref,
-    state_ref,
-    carry_ref,
-    w_ref,
-    sem,
-    *,
-    n_tp,
-):
-    copy = pltpu.make_async_copy(w_hbm, w_ref, sem)
-    copy.start()
-    copy.wait()
+def state_kernel(rank_ref, z0, z1, z2, z3, z4, *refs, n_tp):
+    sources, (branch_grad_ref, state_ref, carry_ref) = refs[:6], refs[6:9]
+    holds, sems = refs[9:15], refs[15]
+    copies = [pltpu.make_async_copy(a, b, sems.at[i]) for i, (a, b) in enumerate(zip(sources, holds))]
+    for copy in copies:
+        copy.start()
+    copies[0].wait()
+    w_ref, mixed_ref, branch_ref, decay_ref, later_ref, earlier_ref = holds
     total = None
     for at, z in pieces_of(rank_ref, (z0, z1, z2, z3, z4), n_tp):
         term = jnp.dot(z, w_ref[pl.ds(at, z.shape[1]), :], preferred_element_type=F32)
         total = term if total is None else total + term
+    for copy in copies[1:]:
+        copy.wait()
     branch_grad_ref[...] = (total * mixed_ref[...].astype(F32)).astype(BF)
     state = total * branch_ref[...].astype(F32)
     state_ref[...] = state
@@ -470,19 +456,20 @@
     full = lambda *shape: pl.BlockSpec(shape, lambda i: (0,) * len(shape))
     held = full(tokens, channels)
     carry = (n_sp, 16, channels // 4)
+    sources = (w_out, mixed, branch, decay, later_prod, earlier_prod)
     return pl.pallas_call(
         functools.partial(state_kernel, n_tp=n_tp),
         grid=(1,),
         in_specs=[pl.BlockSpec(memory_space=pltpu.SMEM)]
         + [full(*z.shape) for z in zs]
-        + [pl.BlockSpec(memory_space=pl.ANY)]
-        + [held] * 5,
+        + [pl.BlockSpec(memory_space=pl.ANY)] * len(sources),
         out_specs=(held, held, full(*carry)),
         out_shape=(hbm((tokens, channels)), hbm((tokens, channels), F32), hbm(carry, F32)),
-        scratch_shapes=[pltpu.VMEM(w_out.shape, BF), pltpu.SemaphoreType.DMA(())],
+        scratch_shapes=[pltpu.VMEM(a.shape, a.dtype) for a in sources]
+        + [pltpu.SemaphoreType.DMA((len(sources),))],
         compiler_params=params(32),
         name="state_grads",
-    )(rank, *zs, *in_hbm(w_out, mixed, branch, decay, later_prod, earlier_prod))
+    )(rank, *zs, *in_hbm(*sources))
 
 
 def proj_kernel(rank_ref, core_ref, z_ref, own, above, left, right, below, keep_ref, send_ref, *, n_tp, size):
@@ -540,16 +527,16 @@
     return ahead[: half // 2], behind[half // 2 :]
 
 
-def final_kernel(me_ref, got_ref, *refs):
-    sources, out_ref = refs[:8], refs[8]
-    later_ref, earlier_ref = refs[9:11]
-    holds, sems = refs[11:19], refs[19]
+def final_kernel(me_ref, *refs):
+    sources, out_ref = refs[:9], refs[9]
+    later_ref, earlier_ref = refs[10:12]
+    holds, sems = refs[12:21], refs[21]
     copies = [pltpu.make_async_copy(a, b, sems.at[i]) for i, (a, b) in enumerate(zip(sources, holds))]
     for copy in copies:
         copy.start()
-    for copy in copies[:2]:
+    for copy in copies[:3]:
         copy.wait()
-    state_ref, decay_ref, h_later, h_earlier, q_ref, r_ref, rec_w, inp_w = holds
+    got_ref, state_ref, decay_ref, h_later, h_earlier, q_ref, r_ref, rec_w, inp_w = holds
     rows = state_ref.shape[0]
     ahead, behind = carried_in(me_ref[0], got_ref)
     spread = lambda v: jnp.concatenate([v[b : b + 1] for b in range(v.shape[0])], axis=1)
@@ -564,7 +551,7 @@
         return (later * decay_ref[pl.ds(t, 1), :], earlier * decay_ref[pl.ds(i, 1), :])
 
     lax.fori_loop(0, rows, step, (spread(ahead), spread(behind)), unroll=8)
-    for copy in copies[2:]:
+    for copy in copies[3:]:
         copy.wait()
     later, earlier = later_ref[...], earlier_ref[...]
     total = later + earlier
@@ -584,14 +571,11 @@
 
 def final_grads(me, got, arrays, rec_w, inp_w):
     tokens, channels = arrays[0].shape
-    sources = (*arrays, rec_w, inp_w)
+    sources = (got, *arrays, rec_w, inp_w)
     return pl.pallas_call(
         final_kernel,
         grid=(1,),
-        in_specs=[
-            pl.BlockSpec(memory_space=pltpu.SMEM),
-            pl.BlockSpec(got.shape, lambda i: (0, 0, 0)),
-        ]
+        in_specs=[pl.BlockSpec(memory_space=pltpu.SMEM)]
         + [pl.BlockSpec(memory_space=pl.ANY)] * len(sources),
         out_specs=pl.BlockSpec((tokens, channels), lambda i: (0, 0)),
         out_shape=hbm((tokens, channels)),
@@ -600,7 +584,7 @@
         + [pltpu.SemaphoreType.DMA((len(sources),))],
         compiler_params=params(24),
         name="final_grads",
-    )(me, got, *in_hbm(*sources))
+    )(me, *in_hbm(*sources))
 
 
 def blockwise(rows, weights):

time: 230 us -> 229 us (level)
    unnamed x76 -> x78, local copies, waits for them, and re-layouts: 5.55 us -> 6.25 us
  transfers between devices with their start and end apart: 29 -> 29, of which waited for: 16 -> 16; matrix products, arithmetic and copies ran while one was open for 8% -> 8% of each run, Pallas kernels for 27% -> 26%
where the time goes in v5:
time: 229 us; the launch traced here: 228 us
  starting transfers between devices  71.5 us (31%)
  Pallas kernels  64.7 us (28%)
  waiting for transfers between devices  62.6 us (27%)
  local copies, waits for them, and re-layouts  14.2 us (6%)
  other arithmetic  11.3 us (5%)
  matrix products  2.6 us (1%)
    pallas_call x2, Pallas kernels, expert_backward(): pl.pallas_call(functools.partial(backward_kernel, count=len(gots), fetche...  15.6 us
    ppermute x2, waiting for transfers between devices, gathered_over_tp(): below = lax.ppermute(x, 'tp', ring(n_tp, 1))  14.5 us
    all_to_all x2, starting transfers between devices, shards(): got = lax.all_to_all(out.reshape(experts, size, -1), 'sp', 0, 0, tiled=True)  14.5 us
    all_to_all x2, waiting for transfers between devices, shards(): got = lax.all_to_all(out.reshape(experts, size, -1), 'sp', 0, 0, tiled=True)  10.7 us
    all_to_all x1, starting transfers between devices, shards(): back = lax.all_to_all(jnp.concatenate(sums, axis=1), 'sp', 0, 0, tiled=True)  10.1 us
    all_to_all x1, starting transfers between devices, shards(): carried = lax.all_to_all(carry, 'sp', 0, 0, tiled=True)  9.95 us
    pallas_call x1, Pallas kernels, gate_up_grads(): pl.pallas_call(functools.partial(gate_up_kernel, groups=len(saved)), grid...  9.24 us
    pallas_call x2, Pallas kernels, expert_forward(): pl.pallas_call(forward_kernel, grid=(rows // block,), in_specs=[pl.BlockS...  9.22 us
  transfers between devices with their start and end apart: 29, of which 16 were waited for; matrix products, arithmetic and copies ran while one was open for 8% of the time, Pallas kernels for 26%

profile of v5, /device:TPU:13, one launch (start us, length us, event | category | flops | bytes accessed | tf_op | source)
XLA Modules:
  0.0 228.2 jit_solution(741085377787498779)
XLA Ops:
  2.1 3.2 %dispatch.2 = bf16[768,512]{1,0:T(8,128)(2,1)} custom-call(s32[1]{0:T(128)} %bitcast.3._.rank_ref, s32[2,384]{1,0:T(2,128)S(1)} %bitcast.48, f32[2,384]{1,0:T(2,128)S(1)} %bitcast.50, bf16[384,2048]{1,0:T(8,128)(2,1)} %cot_ref.3), custom_call_target="tpu_custom_call" | custom-call | tf_op jit(solution)/shard_map/dispatch/pallas_call | solution.py:95
  5.4 8.8 %all-to-all-start = ((bf16[32,24,512]{2,1,0:T(8,128)(2,1)}), bf16[32,24,512]{2,1,0:T(8,128)(2,1)S(1)}, u32[]{:S(2)}, u32[]{:S(2)}) async-start(bf16[32,24,512]{2,1,0:T(8,128)(2,1)} %bitcast.58), calls=%async_computation | async-start | bytes 1572864 | tf_op jit(solution)/shard_map/all_to_all | solution.py:650
  16.9 10.7 %all-to-all-done = bf16[32,24,512]{2,1,0:T(8,128)(2,1)S(1)} async-done(((bf16[32,24,512]{2,1,0:T(8,128)(2,1)}), bf16[32,24,512]{2,1,0:T(8,128)(2,1)S(1)}, u32[]{:S(2)}, u32[]{:S(2)}) %all-to-all-start) | async-done | bytes 786464 | tf_op jit(solution)/shard_map/all_to_all | solution.py:650
  27.6 5.7 %all-to-all-start.1 = ((bf16[32,16,2048]{2,1,0:T(8,128)(2,1)}), bf16[32,16,2048]{2,1,0:T(8,128)(2,1)}, u32[]{:S(2)}, u32[]{:S(2)}) async-start(bf16[32,16,2048]{2,1,0:T(8,128)(2,1)} %bitcast.54), calls=%async_computation.1 | async-start | bytes 4194304 | tf_op jit(solution)/shard_map/all_to_all | solution.py:650
  36.4 7.5 %collective-permute-done.2.refs_5_ = bf16[768,256]{1,0:T(8,128)(2,1)S(1)} collective-permute-done((bf16[768,256]{1,0:T(8,128)(2,1)S(1)}, bf16[768,256]{1,0:T(8,128)(2,1)S(1)}, u32[]{:S(2)}, u32[]{:S(2)}) %collective-permute-start.2) | collective-permute-done | bytes 393248 | tf_op jit(solution)/shard_map/ppermute | solution.py:368
  47.7 4.1 %fetch.1 = (bf16[512,2048]{1,0:T(8,128)(2,1)S(1)}, bf16[2048,1024]{1,0:T(8,128)(2,1)S(1)}) custom-call(s32[1]{0:T(128)} %bitcast.3._.rank_ref, bf16[512,2048]{1,0:T(8,128)(2,1)} %bitcast.52, bf16[2048,512]{1,0:T(8,128)(2,1)} %bitcast.36, bf16[2048,512]{1,0:T(8,128)(2,1)} %bitcast.39), custom_call_target="tpu_custom_call" | custom-call | tf_op jit(solution)/shard_map/fetch/pallas_call | solution.py:139
  52.9 5.3 %expert_forward.2 = (bf16[768,512]{1,0:T(8,128)(2,1)}, f32[768,1024]{1,0:T(8,128)}) custom-call(bf16[768,2048]{1,0:T(8,128)(2,1)S(1)} %bitcast.34, bf16[2048,512]{1,0:T(8,128)(2,1)S(1)} %bitcast.38, bf16[2048,512]{1,0:T(8,128)(2,1)S(1)} %bitcast.41), custom_call_target="tpu_custom_call" | custom-call | tf_op jit(solution)/shard_map/expert_forward/pallas_call | solution.py:171
  63.4 6.5 %expert_backward.2 = (bf16[768,1024]{1,0:T(8,128)(2,1)}, bf16[768,512]{1,0:T(8,128)(2,1)}, bf16[768,512]{1,0:T(8,128)(2,1)}, bf16[768,256]{1,0:T(8,128)(2,1)}, b...) custom-call(s32[1]{0:T(128)} %bitcast.3._.rank_ref, bf16[768,512]{1,0:T(8,128)(2,1)S(1)} %bitcast.46, ...), custom_call_target="tpu_custom_call" | custom-call | tf_op jit(solution)/shard_map/expert_backward/pallas_call | solution.py:255
  74.2 3.9 %expert_forward.3 = (bf16[512,512]{1,0:T(8,128)(2,1)}, f32[512,1024]{1,0:T(8,128)}) custom-call(bf16[512,2048]{1,0:T(8,128)(2,1)S(1)} %bitcast.42, bf16[2048,1024]{1,0:T(8,128)(2,1)S(1)} %get-tuple-element.33.refs_9_.refs_0_), custom_call_target="tpu_custom_call" | custom-call | tf_op jit(solution)/shard_map/expert_forward/pallas_call | solution.py:171
  78.4 9.1 %expert_backward.3 = (bf16[512,1024]{1,0:T(8,128)(2,1)}, bf16[512,512]{1,0:T(8,128)(2,1)}, bf16[512,512]{1,0:T(8,128)(2,1)}, bf16[512,256]{1,0:T(8,128)(2,1)}, b...) custom-call(s32[1]{0:T(128)} %bitcast.3._.rank_ref, bf16[512,2048]{1,0:T(8,128)(2,1)} %bitcast.12.refs_0_.second, ...), custom_call_target="tpu_custom_call" | custom-call | tf_op jit(solution)/shard_map/expert_backward/pallas_call | solution.py:255
  94.0 5.3 %collective-permute-done.10 = bf16[512,512]{1,0:T(8,128)(2,1)S(1)} collective-permute-done((bf16[512,512]{1,0:T(8,128)(2,1)}, bf16[512,512]{1,0:T(8,128)(2,1)S(1)}, u32[]{:S(2)}, u32[]{:S(2)}) %collective-permute-start.10) | collective-permute-done | bytes 524320 | tf_op jit(solution)/shard_map/ppermute | solution.py:379
  101.7 6.0 %collective-permute-done.7 = bf16[768,256]{1,0:T(8,128)(2,1)S(1)} collective-permute-done((bf16[768,256]{1,0:T(8,128)(2,1)S(1)}, bf16[768,256]{1,0:T(8,128)(2,1)S(1)}, u32[]{:S(2)}, u32[]{:S(2)}) %collective-permute-start.7) | collective-permute-done | bytes 393248 | tf_op jit(solution)/shard_map/ppermute | solution.py:384
  110.3 3.0 %collective-permute-done.11 = bf16[512,256]{1,0:T(8,128)(2,1)S(1)} collective-permute-done((bf16[512,256]{1,0:T(8,128)(2,1)S(1)}, bf16[512,256]{1,0:T(8,128)(2,1)S(1)}, u32[]{:S(2)}, u32[]{:S(2)}) %collective-permute-start.11) | collective-permute-done | bytes 262176 | tf_op jit(solution)/shard_map/ppermute | solution.py:384
  116.9 10.1 %all-to-all-start.2 = ((bf16[32,40,512]{2,1,0:T(8,128)(2,1)}), bf16[32,40,512]{2,1,0:T(8,128)(2,1)S(1)}, u32[]{:S(2)}, u32[]{:S(2)}) async-start(bf16[32,40,512]{2,1,0:T(8,128)(2,1)} %pad_maximum_fusion), calls=%async_computation.2 | async-start | bytes 2621440 | tf_op jit(solution)/shard_map/all_to_all | solution.py:696
  127.1 4.1 %multiply_convert_fusion.2 = (bf16[384,512]{1,0:T(8,128)(2,1)S(1)}, bf16[384,512]{1,0:T(8,128)(2,1)}, bf16[384,512]{1,0:T(8,128)(2,1)}, bf16[384,512]{1,0:T(8,128)(2,1)}) fusion(bf16[384,512]{1,0:T(8,128)(2,1)} %refs_2_.1, f32[384,512]{1,0:T(8,128)} %param.27, bf16[384,512]{1,0:T(8,128)(2,1)S(1)} %copy-done.17, f32[384,256]{1,0:T(8,128)S(1)} %fusion.14, ...), kind=kLoop, calls=%fused_computation.26 | loop fusion | flops 7274496 | bytes 5508608 | tf_op jit(solution)/shard_map/convert_element_type | solution.py:678
  133.9 8.1 %collective-permute-done.15.below = bf16[384,512]{1,0:T(8,128)(2,1)S(1)} collective-permute-done((bf16[384,512]{1,0:T(8,128)(2,1)S(1)}, bf16[384,512]{1,0:T(8,128)(2,1)S(1)}, u32[]{:S(2)}, u32[]{:S(2)}) %collective-permute-start.15) | collective-permute-done | bytes 393248 | tf_op jit(solution)/shard_map/ppermute | solution.py:356
  159.2 6.7 %all-to-all-start.3 = ((bf16[16,64,512]{2,1,0:T(8,128)(2,1)}), bf16[16,64,512]{2,1,0:T(8,128)(2,1)S(1)}, u32[]{:S(2)}, u32[]{:S(2)}) async-start(bf16[16,64,512]{2,1,0:T(8,128)(2,1)} %bitcast.57), calls=%async_computation.3 | async-start | bytes 2097152 | tf_op jit(solution)/shard_map/all_to_all | solution.py:713
  169.8 6.5 %collective-permute-done.20.z1 = bf16[384,512]{1,0:T(8,128)(2,1)S(1)} collective-permute-done((bf16[384,512]{1,0:T(8,128)(2,1)S(1)}, bf16[384,512]{1,0:T(8,128)(2,1)S(1)}, u32[]{:S(2)}, u32[]{:S(2)}) %collective-permute-start.20) | collective-permute-done | bytes 393248 | tf_op jit(solution)/shard_map/ppermute | solution.py:356
  183.4 3.9 %state_grads.1 = (bf16[384,512]{1,0:T(8,128)(2,1)}, f32[384,512]{1,0:T(8,128)}, f32[32,16,128]{2,1,0:T(8,128)}) custom-call(s32[1]{0:T(128)} %bitcast.3._.rank_ref, bf16[384,512]{1,0:T(8,128)(2,1)S(1)} %combine.1.z_ref.z0, bf16[384,512]{1,0:T(8,128)(2,1)S(1)} %collective-permute-done.20.z1, bf16[384,512]{1,0:T(8,128)(2,1)S(1)} %collective-permute-done.21.z2, ...), custom_call_target="tpu_custom_call" | custom-call | tf_op jit(solution)/shard_map/state_grads/pallas_call | solution.py:460
  187.3 10.0 %all-to-all-start.4 = ((f32[32,16,128]{2,1,0:T(8,128)}), f32[32,16,128]{2,1,0:T(8,128)S(1)}, u32[]{:S(2)}, u32[]{:S(2)}) async-start(f32[32,16,128]{2,1,0:T(8,128)} %get-tuple-element.54), calls=%async_computation.4 | async-start | bytes 524288 | tf_op jit(solution)/shard_map/all_to_all | solution.py:735
  197.4 7.0 %collective-permute-start.19 = (f32[64,512]{1,0:T(8,128)S(1)}, f32[64,512]{1,0:T(8,128)S(1)}, u32[]{:S(2)}, u32[]{:S(2)}) collective-permute-start(f32[64,512]{1,0:T(8,128)S(1)} %convert_reduce_fusion), channel_id=1, source_target_pairs={{0,0},{1,32},{2,64},{3,96},{4,1},{5,33},{6,65},{7,97},{8,2},{9,34}... | collective-permute-start | bytes 393224 | tf_op jit(solution)/shard_map/ppermute | solution.py:721
  204.5 9.2 %gate_up_grads.1 = (bf16[2048,512]{1,0:T(8,128)(2,1)}, bf16[2048,512]{1,0:T(8,128)(2,1)}) custom-call(bf16[768,2048]{1,0:T(8,128)(2,1)} %bitcast.35, bf16[512,2048]{1,0:T(8,128)(2,1)} %bitcast.43, bf16[768,1024]{1,0:T(8,128)(2,1)} %get-tuple-element.34.refs_2_, bf16[512,1024]{1,0:T(8,128)(2,1)} %get-tuple-element.36.refs_3_), custom_call_target="tpu_custom_call" | custom-call | tf_op jit(solution)/shard_map/gate_up_grads/pallas_call | solution.py:290
  213.7 7.1 %down_grads.1 = bf16[512,2048]{1,0:T(8,128)(2,1)} custom-call(s32[1]{0:T(128)} %bitcast.3._.rank_ref, bf16[768,512]{1,0:T(8,128)(2,1)} %get-tuple-element.39.first_act, bf16[512,512]{1,0:T(8,128)(2,1)} %get-tuple-element.40.second_act, bf16[512,2048]{1,0:T(8,128)(2,1)} %bitcast.12.refs_0_.second, bf16[768,512]{1,0:T(8,128)(2,1)} %bitcast.45, ...), custom_call_target="tpu_custom_call" | custom-call | tf_op jit(solution)/shard_map/down_grads/pallas_call | solution.py:334
  221.5 6.0 %final_grads.1 = bf16[384,512]{1,0:T(8,128)(2,1)} custom-call(s32[1]{0:T(128)} %bitcast.16.me_ref, f32[32,16,128]{2,1,0:T(8,128)} %copy-done.27, f32[384,512]{1,0:T(8,128)} %get-tuple-element.55.refs_1_, f32[384,512]{1,0:T(8,128)} %get-tuple-element.63.refs_3_.refs_2_, bf16[384,512]{1,0:T(8,128)(2,1)} %get-tuple-element.59.refs_3_, ...), custom_call_target="tpu_custom_call" | custom-call | tf_op jit(solution)/shard_map/final_grads/pallas_call | solution.py:575
  (157 shorter events, 69.1 us)
Async XLA Ops:
  5.4 22.3 %all-to-all-start = ((bf16[32,24,512]{2,1,0:T(8,128)(2,1)}), bf16[32,24,512]{2,1,0:T(8,128)(2,1)S(1)}, u32[]{:S(2)}, u32[]{:S(2)}) async-start(bf16[32,24,512]{2,1,0:T(8,128)(2,1)} %bitcast.58), calls=%async_computation | async-start | bytes 1572864 | tf_op jit(solution)/shard_map/all_to_all | solution.py:650
  27.6 50.7 %all-to-all-start.1 = ((bf16[32,16,2048]{2,1,0:T(8,128)(2,1)}), bf16[32,16,2048]{2,1,0:T(8,128)(2,1)}, u32[]{:S(2)}, u32[]{:S(2)}) async-start(bf16[32,16,2048]{2,1,0:T(8,128)(2,1)} %bitcast.54), calls=%async_computation.1 | async-start | bytes 4194304 | tf_op jit(solution)/shard_map/all_to_all | solution.py:650
  33.4 10.5 %collective-permute-start.2 = (bf16[768,256]{1,0:T(8,128)(2,1)S(1)}, bf16[768,256]{1,0:T(8,128)(2,1)S(1)}, u32[]{:S(2)}, u32[]{:S(2)}) collective-permute-start(bf16[768,256]{1,0:T(8,128)(2,1)S(1)} %get-tuple-element.66), channel_id=1, source_target_pairs={{0,1},{1,2},{2,3},{3,0},{4,5},{5,6},{6,7},{7,4},{8,9},{9,10},{10,1... | collective-permute-start | bytes 1179656 | tf_op jit(solution)/shard_map/ppermute | solution.py:368
  34.4 10.4 %collective-permute-start.1 = (bf16[768,256]{1,0:T(8,128)(2,1)S(1)}, bf16[768,256]{1,0:T(8,128)(2,1)S(1)}, u32[]{:S(2)}, u32[]{:S(2)}) collective-permute-start(bf16[768,256]{1,0:T(8,128)(2,1)S(1)} %get-tuple-element.65), channel_id=1, source_target_pairs={{0,3},{1,0},{2,1},{3,2},{4,7},{5,4},{6,5},{7,6},{8,11},{9,8},{10,9... | collective-permute-start | bytes 1179656 | tf_op jit(solution)/shard_map/ppermute | solution.py:369
  34.9 23.2 %collective-permute-start = (bf16[768,256]{1,0:T(8,128)(2,1)S(1)}, bf16[768,256]{1,0:T(8,128)(2,1)S(1)}, u32[]{:S(2)}, u32[]{:S(2)}) collective-permute-start(bf16[768,256]{1,0:T(8,128)(2,1)S(1)} %get-tuple-element.66), channel_id=1, source_target_pairs={{0,3},{1,0},{2,1},{3,2},{4,7},{5,4},{6,5},{7,6},{8,11},{9,8},{10,9... | collective-permute-start | bytes 1179656 | tf_op jit(solution)/shard_map/ppermute | solution.py:371
  35.2 23.0 %collective-permute-start.5 = (bf16[768,256]{1,0:T(8,128)(2,1)S(1)}, bf16[768,256]{1,0:T(8,128)(2,1)S(1)}, u32[]{:S(2)}, u32[]{:S(2)}) collective-permute-start(bf16[768,256]{1,0:T(8,128)(2,1)S(1)} %get-tuple-element.65), channel_id=1, source_target_pairs={{0,1},{1,2},{2,3},{3,0},{4,5},{5,6},{6,7},{7,4},{8,9},{9,10},{10,1... | collective-permute-start | bytes 1179656 | tf_op jit(solution)/shard_map/ppermute | solution.py:370
  43.9 16.9 %collective-permute-start.3 = (bf16[768,256]{1,0:T(8,128)(2,1)S(1)}, bf16[768,256]{1,0:T(8,128)(2,1)S(1)}, u32[]{:S(2)}, u32[]{:S(2)}) collective-permute-start(bf16[768,256]{1,0:T(8,128)(2,1)S(1)} %collective-permute-done.2.refs_5_), channel_id=1, source_target_pairs={{0,1},{1,2},{2,3},{3,0},{4,5},{5,6},{6,7},{7,4},{8,9},{9,10},{10,1... | collective-permute-start | bytes 1179656 | tf_op jit(solution)/shard_map/ppermute | solution.py:372
  44.8 16.6 %collective-permute-start.4 = (bf16[768,256]{1,0:T(8,128)(2,1)S(1)}, bf16[768,256]{1,0:T(8,128)(2,1)S(1)}, u32[]{:S(2)}, u32[]{:S(2)}) collective-permute-start(bf16[768,256]{1,0:T(8,128)(2,1)S(1)} %collective-permute-done.1.refs_2_), channel_id=1, source_target_pairs={{0,3},{1,0},{2,1},{3,2},{4,7},{5,4},{6,5},{7,6},{8,11},{9,8},{10,9... | collective-permute-start | bytes 1179656 | tf_op jit(solution)/shard_map/ppermute | solution.py:373
  70.0 20.0 %collective-permute-start.6 = (bf16[768,512]{1,0:T(8,128)(2,1)}, bf16[768,512]{1,0:T(8,128)(2,1)S(1)}, u32[]{:S(2)}, u32[]{:S(2)}) collective-permute-start(bf16[768,512]{1,0:T(8,128)(2,1)} %get-tuple-element.43), channel_id=1, source_target_pairs={{0,1},{1,2},{2,3},{3,0},{4,5},{5,6},{6,7},{7,4},{8,9},{9,10},{10,1... | collective-permute-start | bytes 2359304 | tf_op jit(solution)/shard_map/ppermute | solution.py:379
  71.6 20.1 %collective-permute-start.8 = (bf16[768,512]{1,0:T(8,128)(2,1)}, bf16[768,512]{1,0:T(8,128)(2,1)}, u32[]{:S(2)}, u32[]{:S(2)}) collective-permute-start(bf16[768,512]{1,0:T(8,128)(2,1)} %get-tuple-element.45), channel_id=1, source_target_pairs={{0,3},{1,0},{2,1},{3,2},{4,7},{5,4},{6,5},{7,6},{8,11},{9,8},{10,9... | collective-permute-start | bytes 2359304 | tf_op jit(solution)/shard_map/ppermute | solution.py:380
  87.5 11.8 %collective-permute-start.10 = (bf16[512,512]{1,0:T(8,128)(2,1)}, bf16[512,512]{1,0:T(8,128)(2,1)S(1)}, u32[]{:S(2)}, u32[]{:S(2)}) collective-permute-start(bf16[512,512]{1,0:T(8,128)(2,1)} %get-tuple-element.48), channel_id=1, source_target_pairs={{0,1},{1,2},{2,3},{3,0},{4,5},{5,6},{6,7},{7,4},{8,9},{9,10},{10,1... | collective-permute-start | bytes 1572872 | tf_op jit(solution)/shard_map/ppermute | solution.py:379
  89.8 11.7 %collective-permute-start.12 = (bf16[512,512]{1,0:T(8,128)(2,1)}, bf16[512,512]{1,0:T(8,128)(2,1)S(1)}, u32[]{:S(2)}, u32[]{:S(2)}) collective-permute-start(bf16[512,512]{1,0:T(8,128)(2,1)} %get-tuple-element.50), channel_id=1, source_target_pairs={{0,3},{1,0},{2,1},{3,2},{4,7},{5,4},{6,5},{7,6},{8,11},{9,8},{10,9... | collective-permute-start | bytes 1572872 | tf_op jit(solution)/shard_map/ppermute | solution.py:380
  90.1 17.6 %collective-permute-start.7 = (bf16[768,256]{1,0:T(8,128)(2,1)S(1)}, bf16[768,256]{1,0:T(8,128)(2,1)S(1)}, u32[]{:S(2)}, u32[]{:S(2)}) collective-permute-start(bf16[768,256]{1,0:T(8,128)(2,1)S(1)} %add_convert_fusion.5), channel_id=1, source_target_pairs={{0,1},{1,2},{2,3},{3,0},{4,5},{5,6},{6,7},{7,4},{8,9},{9,10},{10,1... | collective-permute-start | bytes 1179656 | tf_op jit(solution)/shard_map/ppermute | solution.py:384
  92.8 17.1 %collective-permute-start.9 = (bf16[768,256]{1,0:T(8,128)(2,1)S(1)}, bf16[768,256]{1,0:T(8,128)(2,1)S(1)}, u32[]{:S(2)}, u32[]{:S(2)}) collective-permute-start(bf16[768,256]{1,0:T(8,128)(2,1)S(1)} %add_convert_fusion.4), channel_id=1, source_target_pairs={{0,3},{1,0},{2,1},{3,2},{4,7},{5,4},{6,5},{7,6},{8,11},{9,8},{10,9... | collective-permute-start | bytes 1179656 | tf_op jit(solution)/shard_map/ppermute | solution.py:385
  99.4 14.0 %collective-permute-start.11 = (bf16[512,256]{1,0:T(8,128)(2,1)S(1)}, bf16[512,256]{1,0:T(8,128)(2,1)S(1)}, u32[]{:S(2)}, u32[]{:S(2)}) collective-permute-start(bf16[512,256]{1,0:T(8,128)(2,1)S(1)} %add_convert_fusion.7), channel_id=1, source_target_pairs={{0,1},{1,2},{2,3},{3,0},{4,5},{5,6},{6,7},{7,4},{8,9},{9,10},{10,1... | collective-permute-start | bytes 786440 | tf_op jit(solution)/shard_map/ppermute | solution.py:384
  101.6 14.0 %collective-permute-start.13 = (bf16[512,256]{1,0:T(8,128)(2,1)S(1)}, bf16[512,256]{1,0:T(8,128)(2,1)S(1)}, u32[]{:S(2)}, u32[]{:S(2)}) collective-permute-start(bf16[512,256]{1,0:T(8,128)(2,1)S(1)} %add_convert_fusion.6), channel_id=1, source_target_pairs={{0,3},{1,0},{2,1},{3,2},{4,7},{5,4},{6,5},{7,6},{8,11},{9,8},{10,9... | collective-permute-start | bytes 786440 | tf_op jit(solution)/shard_map/ppermute | solution.py:385
  116.9 30.4 %all-to-all-start.2 = ((bf16[32,40,512]{2,1,0:T(8,128)(2,1)}), bf16[32,40,512]{2,1,0:T(8,128)(2,1)S(1)}, u32[]{:S(2)}, u32[]{:S(2)}) async-start(bf16[32,40,512]{2,1,0:T(8,128)(2,1)} %pad_maximum_fusion), calls=%async_computation.2 | async-start | bytes 2621440 | tf_op jit(solution)/shard_map/all_to_all | solution.py:696
  131.3 10.8 %collective-permute-start.15 = (bf16[384,512]{1,0:T(8,128)(2,1)S(1)}, bf16[384,512]{1,0:T(8,128)(2,1)S(1)}, u32[]{:S(2)}, u32[]{:S(2)}) collective-permute-start(bf16[384,512]{1,0:T(8,128)(2,1)S(1)} %get-tuple-element.56.own), channel_id=1, source_target_pairs={{0,1},{1,2},{2,3},{3,0},{4,5},{5,6},{6,7},{7,4},{8,9},{9,10},{10,1... | collective-permute-start | bytes 1179656 | tf_op jit(solution)/shard_map/ppermute | solution.py:356
  133.9 11.0 %collective-permute-start.14 = (bf16[384,512]{1,0:T(8,128)(2,1)S(1)}, bf16[384,512]{1,0:T(8,128)(2,1)S(1)}, u32[]{:S(2)}, u32[]{:S(2)}) collective-permute-start(bf16[384,512]{1,0:T(8,128)(2,1)S(1)} %get-tuple-element.56.own), channel_id=1, source_target_pairs={{0,3},{1,0},{2,1},{3,2},{4,7},{5,4},{6,5},{7,6},{8,11},{9,8},{10,9... | collective-permute-start | bytes 1179656 | tf_op jit(solution)/shard_map/ppermute | solution.py:357
  159.2 28.1 %all-to-all-start.3 = ((bf16[16,64,512]{2,1,0:T(8,128)(2,1)}), bf16[16,64,512]{2,1,0:T(8,128)(2,1)S(1)}, u32[]{:S(2)}, u32[]{:S(2)}) async-start(bf16[16,64,512]{2,1,0:T(8,128)(2,1)} %bitcast.57), calls=%async_computation.3 | async-start | bytes 2097152 | tf_op jit(solution)/shard_map/all_to_all | solution.py:713
  166.0 10.3 %collective-permute-start.20 = (bf16[384,512]{1,0:T(8,128)(2,1)S(1)}, bf16[384,512]{1,0:T(8,128)(2,1)S(1)}, u32[]{:S(2)}, u32[]{:S(2)}) collective-permute-start(bf16[384,512]{1,0:T(8,128)(2,1)S(1)} %combine.1.z_ref.z0), channel_id=1, source_target_pairs={{0,1},{1,2},{2,3},{3,0},{4,5},{5,6},{6,7},{7,4},{8,9},{9,10},{10,1... | collective-permute-start | bytes 1179656 | tf_op jit(solution)/shard_map/ppermute | solution.py:356
  168.7 9.8 %collective-permute-start.21 = (bf16[384,512]{1,0:T(8,128)(2,1)S(1)}, bf16[384,512]{1,0:T(8,128)(2,1)S(1)}, u32[]{:S(2)}, u32[]{:S(2)}) collective-permute-start(bf16[384,512]{1,0:T(8,128)(2,1)S(1)} %combine.1.z_ref.z0), channel_id=1, source_target_pairs={{0,3},{1,0},{2,1},{3,2},{4,7},{5,4},{6,5},{7,6},{8,11},{9,8},{10,9... | collective-permute-start | bytes 1179656 | tf_op jit(solution)/shard_map/ppermute | solution.py:357
  187.3 33.5 %all-to-all-start.4 = ((f32[32,16,128]{2,1,0:T(8,128)}), f32[32,16,128]{2,1,0:T(8,128)S(1)}, u32[]{:S(2)}, u32[]{:S(2)}) async-start(f32[32,16,128]{2,1,0:T(8,128)} %get-tuple-element.54), calls=%async_computation.4 | async-start | bytes 524288 | tf_op jit(solution)/shard_map/all_to_all | solution.py:735
  197.4 30.1 %collective-permute-start.19 = (f32[64,512]{1,0:T(8,128)S(1)}, f32[64,512]{1,0:T(8,128)S(1)}, u32[]{:S(2)}, u32[]{:S(2)}) collective-permute-start(f32[64,512]{1,0:T(8,128)S(1)} %convert_reduce_fusion), channel_id=1, source_target_pairs={{0,0},{1,32},{2,64},{3,96},{4,1},{5,33},{6,65},{7,97},{8,2},{9,34}... | collective-permute-start | bytes 393224 | tf_op jit(solution)/shard_map/ppermute | solution.py:721
  (44 other events, 510.9 us)
